TPU v7x, 256 devices: a whole 4x4x8 slice. The times are simulated.
256 devices in a mesh: ep: 128 (over z, y, x), tp: 2 (over core).
Axes of the slice: x: 4, y: 4, z: 8, core: 2. Of those that a mesh axis runs over, the one named last changes fastest.
Arguments:
- tokens: bfloat16 [8192, 1024], P('ep', 'tp'), may hold values from -6 to 6
- norm_gain: float32 [1024], P('tp'), may hold values from 0.1 to 1.9
- routing: int32 [8192, 2], P('ep'), may hold values from 0 to 255, as said below
- route_weight: float32 [8192, 2], P('ep'), may hold values from 0.25 to 1
- w_gate: bfloat16 [256, 1024, 512], P('ep', None, 'tp'), may hold values from -0.1875 to 0.1875
- w_up: bfloat16 [256, 1024, 512], P('ep', None, 'tp'), may hold values from -0.1875 to 0.1875
- w_down: bfloat16 [256, 512, 1024], P('ep', None, 'tp'), may hold values from -0.25 to 0.25
Outputs:
- mixed: bfloat16 [8192, 1024], P('ep', 'tp')
Inputs may be any that keep to these rules, and one draw needn't show every extreme that they name: `routing`: each row names 2 different experts, all in the same group of 8 consecutive expert numbers. Among the rows of one device (aligned blocks of 64 rows) no expert is named more than 8 times, and in every block some expert is named exactly 8 times.
All inputs are finite; a program needn't handle non-finite values.
Results may differ from a plain program's by a relative error of at most 0.0015.
Values may be sent and summed in bfloat16 or wider, within the bound.
No kernel may reach another device: no remote copies, remote signals or barrier semaphores. Data moves between devices by JAX's collectives and lax.ppermute only.
A program may use at most 64 MiB of HBM per device.

v0:
```python
import jax
import jax.numpy as jnp
from jax import lax
from jax.sharding import PartitionSpec as P

CAP = 8


epsilon = 1e-06


def taken_in(shard, axis, dim, update, carry):
    whole = jax.tree.map(lambda part: lax.all_gather(part, axis, axis=dim, tiled=True), shard)
    return update(carry, whole, jnp.int32(0))


def total_of_pieces(shard, axis):
    pieces = lax.all_gather(shard, axis)
    return pieces.sum(axis=0)


def expert_rows(arrivals, gate_weight, up_weight, down_weight):
    row_total = arrivals.shape[0]
    hidden_half = gate_weight.shape[1]
    half_width = down_weight.shape[1]
    zero_acc = jnp.zeros((row_total, hidden_half), jnp.float32)

    def add_feature(totals, block_part, offset):
        span = block_part.shape[1]
        gate_rows = lax.dynamic_slice_in_dim(gate_weight, offset, span, 0)
        up_rows = lax.dynamic_slice_in_dim(up_weight, offset, span, 0)
        return (
            totals[0] + jnp.dot(block_part, gate_rows, preferred_element_type=jnp.float32),
            totals[1] + jnp.dot(block_part, up_rows, preferred_element_type=jnp.float32),
        )

    gate_acc, up_acc = taken_in(arrivals, "tp", 1, add_feature, (zero_acc, zero_acc))
    hidden = (jax.nn.silu(gate_acc) * up_acc).astype(jnp.bfloat16)

    def add_hidden(totals, block_part, offset):
        down_rows = lax.dynamic_slice_in_dim(down_weight, offset, block_part.shape[1], 0)
        return totals + jnp.dot(block_part, down_rows, preferred_element_type=jnp.float32)

    result = taken_in(hidden, "tp", 1, add_hidden, jnp.zeros((row_total, half_width), jnp.float32))
    return result.astype(jnp.bfloat16)


def local(tokens, norm_gain, routing, route_weight, w_gate, w_up, w_down):
    tok_rows, half_width = tokens.shape
    float_rows = tokens.astype(jnp.float32)
    square_sum = jnp.sum(float_rows * float_rows, axis=1)
    total_squares = total_of_pieces(square_sum, "tp")
    full_width = half_width * lax.axis_size("tp")
    scale = lax.rsqrt(total_squares[:, None] / full_width + epsilon)
    normed = (float_rows * scale * norm_gain[None, :]).astype(jnp.bfloat16)
    peer_count = lax.axis_size("ep")
    local_experts = w_gate.shape[0]
    experts = local_experts * peer_count
    pick_count = routing.shape[1]
    flat_expert = routing.reshape(-1).astype(jnp.int32)
    onehot = (flat_expert[:, None] == jnp.arange(experts, dtype=jnp.int32)[None, :]).astype(
        jnp.int32
    )
    earlier = jnp.cumsum(onehot, axis=0).astype(jnp.int32) - onehot
    slot_index = jnp.sum(earlier * onehot, axis=1).astype(jnp.int32)
    target = flat_expert * CAP + slot_index
    source_rows = jnp.repeat(normed, pick_count, axis=0)
    outgoing = jnp.zeros((experts * CAP, half_width), jnp.bfloat16).at[target].set(source_rows)
    outgoing = outgoing.reshape(peer_count, local_experts, CAP, half_width)
    pieces_back = []
    for local_index in range(local_experts):
        arrived = lax.all_to_all(
            outgoing[:, local_index], "ep", split_axis=0, concat_axis=0, tiled=True
        )
        arrivals = arrived.reshape(peer_count * CAP, half_width)
        result = expert_rows(arrivals, w_gate[local_index], w_up[local_index], w_down[local_index])
        pieces_back.append(
            lax.all_to_all(
                result.reshape(peer_count, CAP, half_width),
                "ep",
                split_axis=0,
                concat_axis=0,
                tiled=True,
            )
        )
    returned = jnp.stack(pieces_back, axis=1)
    returned_rows = returned.reshape(experts * CAP, half_width)
    gathered = returned_rows[target].astype(jnp.float32) * route_weight.reshape(-1)[:, None]
    combined = jnp.sum(gathered.reshape(tok_rows, pick_count, half_width), axis=1)
    return combined.astype(jnp.bfloat16)


def solution(mesh):
    in_specs = (
        P("ep", "tp"),
        P("tp"),
        P("ep", None),
        P("ep", None),
        P("ep", None, "tp"),
        P("ep", None, "tp"),
        P("ep", None, "tp"),
    )
    out_specs = P("ep", "tp")
    return jax.shard_map(local, mesh=mesh, in_specs=in_specs, out_specs=out_specs, check_vma=False)
```

profile of v0, /device:TPU:32, one launch (start us, length us, event | category | flops | bytes accessed | tf_op | source)
XLA Modules:
  0.0 190.8 jit_solution(8570603322791456019)
XLA Ops:
  6.5 0.0 all-gather.6.cloned.1.call-start
  6.5 0.8 copy.13
  7.3 0.7 broadcast_multiply_fusion
  8.0 0.1 eq.15
  8.1 0.1 fusion.23
  8.2 0.2 reduce_window_sum.11
  8.4 0.2 select_reduce_fusion
  8.6 0.1 copy.12
  8.7 0.1 mul.62
  8.8 1.0 fusion.20
  9.8 1.3 dynamic-slice
  11.7 0.2 dynamic-update-slice
  12.0 2.4 %all-reduce = f32[128]{0:T(128)S(1)} all-reduce(f32[128]{0:T(128)S(1)} %dynamic-update-slice), channel_id=2, replica_groups=mesh['ep'=128,'tp'=2] {'tp'}, use_global_device_ids=true, to_apply=%add | all-reduce | flops 128 | bytes 1024
  14.4 0.1 reshape.94
  14.5 0.9 fusion.22
  15.5 0.1 broadcast_in_dim.5
  15.5 0.1 reshape.90
  15.6 1.9 scatter_custom_fusion
  17.5 1.2 slice_bitcast_fusion.1
  18.6 46.6 %all_to_all.20 = bf16[128,8,512]{2,1,0:T(8,128)(2,1)} all-to-all(bf16[128,8,512]{2,1,0:T(8,128)(2,1)S(1)} %get-tuple-element.5), channel_id=1, replica_groups=mesh['ep'=128,'tp'=2] {'ep'}, dimensions={0} | all-to-all | bytes 2097152 | tf_op jit(solution)/shard_map/all_to_all | solution.py:72
  65.2 0.0 copy-start.4
  65.2 0.0 all-gather.6.cloned.1.call-update
  65.3 6.3 %all-to-all-start.2 = ((bf16[128,8,512]{2,1,0:T(8,128)(2,1)}), bf16[128,8,512]{2,1,0:T(8,128)(2,1)S(1)}, u32[]{:S(2)}, u32[]{:S(2)}) async-start(bf16[128,8,512]{2,1,0:T(8,128)(2,1)} %get-tuple-element.6), calls=%async_computation.2 | async-start | bytes 2097152 | tf_op jit(solution)/shard_map/all_to_all | solution.py:72
  71.6 0.0 copy-start.5
  71.6 0.0 all-gather.8.cloned.1.call-start
  71.6 3.0 %all-gather.6.cloned.1.call-done = bf16[1024,1024]{1,0:T(8,128)(2,1)} async-done(((bf16[1024,512]{1,0:T(8,128)(2,1)}), bf16[1024,1024]{1,0:T(8,128)(2,1)}) %all-gather.6.cloned.1.call-update) | async-done | bytes 2097168 | tf_op jit(solution)/shard_map/all_gather | solution.py:13
  74.7 0.0 copy-done.4
  74.7 0.0 copy-start.3
  74.7 2.5 %fusion.12 = f32[1024,256]{1,0:T(8,128)S(1)} fusion(bf16[1024,1024]{1,0:T(8,128)(2,1)} %all-gather.6.cloned.1.call-done, bf16[2,1024,256]{2,1,0:T(8,128)(2,1)S(1)} %copy-done.4), kind=kOutput, calls=%fused_computation.21 | convolution fusion | flops 536870912 | bytes 3670016 | tf_op jit(solution)/shard_map/dot_general | solution.py:33
  77.1 0.0 copy-done.5
  77.1 0.0 copy-done.3
  77.1 1.6 fusion.2
  78.7 0.0 all-gather.8.cloned.1.call-update
  78.7 0.0 all-gather.10.cloned.1.call-start
  78.8 23.4 %all-to-all-done.2 = bf16[128,8,512]{2,1,0:T(8,128)(2,1)S(1)} async-done(((bf16[128,8,512]{2,1,0:T(8,128)(2,1)}), bf16[128,8,512]{2,1,0:T(8,128)(2,1)S(1)}, u32[]{:S(2)}, u32[]{:S(2)}) %all-to-all-start.2) | async-done | bytes 1048608 | tf_op jit(solution)/shard_map/all_to_all | solution.py:72
  102.1 0.0 copy-start
  102.1 1.0 copy-done
  103.1 0.0 all-gather.10.cloned.1.call-update
  103.1 0.0 all-gather.8.cloned.1.call-done
  103.2 3.0 %fusion = bf16[128,8,512]{2,1,0:T(8,128)(2,1)} fusion(bf16[1024,512]{1,0:T(8,128)(2,1)} %all-gather.8.cloned.1.call-done, bf16[2,512,512]{2,1,0:T(8,128)(2,1)} %param.13), kind=kOutput, calls=%fused_computation.5 | convolution fusion | flops 537395200 | bytes 2621440 | tf_op jit(solution)/shard_map/dot_general | solution.py:42
  106.2 6.2 %all-to-all-start.1 = ((bf16[128,8,512]{2,1,0:T(8,128)(2,1)}), bf16[128,8,512]{2,1,0:T(8,128)(2,1)S(1)}, u32[]{:S(2)}, u32[]{:S(2)}) async-start(bf16[128,8,512]{2,1,0:T(8,128)(2,1)} %fusion), calls=%async_computation.1 | async-start | bytes 2097152 | tf_op jit(solution)/shard_map/all_to_all | solution.py:78
  112.5 0.2 all-gather.12.cloned.1.call-start
  112.7 0.7 all-gather.10.cloned.1.call-done
  113.4 0.0 copy-start.2
  113.4 2.5 %fusion.8 = f32[1024,256]{1,0:T(8,128)S(1)} fusion(bf16[1024,1024]{1,0:T(8,128)(2,1)} %all-gather.10.cloned.1.call-done, bf16[2,1024,256]{2,1,0:T(8,128)(2,1)S(1)} %copy-done.4), kind=kOutput, calls=%fused_computation.17 | convolution fusion | flops 536870912 | bytes 3670016 | tf_op jit(solution)/shard_map/dot_general | solution.py:33
  115.8 0.0 copy-done.2
  115.8 1.6 fusion.3
  117.4 0.0 all-gather.12.cloned.1.call-update
  117.4 0.0 copy-start.1
  117.4 15.6 %all-gather.12.cloned.1.call-done = bf16[1024,512]{1,0:T(8,128)(2,1)} async-done(((bf16[1024,256]{1,0:T(8,128)(2,1)}), bf16[1024,512]{1,0:T(8,128)(2,1)}) %all-gather.12.cloned.1.call-update) | async-done | bytes 1048592 | tf_op jit(solution)/shard_map/all_gather | solution.py:13
  133.0 3.1 %fusion.1 = bf16[128,8,512]{2,1,0:T(8,128)(2,1)} fusion(bf16[1024,512]{1,0:T(8,128)(2,1)} %all-gather.12.cloned.1.call-done, bf16[2,512,512]{2,1,0:T(8,128)(2,1)} %param.13), kind=kOutput, calls=%fused_computation.6 | convolution fusion | flops 537395200 | bytes 2621440 | tf_op jit(solution)/shard_map/dot_general | solution.py:42
  136.1 6.9 %all-to-all-done.1 = bf16[128,8,512]{2,1,0:T(8,128)(2,1)S(1)} async-done(((bf16[128,8,512]{2,1,0:T(8,128)(2,1)}), bf16[128,8,512]{2,1,0:T(8,128)(2,1)S(1)}, u32[]{:S(2)}, u32[]{:S(2)}) %all-to-all-start.1) | async-done | bytes 1048608 | tf_op jit(solution)/shard_map/all_to_all | solution.py:78
  143.0 6.8 %all-to-all-start.3 = ((bf16[128,8,512]{2,1,0:T(8,128)(2,1)}), bf16[128,8,512]{2,1,0:T(8,128)(2,1)S(1)}, u32[]{:S(2)}, u32[]{:S(2)}) async-start(bf16[128,8,512]{2,1,0:T(8,128)(2,1)} %fusion.1), calls=%async_computation.3 | async-start | bytes 2097152 | tf_op jit(solution)/shard_map/all_to_all | solution.py:78
  149.8 0.0 copy-done.1
  149.8 0.1 copy.15
  149.9 31.8 %all-to-all-done.3 = bf16[128,8,512]{2,1,0:T(8,128)(2,1)S(1)} async-done(((bf16[128,8,512]{2,1,0:T(8,128)(2,1)}), bf16[128,8,512]{2,1,0:T(8,128)(2,1)S(1)}, u32[]{:S(2)}, u32[]{:S(2)}) %all-to-all-start.3) | async-done | bytes 1048608 | tf_op jit(solution)/shard_map/all_to_all | solution.py:78
  181.7 0.2 pad_maximum_fusion
  181.9 0.2 copy.14
  182.2 0.9 gather_fusion
  183.0 0.2 reshape.77
  183.2 1.0 multiply_reduce_fusion
  (5 shorter events, 0.0 us)
Async XLA Ops:
  6.5 68.1 %all-gather.6.cloned.1.call-start = ((), (), s32[]{:S(2)}) async-start(), calls=%async_computation.4 | async-start | bytes 3145728 | tf_op jit(solution)/shard_map/all_gather | solution.py:13
  65.2 9.4 %copy-start.4 = (bf16[2,1024,256]{2,1,0:T(8,128)(2,1)S(1)}, bf16[2,1024,256]{2,1,0:T(8,128)(2,1)}, u32[]{:S(2)}) copy-start(bf16[2,1024,256]{2,1,0:T(8,128)(2,1)} %param.11) | copy-start | bytes 3145732
  65.3 36.9 %all-to-all-start.2 = ((bf16[128,8,512]{2,1,0:T(8,128)(2,1)}), bf16[128,8,512]{2,1,0:T(8,128)(2,1)S(1)}, u32[]{:S(2)}, u32[]{:S(2)}) async-start(bf16[128,8,512]{2,1,0:T(8,128)(2,1)} %get-tuple-element.6), calls=%async_computation.2 | async-start | bytes 2097152 | tf_op jit(solution)/shard_map/all_to_all | solution.py:72
  71.6 5.6 %copy-start.5 = (bf16[2,1024,256]{2,1,0:T(8,128)(2,1)S(1)}, bf16[2,1024,256]{2,1,0:T(8,128)(2,1)}, u32[]{:S(2)}) copy-start(bf16[2,1024,256]{2,1,0:T(8,128)(2,1)} %param.12) | copy-start | bytes 3145732
  71.6 31.6 %all-gather.8.cloned.1.call-start = ((), (), s32[]{:S(2)}) async-start(), calls=%async_computation.5 | async-start | bytes 1572864 | tf_op jit(solution)/shard_map/all_gather | solution.py:13
  74.7 2.5 %copy-start.3 = (bf16[1024,1024]{1,0:T(8,128)(2,1)S(1)}, bf16[1024,1024]{1,0:T(8,128)(2,1)}, u32[]{:S(2)}) copy-start(bf16[1024,1024]{1,0:T(8,128)(2,1)} %all-gather.6.cloned.1.call-done) | copy-start | bytes 6291460
  78.7 34.6 %all-gather.10.cloned.1.call-start = ((), (), s32[]{:S(2)}) async-start(), calls=%async_computation.6 | async-start | bytes 3145728 | tf_op jit(solution)/shard_map/all_gather | solution.py:13
  102.1 1.0 copy-start
  106.2 36.8 %all-to-all-start.1 = ((bf16[128,8,512]{2,1,0:T(8,128)(2,1)}), bf16[128,8,512]{2,1,0:T(8,128)(2,1)S(1)}, u32[]{:S(2)}, u32[]{:S(2)}) async-start(bf16[128,8,512]{2,1,0:T(8,128)(2,1)} %fusion), calls=%async_computation.1 | async-start | bytes 2097152 | tf_op jit(solution)/shard_map/all_to_all | solution.py:78
  112.5 20.5 %all-gather.12.cloned.1.call-start = ((), (), s32[]{:S(2)}) async-start(), calls=%async_computation.7 | async-start | bytes 1572864 | tf_op jit(solution)/shard_map/all_gather | solution.py:13
  113.4 2.5 %copy-start.2 = (bf16[1024,1024]{1,0:T(8,128)(2,1)S(1)}, bf16[1024,1024]{1,0:T(8,128)(2,1)}, u32[]{:S(2)}) copy-start(bf16[1024,1024]{1,0:T(8,128)(2,1)} %all-gather.10.cloned.1.call-done) | copy-start | bytes 6291460
  117.4 32.4 %copy-start.1 = (f32[64,2]{0,1:T(2,128)S(1)}, f32[64,2]{0,1:T(2,128)}, u32[]{:S(2)}) copy-start(f32[64,2]{0,1:T(2,128)} %param.10) | copy-start | bytes 1540
  143.0 38.7 %all-to-all-start.3 = ((bf16[128,8,512]{2,1,0:T(8,128)(2,1)}), bf16[128,8,512]{2,1,0:T(8,128)(2,1)S(1)}, u32[]{:S(2)}, u32[]{:S(2)}) async-start(bf16[128,8,512]{2,1,0:T(8,128)(2,1)} %fusion.1), calls=%async_computation.3 | async-start | bytes 2097152 | tf_op jit(solution)/shard_map/all_to_all | solution.py:78
Sparse Core Ops, SparseCore 0:
  65.4 9.2 all-gather.5
  78.8 15.4 all-gather.7
  103.3 10.0 all-gather.9
  117.5 15.4 all-gather.11
where the time goes:
time: 191 us
  waiting for transfers between devices  81.5 us (43%)
  blocking collectives  49 us (26%)
  starting transfers between devices  19.6 us (10%)
  matrix products  14.1 us (7%)
  between operations  14 us (7%)
  local copies, waits for them, and re-layouts  8.27 us (4%)
  other arithmetic  4.27 us (2%)
    all_to_all x1, blocking collectives, local(): lax.all_to_all(outgoing[:, local_index], 'ep', split_axis=0, concat_axis=...  46.6 us
    all_to_all x2, waiting for transfers between devices, local(): lax.all_to_all(result.reshape(peer_count, CAP, half_width), 'ep', split_a...  38.7 us
    all_to_all x1, waiting for transfers between devices, local(): lax.all_to_all(outgoing[:, local_index], 'ep', split_axis=0, concat_axis=...  23.4 us
    all_gather x4, waiting for transfers between devices, taken_in(): lax.all_gather(part, axis, axis=dim, tiled=True)  19.3 us
    all_to_all x2, starting transfers between devices, local(): lax.all_to_all(result.reshape(peer_count, CAP, half_width), 'ep', split_a...  13 us
    all_to_all x1, starting transfers between devices, local(): lax.all_to_all(outgoing[:, local_index], 'ep', split_axis=0, concat_axis=...  6.3 us
    dot_general x2, matrix products, add_hidden(): jnp.dot(block_part, down_rows, preferred_element_type=jnp.float32)  6.13 us
    dot_general x2, matrix products, add_feature(): jnp.dot(block_part, gate_rows, preferred_element_type=jnp.float32)  4.9 us
  transfers between devices with their start and end apart: 7, of which 6 were waited for; matrix products, arithmetic and copies ran while one was open for 7% of the time, Pallas kernels for 0%

commit v1 on v0

v1 whole, which is shorter than its diff:
```python
import functools

import jax
import jax.numpy as jnp
from jax import lax
from jax.experimental import pallas as pl
from jax.experimental.pallas import tpu as pltpu
from jax.sharding import Mesh, PartitionSpec as P

CAP = 8
EPS = 1e-06
INFO = 8
F32 = jnp.float32
BF16 = jnp.bfloat16


def iota(shape, dim):
    return lax.broadcasted_iota(jnp.int32, shape, dim)


def norm_kernel(own_ref, other_ref, gain_ref, route_ref, weight_ref, out_ref):
    rows, width = own_ref.shape
    own = own_ref[...].astype(F32)
    other = other_ref[...].astype(F32)
    total = jnp.sum(own * own, axis=1, keepdims=True) + jnp.sum(other * other, axis=1, keepdims=True)
    scale = lax.rsqrt(total / (2 * width) + EPS)
    out_ref[0:rows, :] = (own * scale * gain_ref[...]).astype(BF16)
    weight = weight_ref[...]
    high = weight.astype(BF16).astype(F32)
    middle = (weight - high).astype(BF16).astype(F32)
    low = weight - high - middle
    info = jnp.concatenate([route_ref[...].astype(F32), high, middle, low], axis=0)
    out_ref[rows:, :] = jnp.zeros((INFO, width), BF16)
    out_ref[rows:, 0:rows] = info.astype(BF16)


def dispatch_kernel(plane_ref, *refs):
    blocks, (out0_ref, out1_ref, slot_ref, weight_ref) = refs[:-4], refs[-4:]
    rows = blocks[0].shape[0] - INFO
    span = 2 * rows
    chips = out0_ref.shape[0]
    experts = 2 * chips
    first_expert = plane_ref[0] * experts
    earlier = (iota((span, span), 0) < iota((span, span), 1)) & (
        iota((span, span), 0) // rows == iota((span, span), 1) // rows
    )
    earlier = earlier.astype(F32).astype(BF16)
    lane = iota((1, span), 1)
    slots, weights = [], []
    for pair in range(len(blocks) // 2):
        a, b = blocks[2 * pair], blocks[2 * pair + 1]
        info = jnp.concatenate([a[rows:, 0:rows].astype(F32), b[rows:, 0:rows].astype(F32)], axis=1)
        tokens = jnp.concatenate([a[0:rows, :], b[0:rows, :]], axis=0)
        picks = [info[k : k + 1].astype(jnp.int32) - first_expert for k in range(2)]
        row = iota((experts, span), 0)
        named = (row == picks[0]) | (row == picks[1])
        ahead = jnp.dot(
            named.astype(F32).astype(BF16), earlier, preferred_element_type=F32
        )
        targets = []
        for k in range(2):
            rank = jnp.sum(jnp.where(row == picks[k], ahead, 0.0), axis=0, keepdims=True).astype(jnp.int32)
            inside = (picks[k] >= 0) & (picks[k] < experts)
            place = (picks[k] % 2) * (16 * chips) + (picks[k] // 2) * 16 + (lane // rows) * CAP + rank
            targets.append(jnp.where(inside, place, -1))
            slots.append(targets[k].astype(F32))
            weights.append(info[2 + k : 3 + k] + info[4 + k : 5 + k] + info[6 + k : 7 + k])
        for local, out_ref in enumerate((out0_ref, out1_ref)):
            slot = iota((16 * chips, span), 0) + local * 16 * chips
            chosen = ((slot == targets[0]) | (slot == targets[1])).astype(F32).astype(BF16)
            sent = jnp.dot(chosen, tokens, preferred_element_type=F32).astype(BF16)
            out_ref[:, 16 * pair : 16 * (pair + 1), :] = sent.reshape(chips, 16, -1)
    slot_ref[...] = jnp.concatenate(slots, axis=0)
    weight_ref[...] = jnp.concatenate(weights, axis=0)


def hidden_kernel(core_ref, own_ref, other_ref, gate_ref, up_ref, out_ref):
    core = core_ref[0]
    half = own_ref.shape[1]
    here = pl.ds(pl.multiple_of(core * half, half), half)
    there = pl.ds(pl.multiple_of((1 - core) * half, half), half)
    dot = functools.partial(jnp.dot, preferred_element_type=F32)
    gate = dot(own_ref[...], gate_ref[0, here, :]) + dot(other_ref[...], gate_ref[0, there, :])
    up = dot(own_ref[...], up_ref[0, here, :]) + dot(other_ref[...], up_ref[0, there, :])
    out_ref[...] = (gate / (1.0 + jnp.exp(-gate)) * up).astype(BF16)


def down_kernel(core_ref, own_ref, other_ref, down_ref, out_ref):
    core = core_ref[0]
    half = own_ref.shape[1]
    here = pl.ds(pl.multiple_of(core * half, half), half)
    there = pl.ds(pl.multiple_of((1 - core) * half, half), half)
    dot = functools.partial(jnp.dot, preferred_element_type=F32)
    out_ref[...] = (dot(own_ref[...], down_ref[0, here, :]) + dot(other_ref[...], down_ref[0, there, :])).astype(BF16)


def combine_kernel(plane_ref, back0_ref, back1_ref, slot_ref, weight_ref, out_ref):
    planes, rows, width = out_ref.shape
    chips = back0_ref.shape[0]
    span = 2 * rows
    plane = plane_ref[0]
    for pair in range(planes // 2):
        part = slice(16 * pair, 16 * (pair + 1))
        back = jnp.concatenate(
            [r[:, part, :].reshape(16 * chips, width) for r in (back0_ref, back1_ref)], axis=0
        )
        total = None
        for k in range(2):
            column = 2 * pair + k
            slot = slot_ref[:, column : column + 1].astype(jnp.int32)
            chosen = (iota((span, 32 * chips), 1) == slot).astype(F32).astype(BF16)
            picked = jnp.dot(chosen, back, preferred_element_type=F32)
            term = picked * weight_ref[:, column : column + 1]
            total = term if total is None else total + term
        total = total.astype(BF16)
        for side in range(2):
            out_ref[lax.rem(plane - (2 * pair + side) + planes, planes)] = total[side * rows : (side + 1) * rows]


def call(kernel, out_shape, args, flops, specs=None, **kw):
    moved = sum(a.size * a.dtype.itemsize for a in args)
    return pl.pallas_call(
        kernel,
        out_shape=out_shape,
        cost_estimate=pl.CostEstimate(flops=flops, bytes_accessed=moved, transcendentals=0),
        **kw,
    )(*args)


def local(tokens, norm_gain, routing, route_weight, w_gate, w_up, w_down):
    rows, half = tokens.shape
    planes = lax.axis_size("z")
    chips = lax.axis_size("y") * lax.axis_size("x")
    plane = lax.axis_index("z").astype(jnp.int32).reshape(1)
    core = lax.axis_index("tp").astype(jnp.int32).reshape(1)
    smem = pl.BlockSpec(memory_space=pltpu.SMEM)
    whole = pl.BlockSpec(memory_space=pltpu.VMEM)

    def swap(v):
        return lax.ppermute(v, "tp", [(0, 1), (1, 0)])

    other = swap(tokens)
    block = call(
        norm_kernel,
        jax.ShapeDtypeStruct((rows + INFO, half), BF16),
        (tokens, other, norm_gain.reshape(1, half), routing.T, route_weight.T),
        4 * rows * half,
    )

    right = [(i, (i + 1) % planes) for i in range(planes)]
    left = [(i, (i - 1) % planes) for i in range(planes)]
    blocks = [None] * planes
    blocks[0] = block
    up_going = down_going = block
    for step in range(1, planes // 2 + 1):
        up_going = lax.ppermute(up_going, "z", right)
        blocks[step] = up_going
        if planes - step > step:
            down_going = lax.ppermute(down_going, "z", left)
            blocks[planes - step] = down_going

    slots = planes * CAP
    shape = jax.ShapeDtypeStruct((chips, slots, half), BF16)
    small = jax.ShapeDtypeStruct((planes, 2 * rows), F32)
    sent0, sent1, place, weight = call(
        dispatch_kernel,
        (shape, shape, small, small),
        (plane, *blocks),
        4 * planes * chips * CAP * 2 * rows * half,
        in_specs=[smem] + [whole] * planes,
    )
    place, weight = place.T, weight.T
    back = []
    for index, sent in enumerate((sent0, sent1)):
        arrived = lax.all_to_all(sent, ("y", "x"), split_axis=0, concat_axis=0, tiled=True)
        arrived = arrived.reshape(chips * slots, half)
        total = arrived.shape[0]
        hidden_half = w_gate.shape[2]
        pick = lambda i: (index, 0, 0)
        hidden = call(
            hidden_kernel,
            jax.ShapeDtypeStruct((total, hidden_half), BF16),
            (core, arrived, swap(arrived), w_gate, w_up),
            8 * total * half * hidden_half,
            grid=(4,),
            in_specs=[
                smem,
                pl.BlockSpec((total // 4, half), lambda i: (i, 0)),
                pl.BlockSpec((total // 4, half), lambda i: (i, 0)),
                pl.BlockSpec((1, 2 * half, hidden_half), lambda i, index=index: (index, 0, 0)),
                pl.BlockSpec((1, 2 * half, hidden_half), lambda i, index=index: (index, 0, 0)),
            ],
            out_specs=pl.BlockSpec((total // 4, hidden_half), lambda i: (i, 0)),
        )
        result = call(
            down_kernel,
            jax.ShapeDtypeStruct((total, half), BF16),
            (core, hidden, swap(hidden), w_down),
            4 * total * half * hidden_half,
            grid=(4,),
            in_specs=[
                smem,
                pl.BlockSpec((total // 4, hidden_half), lambda i: (i, 0)),
                pl.BlockSpec((total // 4, hidden_half), lambda i: (i, 0)),
                pl.BlockSpec((1, 2 * hidden_half, half), lambda i, index=index: (index, 0, 0)),
            ],
            out_specs=pl.BlockSpec((total // 4, half), lambda i: (i, 0)),
        )
        back.append(
            lax.all_to_all(
                result.reshape(chips, slots, half), ("y", "x"), split_axis=0, concat_axis=0, tiled=True
            )
        )
    mixed = call(
        combine_kernel,
        jax.ShapeDtypeStruct((planes, rows, half), BF16),
        (plane, *back, place, weight),
        8 * planes * rows * 2 * chips * 16 * half,
        in_specs=[smem] + [whole] * 4,
    )
    home = lax.all_to_all(mixed, "z", split_axis=0, concat_axis=0, tiled=True)
    return jnp.sum(home.astype(F32), axis=0).astype(BF16)


def solution(mesh):
    mesh = Mesh(mesh.devices.reshape(8, 4, 4, 2), ("z", "y", "x", "tp"))
    ep = ("z", "y", "x")
    in_specs = (
        P(ep, "tp"),
        P("tp"),
        P(ep, None),
        P(ep, None),
        P(ep, None, "tp"),
        P(ep, None, "tp"),
        P(ep, None, "tp"),
    )
    return jax.shard_map(local, mesh=mesh, in_specs=in_specs, out_specs=P(ep, "tp"), check_vma=False)
```

time: 191 us -> 157 us (0.82)
  waiting for transfers between devices: 81.5 us -> 39.8 us
  Pallas kernels: 0 us -> 26.3 us
  blocking collectives: 49 us -> 64.8 us
  matrix products: 14.1 us -> 0 us
  between operations: 14 us -> 0.11 us
  other arithmetic: 4.27 us -> 0.71 us
  starting transfers between devices: 19.6 us -> 17.3 us
    all_to_all x3 -> x2, waiting for transfers between devices: 62.1 us -> 21.6 us  [local(): lax.all_to_all(result.reshape(chips, slots, half), ('y', 'x'), split_axis...]
    pallas_call x0 -> x7, Pallas kernels: none -> 26.3 us  [call(): pl.pallas_call(kernel, out_shape=out_shape, cost_estimate=pl.CostEstimate...]
    all_gather x4 -> x0, waiting for transfers between devices: 19.3 us -> none  [taken_in(): lax.all_gather(part, axis, axis=dim, tiled=True)]
    ppermute x0 -> x12, waiting for transfers between devices: none -> 18.2 us  [the longest x4 11.8 us: local(): up_going = lax.ppermute(up_going, 'z', right)]
    all_to_all x1 -> x3, blocking collectives: 46.6 us -> 64.8 us  [the longest x2 42.9 us: local(): lax.all_to_all(sent, ('y', 'x'), split_axis=0, concat_axis=0, tiled=True)]
    dot_general x6 -> x0, matrix products: 14.1 us -> none  [the longest x2 6.13 us: add_hidden(): jnp.dot(block_part, down_rows, preferred_element_type=jnp.float32)]
    all_to_all x3 -> x2, starting transfers between devices: 19.3 us -> 7.31 us  [local(): lax.all_to_all(result.reshape(chips, slots, half), ('y', 'x'), split_axis...]
    ppermute x0 -> x12, starting transfers between devices: none -> 10 us  [the longest x3 5.07 us: local(): down_going = lax.ppermute(down_going, 'z', left)]
  transfers between devices with their start and end apart: 7 -> 14, of which waited for: 6 -> 11; matrix products, arithmetic and copies ran while one was open for 7% -> 1% of each run, Pallas kernels for 0% -> 11%
where the time goes in v1:
time: 157 us; the launch traced here: 156 us
  blocking collectives  64.8 us (41%)
  waiting for transfers between devices  39.8 us (25%)
  Pallas kernels  26.3 us (17%)
  starting transfers between devices  17.3 us (11%)
  local copies, waits for them, and re-layouts  7.26 us (5%)
    all_to_all x2, blocking collectives, local(): lax.all_to_all(sent, ('y', 'x'), split_axis=0, concat_axis=0, tiled=True)  42.9 us
    pallas_call x7, Pallas kernels, call(): pl.pallas_call(kernel, out_shape=out_shape, cost_estimate=pl.CostEstimate...  26.3 us
    all_to_all x1, blocking collectives, local(): home = lax.all_to_all(mixed, 'z', split_axis=0, concat_axis=0, tiled=True)  21.9 us
    all_to_all x2, waiting for transfers between devices, local(): lax.all_to_all(result.reshape(chips, slots, half), ('y', 'x'), split_axis...  21.6 us
    ppermute x4, waiting for transfers between devices, local(): up_going = lax.ppermute(up_going, 'z', right)  11.8 us
    all_to_all x2, starting transfers between devices, local(): lax.all_to_all(result.reshape(chips, slots, half), ('y', 'x'), split_axis...  7.31 us
    unnamed x36, local copies, waits for them, and re-layouts  5.8 us
    ppermute x3, starting transfers between devices, local(): down_going = lax.ppermute(down_going, 'z', left)  5.07 us
  transfers between devices with their start and end apart: 14, of which 11 were waited for; matrix products, arithmetic and copies ran while one was open for 1% of the time, Pallas kernels for 11%

profile of v1, /device:TPU:32, one launch (start us, length us, event | category | flops | bytes accessed | tf_op | source)
XLA Modules:
  0.0 156.3 jit_solution(14961884852363360881)
XLA Ops:
  0.0 0.0 collective-permute-start
  0.0 1.5 collective-permute-done.other_ref
  1.5 0.0 copy-start.8
  1.5 0.6 copy-done.8
  2.1 1.6 %shard_map.73.refs_0_ = bf16[72,512]{1,0:T(8,128)(2,1)} custom-call(bf16[64,512]{1,0:T(8,128)(2,1)} %own_ref.1, bf16[64,512]{1,0:T(8,128)(2,1)} %copy-done.8, f32[1,512]{1,0:T(1,128)} %bitcast.19, s32[2,64]{1,0:T(2,128)} %bitcast.20, f32[2,64]{1,0:T(2,128)} %bitcast.21), custom_call_target="tpu_custom_call" | custom-call | flops 131072 | bytes 134144 | tf_op jit(solution)/shard_map/pallas_call | solution.py:122
  3.7 1.9 %collective-permute-start.1 = (bf16[72,512]{1,0:T(8,128)(2,1)}, bf16[72,512]{1,0:T(8,128)(2,1)S(1)}, u32[]{:S(2)}, u32[]{:S(2)}) collective-permute-start(bf16[72,512]{1,0:T(8,128)(2,1)} %shard_map.73.refs_0_), channel_id=1, source_target_pairs={{0,32},{32,64},{64,96},{96,128},{128,160},{160,192},{192,224},{224... | collective-permute-start | bytes 221192 | tf_op jit(solution)/shard_map/ppermute | solution.py:156
  5.7 0.1 collective-permute-start.5
  5.8 2.6 %collective-permute-done.1.refs_1_ = bf16[72,512]{1,0:T(8,128)(2,1)S(1)} collective-permute-done((bf16[72,512]{1,0:T(8,128)(2,1)}, bf16[72,512]{1,0:T(8,128)(2,1)S(1)}, u32[]{:S(2)}, u32[]{:S(2)}) %collective-permute-start.1) | collective-permute-done | bytes 73760 | tf_op jit(solution)/shard_map/ppermute | solution.py:156
  8.3 0.0 copy-start.11
  8.3 1.9 %collective-permute-start.2 = (bf16[72,512]{1,0:T(8,128)(2,1)S(1)}, bf16[72,512]{1,0:T(8,128)(2,1)S(1)}, u32[]{:S(2)}, u32[]{:S(2)}) collective-permute-start(bf16[72,512]{1,0:T(8,128)(2,1)S(1)} %collective-permute-done.1.refs_1_), channel_id=1, source_target_pairs={{0,32},{32,64},{64,96},{96,128},{128,160},{160,192},{192,224},{224... | collective-permute-start | bytes 221192 | tf_op jit(solution)/shard_map/ppermute | solution.py:156
  10.2 0.0 collective-permute-done.5.refs_7_
  10.2 0.0 copy-start.12
  10.2 2.4 %collective-permute-start.6 = (bf16[72,512]{1,0:T(8,128)(2,1)S(1)}, bf16[72,512]{1,0:T(8,128)(2,1)S(1)}, u32[]{:S(2)}, u32[]{:S(2)}) collective-permute-start(bf16[72,512]{1,0:T(8,128)(2,1)S(1)} %collective-permute-done.5.refs_7_), channel_id=1, source_target_pairs={{0,224},{32,0},{64,32},{96,64},{128,96},{160,128},{192,160},{224,1... | collective-permute-start | bytes 221192 | tf_op jit(solution)/shard_map/ppermute | solution.py:159
  12.6 2.2 %collective-permute-done.2.refs_2_ = bf16[72,512]{1,0:T(8,128)(2,1)S(1)} collective-permute-done((bf16[72,512]{1,0:T(8,128)(2,1)S(1)}, bf16[72,512]{1,0:T(8,128)(2,1)S(1)}, u32[]{:S(2)}, u32[]{:S(2)}) %collective-permute-start.2) | collective-permute-done | bytes 73760 | tf_op jit(solution)/shard_map/ppermute | solution.py:156
  14.8 0.0 copy-start.13
  14.8 0.0 collective-permute-start.3
  14.9 0.7 collective-permute-done.6.refs_6_
  15.6 2.6 %collective-permute-start.7 = (bf16[72,512]{1,0:T(8,128)(2,1)S(1)}, bf16[72,512]{1,0:T(8,128)(2,1)S(1)}, u32[]{:S(2)}, u32[]{:S(2)}) collective-permute-start(bf16[72,512]{1,0:T(8,128)(2,1)S(1)} %collective-permute-done.6.refs_6_), channel_id=1, source_target_pairs={{0,224},{32,0},{64,32},{96,64},{128,96},{160,128},{192,160},{224,1... | collective-permute-start | bytes 221192 | tf_op jit(solution)/shard_map/ppermute | solution.py:159
  18.2 2.2 %collective-permute-done.3.refs_3_ = bf16[72,512]{1,0:T(8,128)(2,1)S(1)} collective-permute-done((bf16[72,512]{1,0:T(8,128)(2,1)S(1)}, bf16[72,512]{1,0:T(8,128)(2,1)S(1)}, u32[]{:S(2)}, u32[]{:S(2)}) %collective-permute-start.3) | collective-permute-done | bytes 73760 | tf_op jit(solution)/shard_map/ppermute | solution.py:156
  20.4 0.0 collective-permute-start.4
  20.4 0.7 collective-permute-done.7.refs_5_
  21.1 4.8 %collective-permute-done.4.refs_4_ = bf16[72,512]{1,0:T(8,128)(2,1)S(1)} collective-permute-done((bf16[72,512]{1,0:T(8,128)(2,1)S(1)}, bf16[72,512]{1,0:T(8,128)(2,1)S(1)}, u32[]{:S(2)}, u32[]{:S(2)}) %collective-permute-start.4) | collective-permute-done | bytes 73760 | tf_op jit(solution)/shard_map/ppermute | solution.py:156
  26.0 0.0 copy-done.11
  26.0 0.0 copy-done.12
  26.0 0.0 copy-done.13
  26.0 0.0 copy-done.14
  26.0 0.0 copy-done.15
  26.0 0.0 copy-done.16
  26.0 0.6 copy-done.17
  26.6 3.8 %shard_map.74 = (bf16[16,64,512]{2,1,0:T(8,128)(2,1)}, bf16[16,64,512]{2,1,0:T(8,128)(2,1)}, f32[8,128]{1,0:T(8,128)}, f32[8,128]{1,0:T(8,128)}) custom-call(s32[1]{0:T(128)} %bitcast.plane_ref, bf16[72,512]{1,0:T(8,128)(2,1)} %shard_map.73.refs_0_, bf16[72,512]{1,0:T(8,128)(2,1)} %copy-done.11, bf16[72,512]{1,0:T(8,128)(2,1)} %copy-done.13, ...), custom_call_target="tpu_custom_call" | custom-call | flops 268435456 | bytes 589828 | tf_op jit(solution)/shard_map/pallas_call | solution.py:122
  30.4 20.9 %all_to_all.25 = bf16[16,64,512]{2,1,0:T(8,128)(2,1)S(1)} all-to-all(bf16[16,64,512]{2,1,0:T(8,128)(2,1)} %get-tuple-element.10), channel_id=1, replica_groups=mesh['z'=8,'y'=4,'x'=4,'tp'=2] {'y','x'}, dimensions={0} | all-to-all | bytes 2097152 | tf_op jit(solution)/shard_map/all_to_all | solution.py:175
  51.2 0.0 collective-permute-start.10
  51.2 0.0 copy-done.4
  51.2 22.1 %all_to_all.26 = bf16[16,64,512]{2,1,0:T(8,128)(2,1)S(1)} all-to-all(bf16[16,64,512]{2,1,0:T(8,128)(2,1)S(1)} %copy-done.4), channel_id=1, replica_groups=mesh['z'=8,'y'=4,'x'=4,'tp'=2] {'y','x'}, dimensions={0} | all-to-all | bytes 2097152 | tf_op jit(solution)/shard_map/all_to_all | solution.py:175
  73.3 0.0 copy-done.1
  73.3 0.3 collective-permute-start.8
  73.7 0.0 collective-permute-done.10.other_ref
  73.7 4.7 %shard_map.77.own_ref = bf16[1024,256]{1,0:T(8,128)(2,1)} custom-call(s32[1]{0:T(128)} %bitcast.1.core_ref, bf16[1024,512]{1,0:T(8,128)(2,1)} %bitcast.14, bf16[1024,512]{1,0:T(8,128)(2,1)} %collective-permute-done.10.other_ref, bf16[2,1024,256]{2,1,0:T(8,128)(2,1)} %gate_ref.3, bf16[2,1024,256]{2,1,0:T(8,128)(2,1)} %up_ref.3), custom_call_target="tpu_custom_call" | custom-call | flops 1073741824 | bytes 4194308 | tf_op jit(solution)/shard_map/pallas_call | solution.py:122
  78.4 0.0 copy-done
  78.4 0.3 collective-permute-start.11
  78.7 1.8 %collective-permute-done.11.other_ref = bf16[1024,256]{1,0:T(8,128)(2,1)S(1)} collective-permute-done((bf16[1024,256]{1,0:T(8,128)(2,1)}, bf16[1024,256]{1,0:T(8,128)(2,1)S(1)}, u32[]{:S(2)}, u32[]{:S(2)}) %collective-permute-start.11) | collective-permute-done | bytes 524320 | tf_op jit(solution)/shard_map/ppermute | solution.py:140
  80.5 0.8 copy-done.7
  81.3 4.2 %shard_map.78 = bf16[1024,512]{1,0:T(8,128)(2,1)} custom-call(s32[1]{0:T(128)} %bitcast.1.core_ref, bf16[1024,256]{1,0:T(8,128)(2,1)} %shard_map.77.own_ref, bf16[1024,256]{1,0:T(8,128)(2,1)} %copy-done.7, bf16[2,512,512]{2,1,0:T(8,128)(2,1)} %down_ref.3), custom_call_target="tpu_custom_call" | custom-call | flops 536870912 | bytes 2097156 | tf_op jit(solution)/shard_map/pallas_call | solution.py:122
  85.5 3.7 %all-to-all-start.3 = ((bf16[16,64,512]{2,1,0:T(8,128)(2,1)}), bf16[16,64,512]{2,1,0:T(8,128)(2,1)S(1)}, u32[]{:S(2)}, u32[]{:S(2)}) async-start(bf16[16,64,512]{2,1,0:T(8,128)(2,1)} %bitcast.15), calls=%async_computation.3 | async-start | bytes 2097152 | tf_op jit(solution)/shard_map/all_to_all | solution.py:210
  89.2 0.0 collective-permute-done.8.other_ref
  89.2 0.0 copy-start.2
  89.2 1.0 copy-done.2
  90.2 4.7 %shard_map.75.own_ref = bf16[1024,256]{1,0:T(8,128)(2,1)} custom-call(s32[1]{0:T(128)} %bitcast.1.core_ref, bf16[1024,512]{1,0:T(8,128)(2,1)} %bitcast.12, bf16[1024,512]{1,0:T(8,128)(2,1)} %copy-done.2, bf16[2,1024,256]{2,1,0:T(8,128)(2,1)} %gate_ref.3, bf16[2,1024,256]{2,1,0:T(8,128)(2,1)} %up_ref.3), custom_call_target="tpu_custom_call" | custom-call | flops 1073741824 | bytes 4194308 | tf_op jit(solution)/shard_map/pallas_call | solution.py:122
  94.8 0.3 collective-permute-start.9
  95.2 1.8 %collective-permute-done.9.other_ref = bf16[1024,256]{1,0:T(8,128)(2,1)S(1)} collective-permute-done((bf16[1024,256]{1,0:T(8,128)(2,1)}, bf16[1024,256]{1,0:T(8,128)(2,1)S(1)}, u32[]{:S(2)}, u32[]{:S(2)}) %collective-permute-start.9) | collective-permute-done | bytes 524320 | tf_op jit(solution)/shard_map/ppermute | solution.py:140
  96.9 0.8 copy-done.6
  97.7 4.2 %shard_map.76 = bf16[1024,512]{1,0:T(8,128)(2,1)} custom-call(s32[1]{0:T(128)} %bitcast.1.core_ref, bf16[1024,256]{1,0:T(8,128)(2,1)} %shard_map.75.own_ref, bf16[1024,256]{1,0:T(8,128)(2,1)} %copy-done.6, bf16[2,512,512]{2,1,0:T(8,128)(2,1)} %down_ref.3), custom_call_target="tpu_custom_call" | custom-call | flops 536870912 | bytes 2097156 | tf_op jit(solution)/shard_map/pallas_call | solution.py:122
  101.9 6.3 %all-to-all-done.3.back1_ref = bf16[16,64,512]{2,1,0:T(8,128)(2,1)S(1)} async-done(((bf16[16,64,512]{2,1,0:T(8,128)(2,1)}), bf16[16,64,512]{2,1,0:T(8,128)(2,1)S(1)}, u32[]{:S(2)}, u32[]{:S(2)}) %all-to-all-start.3) | async-done | bytes 1048608 | tf_op jit(solution)/shard_map/all_to_all | solution.py:210
  108.3 1.0 copy-done.3
  109.3 3.7 %all-to-all-start.1 = ((bf16[16,64,512]{2,1,0:T(8,128)(2,1)}), bf16[16,64,512]{2,1,0:T(8,128)(2,1)S(1)}, u32[]{:S(2)}, u32[]{:S(2)}) async-start(bf16[16,64,512]{2,1,0:T(8,128)(2,1)} %bitcast.16), calls=%async_computation.1 | async-start | bytes 2097152 | tf_op jit(solution)/shard_map/all_to_all | solution.py:210
  112.9 0.0 copy-done.10
  112.9 0.7 copy.9
  113.7 0.0 copy-done.9
  113.7 0.7 copy.8
  114.4 15.2 %all-to-all-done.1.back0_ref = bf16[16,64,512]{2,1,0:T(8,128)(2,1)S(1)} async-done(((bf16[16,64,512]{2,1,0:T(8,128)(2,1)}), bf16[16,64,512]{2,1,0:T(8,128)(2,1)S(1)}, u32[]{:S(2)}, u32[]{:S(2)}) %all-to-all-start.1) | async-done | bytes 1048608 | tf_op jit(solution)/shard_map/all_to_all | solution.py:210
  129.6 1.0 copy-done.5
  130.6 3.1 %shard_map.79 = bf16[8,64,512]{2,1,0:T(8,128)(2,1)} custom-call(s32[1]{0:T(128)} %bitcast.plane_ref, bf16[16,64,512]{2,1,0:T(8,128)(2,1)} %copy-done.5, bf16[16,64,512]{2,1,0:T(8,128)(2,1)} %copy-done.3, f32[128,8]{1,0:T(8,128)} %bitcast.18, f32[128,8]{1,0:T(8,128)} %bitcast.17), custom_call_target="tpu_custom_call" | custom-call | flops 1073741824 | bytes 2105348 | tf_op jit(solution)/shard_map/pallas_call | solution.py:122
  133.7 21.9 %all_to_all.27 = bf16[8,64,512]{2,1,0:T(8,128)(2,1)S(1)} all-to-all(bf16[8,64,512]{2,1,0:T(8,128)(2,1)} %shard_map.79), channel_id=1, replica_groups=mesh['z'=8,'y'=4,'x'=4,'tp'=2] {'z'}, dimensions={0} | all-to-all | bytes 1048576 | tf_op jit(solution)/shard_map/all_to_all | solution.py:221
  155.6 0.7 reduce_sum.12
  (13 shorter events, 0.0 us)
Async XLA Ops:
  0.0 1.5 collective-permute-start
  1.5 0.6 copy-start.8
  3.7 4.6 %collective-permute-start.1 = (bf16[72,512]{1,0:T(8,128)(2,1)}, bf16[72,512]{1,0:T(8,128)(2,1)S(1)}, u32[]{:S(2)}, u32[]{:S(2)}) collective-permute-start(bf16[72,512]{1,0:T(8,128)(2,1)} %shard_map.73.refs_0_), channel_id=1, source_target_pairs={{0,32},{32,64},{64,96},{96,128},{128,160},{160,192},{192,224},{224... | collective-permute-start | bytes 221192 | tf_op jit(solution)/shard_map/ppermute | solution.py:156
  5.7 4.6 %collective-permute-start.5 = (bf16[72,512]{1,0:T(8,128)(2,1)}, bf16[72,512]{1,0:T(8,128)(2,1)S(1)}, u32[]{:S(2)}, u32[]{:S(2)}) collective-permute-start(bf16[72,512]{1,0:T(8,128)(2,1)} %shard_map.73.refs_0_), channel_id=1, source_target_pairs={{0,224},{32,0},{64,32},{96,64},{128,96},{160,128},{192,160},{224,1... | collective-permute-start | bytes 221192 | tf_op jit(solution)/shard_map/ppermute | solution.py:159
  8.3 17.7 %copy-start.11 = (bf16[72,512]{1,0:T(8,128)(2,1)}, bf16[72,512]{1,0:T(8,128)(2,1)S(1)}, u32[]{:S(2)}) copy-start(bf16[72,512]{1,0:T(8,128)(2,1)S(1)} %collective-permute-done.1.refs_1_) | copy-start | bytes 221188
  8.3 6.5 %collective-permute-start.2 = (bf16[72,512]{1,0:T(8,128)(2,1)S(1)}, bf16[72,512]{1,0:T(8,128)(2,1)S(1)}, u32[]{:S(2)}, u32[]{:S(2)}) collective-permute-start(bf16[72,512]{1,0:T(8,128)(2,1)S(1)} %collective-permute-done.1.refs_1_), channel_id=1, source_target_pairs={{0,32},{32,64},{64,96},{96,128},{128,160},{160,192},{192,224},{224... | collective-permute-start | bytes 221192 | tf_op jit(solution)/shard_map/ppermute | solution.py:156
  10.2 15.7 %copy-start.12 = (bf16[72,512]{1,0:T(8,128)(2,1)}, bf16[72,512]{1,0:T(8,128)(2,1)S(1)}, u32[]{:S(2)}) copy-start(bf16[72,512]{1,0:T(8,128)(2,1)S(1)} %collective-permute-done.5.refs_7_) | copy-start | bytes 221188
  10.2 5.3 %collective-permute-start.6 = (bf16[72,512]{1,0:T(8,128)(2,1)S(1)}, bf16[72,512]{1,0:T(8,128)(2,1)S(1)}, u32[]{:S(2)}, u32[]{:S(2)}) collective-permute-start(bf16[72,512]{1,0:T(8,128)(2,1)S(1)} %collective-permute-done.5.refs_7_), channel_id=1, source_target_pairs={{0,224},{32,0},{64,32},{96,64},{128,96},{160,128},{192,160},{224,1... | collective-permute-start | bytes 221192 | tf_op jit(solution)/shard_map/ppermute | solution.py:159
  14.8 11.1 %copy-start.13 = (bf16[72,512]{1,0:T(8,128)(2,1)}, bf16[72,512]{1,0:T(8,128)(2,1)S(1)}, u32[]{:S(2)}) copy-start(bf16[72,512]{1,0:T(8,128)(2,1)S(1)} %collective-permute-done.2.refs_2_) | copy-start | bytes 221188
  14.8 5.6 %collective-permute-start.3 = (bf16[72,512]{1,0:T(8,128)(2,1)S(1)}, bf16[72,512]{1,0:T(8,128)(2,1)S(1)}, u32[]{:S(2)}, u32[]{:S(2)}) collective-permute-start(bf16[72,512]{1,0:T(8,128)(2,1)S(1)} %collective-permute-done.2.refs_2_), channel_id=1, source_target_pairs={{0,32},{32,64},{64,96},{96,128},{128,160},{160,192},{192,224},{224... | collective-permute-start | bytes 221192 | tf_op jit(solution)/shard_map/ppermute | solution.py:156
  15.6 10.4 %copy-start.14 = (bf16[72,512]{1,0:T(8,128)(2,1)}, bf16[72,512]{1,0:T(8,128)(2,1)S(1)}, u32[]{:S(2)}) copy-start(bf16[72,512]{1,0:T(8,128)(2,1)S(1)} %collective-permute-done.6.refs_6_) | copy-start | bytes 221188
  15.6 5.6 %collective-permute-start.7 = (bf16[72,512]{1,0:T(8,128)(2,1)S(1)}, bf16[72,512]{1,0:T(8,128)(2,1)S(1)}, u32[]{:S(2)}, u32[]{:S(2)}) collective-permute-start(bf16[72,512]{1,0:T(8,128)(2,1)S(1)} %collective-permute-done.6.refs_6_), channel_id=1, source_target_pairs={{0,224},{32,0},{64,32},{96,64},{128,96},{160,128},{192,160},{224,1... | collective-permute-start | bytes 221192 | tf_op jit(solution)/shard_map/ppermute | solution.py:159
  20.4 5.6 %copy-start.15 = (bf16[72,512]{1,0:T(8,128)(2,1)}, bf16[72,512]{1,0:T(8,128)(2,1)S(1)}, u32[]{:S(2)}) copy-start(bf16[72,512]{1,0:T(8,128)(2,1)S(1)} %collective-permute-done.3.refs_3_) | copy-start | bytes 221188
  20.4 5.6 %collective-permute-start.4 = (bf16[72,512]{1,0:T(8,128)(2,1)S(1)}, bf16[72,512]{1,0:T(8,128)(2,1)S(1)}, u32[]{:S(2)}, u32[]{:S(2)}) collective-permute-start(bf16[72,512]{1,0:T(8,128)(2,1)S(1)} %collective-permute-done.3.refs_3_), channel_id=1, source_target_pairs={{0,32},{32,64},{64,96},{96,128},{128,160},{160,192},{192,224},{224... | collective-permute-start | bytes 221192 | tf_op jit(solution)/shard_map/ppermute | solution.py:156
  21.1 4.9 %copy-start.16 = (bf16[72,512]{1,0:T(8,128)(2,1)}, bf16[72,512]{1,0:T(8,128)(2,1)S(1)}, u32[]{:S(2)}) copy-start(bf16[72,512]{1,0:T(8,128)(2,1)S(1)} %collective-permute-done.7.refs_5_) | copy-start | bytes 221188
  26.0 0.6 copy-start.17
  30.4 20.9 %copy-start.4 = (bf16[16,64,512]{2,1,0:T(8,128)(2,1)S(1)}, bf16[16,64,512]{2,1,0:T(8,128)(2,1)}, u32[]{:S(2)}) copy-start(bf16[16,64,512]{2,1,0:T(8,128)(2,1)} %get-tuple-element.9) | copy-start | bytes 3145732
  51.2 22.1 %copy-start.1 = (bf16[16,64,512]{2,1,0:T(8,128)(2,1)}, bf16[16,64,512]{2,1,0:T(8,128)(2,1)S(1)}, u32[]{:S(2)}) copy-start(bf16[16,64,512]{2,1,0:T(8,128)(2,1)S(1)} %all_to_all.25) | copy-start | bytes 3145732
  51.2 22.4 %collective-permute-start.10 = (bf16[1024,512]{1,0:T(8,128)(2,1)S(1)}, bf16[1024,512]{1,0:T(8,128)(2,1)}, u32[]{:S(2)}, u32[]{:S(2)}) collective-permute-start(bf16[1024,512]{1,0:T(8,128)(2,1)S(1)} %bitcast.13), channel_id=1, source_target_pairs={{0,1},{1,0},{2,3},{3,2},{4,5},{5,4},{6,7},{7,6},{8,9},{9,8},{10,11... | collective-permute-start | bytes 3145736 | tf_op jit(solution)/shard_map/ppermute | solution.py:140
  73.3 5.0 %copy-start = (bf16[16,64,512]{2,1,0:T(8,128)(2,1)}, bf16[16,64,512]{2,1,0:T(8,128)(2,1)S(1)}, u32[]{:S(2)}) copy-start(bf16[16,64,512]{2,1,0:T(8,128)(2,1)S(1)} %all_to_all.26) | copy-start | bytes 3145732
  73.3 15.8 %collective-permute-start.8 = (bf16[1024,512]{1,0:T(8,128)(2,1)S(1)}, bf16[1024,512]{1,0:T(8,128)(2,1)S(1)}, u32[]{:S(2)}, u32[]{:S(2)}) collective-permute-start(bf16[1024,512]{1,0:T(8,128)(2,1)S(1)} %bitcast.11), channel_id=1, source_target_pairs={{0,1},{1,0},{2,3},{3,2},{4,5},{5,4},{6,7},{7,6},{8,9},{9,8},{10,11... | collective-permute-start | bytes 3145736 | tf_op jit(solution)/shard_map/ppermute | solution.py:140
  78.4 2.1 %collective-permute-start.11 = (bf16[1024,256]{1,0:T(8,128)(2,1)}, bf16[1024,256]{1,0:T(8,128)(2,1)S(1)}, u32[]{:S(2)}, u32[]{:S(2)}) collective-permute-start(bf16[1024,256]{1,0:T(8,128)(2,1)} %shard_map.77.own_ref), channel_id=1, source_target_pairs={{0,1},{1,0},{2,3},{3,2},{4,5},{5,4},{6,7},{7,6},{8,9},{9,8},{10,11... | collective-permute-start | bytes 1572872 | tf_op jit(solution)/shard_map/ppermute | solution.py:140
  80.5 0.8 copy-start.7
  85.5 22.8 %all-to-all-start.3 = ((bf16[16,64,512]{2,1,0:T(8,128)(2,1)}), bf16[16,64,512]{2,1,0:T(8,128)(2,1)S(1)}, u32[]{:S(2)}, u32[]{:S(2)}) async-start(bf16[16,64,512]{2,1,0:T(8,128)(2,1)} %bitcast.15), calls=%async_computation.3 | async-start | bytes 2097152 | tf_op jit(solution)/shard_map/all_to_all | solution.py:210
  89.2 1.0 copy-start.2
  94.8 2.1 %collective-permute-start.9 = (bf16[1024,256]{1,0:T(8,128)(2,1)}, bf16[1024,256]{1,0:T(8,128)(2,1)S(1)}, u32[]{:S(2)}, u32[]{:S(2)}) collective-permute-start(bf16[1024,256]{1,0:T(8,128)(2,1)} %shard_map.75.own_ref), channel_id=1, source_target_pairs={{0,1},{1,0},{2,3},{3,2},{4,5},{5,4},{6,7},{7,6},{8,9},{9,8},{10,11... | collective-permute-start | bytes 1572872 | tf_op jit(solution)/shard_map/ppermute | solution.py:140
  96.9 0.8 copy-start.6
  108.3 1.0 copy-start.3
  108.3 4.6 %copy-start.10 = (f32[8,128]{1,0:T(8,128)S(1)}, f32[8,128]{1,0:T(8,128)}, u32[]{:S(2)}) copy-start(f32[8,128]{1,0:T(8,128)} %get-tuple-element.12) | copy-start | bytes 12292
  108.3 5.4 %copy-start.9 = (f32[8,128]{1,0:T(8,128)S(1)}, f32[8,128]{1,0:T(8,128)}, u32[]{:S(2)}) copy-start(f32[8,128]{1,0:T(8,128)} %get-tuple-element.11) | copy-start | bytes 12292
  109.3 20.3 %all-to-all-start.1 = ((bf16[16,64,512]{2,1,0:T(8,128)(2,1)}), bf16[16,64,512]{2,1,0:T(8,128)(2,1)S(1)}, u32[]{:S(2)}, u32[]{:S(2)}) async-start(bf16[16,64,512]{2,1,0:T(8,128)(2,1)} %bitcast.16), calls=%async_computation.1 | async-start | bytes 2097152 | tf_op jit(solution)/shard_map/all_to_all | solution.py:210
  129.6 1.0 copy-start.5

commit v2 on v0

v2 whole, which is shorter than its diff:
```python
import functools

import jax
import jax.numpy as jnp
from jax import lax
from jax.experimental import pallas as pl
from jax.experimental.pallas import tpu as pltpu
from jax.sharding import PartitionSpec as P

CAP = 8
EPS = 1e-06
F32 = jnp.float32
BF16 = jnp.bfloat16
dot = functools.partial(jnp.dot, preferred_element_type=F32)


def iota(shape, dim):
    return lax.broadcasted_iota(jnp.int32, shape, dim)


def one_hot(mask):
    return mask.astype(F32).astype(BF16)


def dispatch_kernel(own_ref, other_ref, gain_ref, route_ref, out_ref, slot_ref):
    rows, half = own_ref.shape
    own = own_ref[...].astype(F32)
    other = other_ref[...].astype(F32)
    total = jnp.sum(own * own, axis=1, keepdims=True) + jnp.sum(other * other, axis=1, keepdims=True)
    scale = lax.rsqrt(total / (2 * half) + EPS)
    normed = (own * scale * gain_ref[...]).astype(BF16)

    peers, block, _ = out_ref.shape
    experts = peers * block // CAP
    expert = iota((experts, rows), 0)
    first, second = route_ref[0:1, :], route_ref[1:2, :]
    named = (expert == first) | (expert == second)
    earlier = one_hot(iota((rows, rows), 0) < iota((rows, rows), 1))
    ahead = dot(one_hot(named), earlier)
    slots = []
    for pick in (first, second):
        rank = jnp.sum(jnp.where(expert == pick, ahead, 0.0), axis=0, keepdims=True)
        slots.append(pick * CAP + rank.astype(jnp.int32))
    chunk = 256
    for at in range(0, peers * block, chunk):
        slot = iota((chunk, rows), 0) + at
        sent = dot(one_hot((slot == slots[0]) | (slot == slots[1])), normed).astype(BF16)
        out_ref[at // block : (at + chunk) // block] = sent.reshape(chunk // block, block, half)
    slot_ref[...] = jnp.concatenate(slots, axis=0)


def hidden_kernel(core_ref, own_ref, other_ref, gate_ref, up_ref, out_ref):
    core = core_ref[0]
    peers, block, half = own_ref.shape
    here = pl.ds(pl.multiple_of(core * half, half), half)
    there = pl.ds(pl.multiple_of((1 - core) * half, half), half)
    step = 256 // CAP
    for expert in range(block // CAP):
        for at in range(0, peers, step):
            part = (slice(at, at + step), slice(expert * CAP, (expert + 1) * CAP))
            own = own_ref[part].reshape(step * CAP, half)
            other = other_ref[part].reshape(step * CAP, half)
            gate = dot(own, gate_ref[expert, here, :]) + dot(other, gate_ref[expert, there, :])
            up = dot(own, up_ref[expert, here, :]) + dot(other, up_ref[expert, there, :])
            out_ref[expert, at * CAP : (at + step) * CAP] = (gate / (1.0 + jnp.exp(-gate)) * up).astype(BF16)


def down_kernel(core_ref, own_ref, other_ref, down_ref, out_ref):
    core = core_ref[0]
    experts, total, quarter = own_ref.shape
    here = pl.ds(pl.multiple_of(core * quarter, quarter), quarter)
    there = pl.ds(pl.multiple_of((1 - core) * quarter, quarter), quarter)
    step = 256
    for expert in range(experts):
        for at in range(0, total, step):
            part = slice(at, at + step)
            rows = dot(own_ref[expert, part], down_ref[expert, here, :]) + dot(
                other_ref[expert, part], down_ref[expert, there, :]
            )
            out_ref[at // CAP : (at + step) // CAP, expert * CAP : (expert + 1) * CAP] = (
                rows.astype(BF16).reshape(step // CAP, CAP, -1)
            )


def combine_kernel(back_ref, slot_ref, weight_ref, out_ref):
    peers, block, half = back_ref.shape
    rows = out_ref.shape[0]
    chunk = 256
    picked = [None, None]
    for at in range(0, peers * block, chunk):
        back = back_ref[at // block : (at + chunk) // block].reshape(chunk, half)
        place = iota((rows, chunk), 1) + at
        for k in range(2):
            term = dot(one_hot(place == slot_ref[:, k : k + 1]), back)
            picked[k] = term if picked[k] is None else picked[k] + term
    out_ref[...] = (picked[0] * weight_ref[:, 0:1] + picked[1] * weight_ref[:, 1:2]).astype(BF16)


def call(kernel, out_shape, args, flops, grant, scalars=0):
    moved = sum(a.size * a.dtype.itemsize for a in args)
    smem = pl.BlockSpec(memory_space=pltpu.SMEM)
    whole = pl.BlockSpec(memory_space=pltpu.VMEM)
    return pl.pallas_call(
        kernel,
        out_shape=out_shape,
        in_specs=[smem] * scalars + [whole] * (len(args) - scalars),
        cost_estimate=pl.CostEstimate(flops=flops, bytes_accessed=moved, transcendentals=0),
        compiler_params=pltpu.CompilerParams(vmem_limit_bytes=grant << 20),
    )(*args)


def local(tokens, norm_gain, routing, route_weight, w_gate, w_up, w_down):
    rows, half = tokens.shape
    peers = lax.axis_size("ep")
    experts, _, hidden_half = w_gate.shape
    block = experts * CAP
    core = lax.axis_index("tp").astype(jnp.int32).reshape(1)

    def swap(v):
        return lax.ppermute(v, "tp", [(0, 1), (1, 0)])

    def exchange(v):
        return lax.all_to_all(v, "ep", split_axis=0, concat_axis=0, tiled=True)

    buffer = jax.ShapeDtypeStruct((peers, block, half), BF16)
    sent, slots = call(
        dispatch_kernel,
        (buffer, jax.ShapeDtypeStruct((2, rows), jnp.int32)),
        (tokens, swap(tokens), norm_gain.reshape(1, half), routing.T),
        2 * peers * block * rows * half,
        12,
    )
    arrived = exchange(sent)
    hidden = call(
        hidden_kernel,
        jax.ShapeDtypeStruct((experts, peers * CAP, hidden_half), BF16),
        (core, arrived, swap(arrived), w_gate, w_up),
        8 * peers * block * half * hidden_half,
        20,
        1,
    )
    result = call(
        down_kernel, buffer, (core, hidden, swap(hidden), w_down), 4 * peers * block * hidden_half * half, 16, 1
    )
    back = exchange(result)
    return call(
        combine_kernel,
        jax.ShapeDtypeStruct((rows, half), BF16),
        (back, slots.T, route_weight),
        4 * peers * block * rows * half,
        12,
    )


def solution(mesh):
    in_specs = (
        P("ep", "tp"),
        P("tp"),
        P("ep", None),
        P("ep", None),
        P("ep", None, "tp"),
        P("ep", None, "tp"),
        P("ep", None, "tp"),
    )
    return jax.shard_map(local, mesh=mesh, in_specs=in_specs, out_specs=P("ep", "tp"), check_vma=False)
```

time: 191 us -> 151 us (0.79)
  blocking collectives: 49 us -> 69.3 us
  waiting for transfers between devices: 81.5 us -> 62.7 us
  matrix products: 14.1 us -> 0 us
  between operations: 14 us -> 0.06 us
  starting transfers between devices: 19.6 us -> 6.36 us
  Pallas kernels: 0 us -> 7.76 us
  other arithmetic: 4.27 us -> 0 us
  local copies, waits for them, and re-layouts: 8.27 us -> 4.95 us
    all_to_all x1, blocking collectives: 46.6 us -> 69.3 us  [exchange(): return lax.all_to_all(v, 'ep', split_axis=0, concat_axis=0, tiled=True)]
    all_gather x4 -> x0, waiting for transfers between devices: 19.3 us -> none  [taken_in(): lax.all_gather(part, axis, axis=dim, tiled=True)]
    dot_general x6 -> x0, matrix products: 14.1 us -> none  [the longest x2 6.13 us: add_hidden(): jnp.dot(block_part, down_rows, preferred_element_type=jnp.float32)]
    all_to_all x3 -> x1, starting transfers between devices: 19.3 us -> 6.13 us  [exchange(): return lax.all_to_all(v, 'ep', split_axis=0, concat_axis=0, tiled=True)]
    ppermute x0 -> x3, waiting for transfers between devices: none -> 8.27 us  [swap(): return lax.ppermute(v, 'tp', [(0, 1), (1, 0)])]
    pallas_call x0 -> x4, Pallas kernels: none -> 7.76 us  [call(): pl.pallas_call(kernel, out_shape=out_shape, in_specs=[smem] * scalars + [...]
    all_to_all x3 -> x1, waiting for transfers between devices: 62.1 us -> 54.4 us  [exchange(): return lax.all_to_all(v, 'ep', split_axis=0, concat_axis=0, tiled=True)]
    unnamed x1 -> x0, blocking collectives: 2.44 us -> none
  transfers between devices with their start and end apart: 7 -> 4, of which waited for: 6 -> 4; matrix products, arithmetic and copies ran while one was open for 7% -> 0% of each run, Pallas kernels for 0% -> 0%
where the time goes in v2:
time: 151 us
  blocking collectives  69.3 us (46%)
  waiting for transfers between devices  62.7 us (42%)
  Pallas kernels  7.76 us (5%)
  starting transfers between devices  6.36 us (4%)
  local copies, waits for them, and re-layouts  4.95 us (3%)
    all_to_all x1, blocking collectives, exchange(): return lax.all_to_all(v, 'ep', split_axis=0, concat_axis=0, tiled=True)  69.3 us
    all_to_all x1, waiting for transfers between devices, exchange(): return lax.all_to_all(v, 'ep', split_axis=0, concat_axis=0, tiled=True)  54.4 us
    ppermute x3, waiting for transfers between devices, swap(): return lax.ppermute(v, 'tp', [(0, 1), (1, 0)])  8.27 us
    pallas_call x4, Pallas kernels, call(): pl.pallas_call(kernel, out_shape=out_shape, in_specs=[smem] * scalars + [...  7.76 us
    all_to_all x1, starting transfers between devices, exchange(): return lax.all_to_all(v, 'ep', split_axis=0, concat_axis=0, tiled=True)  6.13 us
    unnamed x17, local copies, waits for them, and re-layouts  4.85 us
  transfers between devices with their start and end apart: 4, of which 4 were waited for; matrix products, arithmetic and copies ran while one was open for 0% of the time, Pallas kernels for 0%

profile of v2, /device:TPU:32, one launch (start us, length us, event | category | flops | bytes accessed | tf_op | source)
XLA Modules:
  0.0 151.1 jit_solution(12847352932731359318)
XLA Ops:
  0.0 0.0 collective-permute-start
  0.0 1.5 collective-permute-done.other_ref
  1.5 0.0 copy-start.4
  1.5 0.8 copy-done.4
  2.3 0.0 copy-start.5
  2.3 0.7 copy-done.5
  3.0 0.0 copy-start.6
  3.0 0.7 copy-done.6
  3.7 0.9 shard_map.73
  4.6 0.0 copy-start.2
  4.6 69.3 %all_to_all.10.own_ref = bf16[128,16,512]{2,1,0:T(8,128)(2,1)S(1)} all-to-all(bf16[128,16,512]{2,1,0:T(8,128)(2,1)S(1)} %get-tuple-element.7), channel_id=1, replica_groups=mesh['ep'=128,'tp'=2] {'ep'}, dimensions={0} | all-to-all | bytes 4194304 | tf_op jit(solution)/shard_map/all_to_all | solution.py:123
  73.9 0.0 collective-permute-start.1
  73.9 4.3 %collective-permute-done.1.other_ref = bf16[128,16,512]{2,1,0:T(8,128)(2,1)} collective-permute-done((bf16[128,16,512]{2,1,0:T(8,128)(2,1)S(1)}, bf16[128,16,512]{2,1,0:T(8,128)(2,1)}, u32[]{:S(2)}, u32[]{:S(2)}) %collective-permute-start.1) | collective-permute-done | bytes 2097184 | tf_op jit(solution)/shard_map/ppermute | solution.py:120
  78.2 0.0 copy-done.2
  78.2 0.0 copy-start.3
  78.2 1.2 copy-done.3
  79.4 0.0 copy-start.1
  79.4 4.1 %shard_map.74.own_ref = bf16[2,1024,256]{2,1,0:T(8,128)(2,1)S(1)} custom-call(s32[1]{0:T(128)} %bitcast.core_ref, bf16[128,16,512]{2,1,0:T(8,128)(2,1)S(1)} %all_to_all.10.own_ref, bf16[128,16,512]{2,1,0:T(8,128)(2,1)} %collective-permute-done.1.other_ref, bf16[2,1024,256]{2,1,0:T(8,128)(2,1)S(1)} %copy-done.2, bf16[2,1024,256]{2,1,0:T(8,128)(2,1)S(1)} %copy-done.3), custom_call_target="tpu_custom_call" | custom-call | flops 2147483648 | bytes 6291460 | tf_op jit(solution)/shard_map/pallas_call | solution.py:103
  83.5 0.2 collective-permute-start.2
  83.7 2.5 %collective-permute-done.2.other_ref = bf16[2,1024,256]{2,1,0:T(8,128)(2,1)S(1)} collective-permute-done((bf16[2,1024,256]{2,1,0:T(8,128)(2,1)S(1)}, bf16[2,1024,256]{2,1,0:T(8,128)(2,1)S(1)}, u32[]{:S(2)}, u32[]{:S(2)}) %collective-permute-start.2) | collective-permute-done | bytes 1048608 | tf_op jit(solution)/shard_map/ppermute | solution.py:120
  86.3 0.0 copy-done.1
  86.3 1.3 shard_map.75
  87.5 0.0 copy-start
  87.5 1.3 copy-done
  88.8 0.0 copy-start.7
  88.8 6.1 %all-to-all-start.1 = ((bf16[128,16,512]{2,1,0:T(8,128)(2,1)}), bf16[128,16,512]{2,1,0:T(8,128)(2,1)S(1)}, u32[]{:S(2)}, u32[]{:S(2)}) async-start(bf16[128,16,512]{2,1,0:T(8,128)(2,1)} %copy-done), calls=%async_computation.1 | async-start | bytes 4194304 | tf_op jit(solution)/shard_map/all_to_all | solution.py:123
  95.0 0.0 copy-done.7
  95.0 0.1 copy.9.weight_ref
  95.1 0.1 copy.8
  95.2 54.4 %all-to-all-done.1.back_ref = bf16[128,16,512]{2,1,0:T(8,128)(2,1)S(1)} async-done(((bf16[128,16,512]{2,1,0:T(8,128)(2,1)}), bf16[128,16,512]{2,1,0:T(8,128)(2,1)S(1)}, u32[]{:S(2)}, u32[]{:S(2)}) %all-to-all-start.1) | async-done | bytes 2097184 | tf_op jit(solution)/shard_map/all_to_all | solution.py:123
  149.6 1.5 %shard_map.76 = bf16[64,512]{1,0:T(8,128)(2,1)} custom-call(bf16[128,16,512]{2,1,0:T(8,128)(2,1)S(1)} %all-to-all-done.1.back_ref, s32[64,2]{1,0:T(8,128)S(1)} %bitcast.4, f32[64,2]{1,0:T(8,128)S(1)} %copy.9.weight_ref), custom_call_target="tpu_custom_call" | custom-call | flops 268435456 | bytes 2098176 | tf_op jit(solution)/shard_map/pallas_call | solution.py:103
Async XLA Ops:
  0.0 1.5 collective-permute-start
  1.5 0.8 copy-start.4
  2.3 0.7 copy-start.5
  3.0 0.7 copy-start.6
  4.6 73.6 %copy-start.2 = (bf16[2,1024,256]{2,1,0:T(8,128)(2,1)S(1)}, bf16[2,1024,256]{2,1,0:T(8,128)(2,1)}, u32[]{:S(2)}) copy-start(bf16[2,1024,256]{2,1,0:T(8,128)(2,1)} %gate_ref.1) | copy-start | bytes 3145732
  73.9 4.3 %collective-permute-start.1 = (bf16[128,16,512]{2,1,0:T(8,128)(2,1)S(1)}, bf16[128,16,512]{2,1,0:T(8,128)(2,1)}, u32[]{:S(2)}, u32[]{:S(2)}) collective-permute-start(bf16[128,16,512]{2,1,0:T(8,128)(2,1)S(1)} %all_to_all.10.own_ref), channel_id=1, source_target_pairs={{0,1},{1,0},{2,3},{3,2},{4,5},{5,4},{6,7},{7,6},{8,9},{9,8},{10,11... | collective-permute-start | bytes 6291464 | tf_op jit(solution)/shard_map/ppermute | solution.py:120
  78.2 1.2 copy-start.3
  79.4 6.9 %copy-start.1 = (bf16[2,512,512]{2,1,0:T(8,128)(2,1)S(1)}, bf16[2,512,512]{2,1,0:T(8,128)(2,1)}, u32[]{:S(2)}) copy-start(bf16[2,512,512]{2,1,0:T(8,128)(2,1)} %down_ref.1) | copy-start | bytes 3145732
  83.5 2.7 %collective-permute-start.2 = (bf16[2,1024,256]{2,1,0:T(8,128)(2,1)S(1)}, bf16[2,1024,256]{2,1,0:T(8,128)(2,1)S(1)}, u32[]{:S(2)}, u32[]{:S(2)}) collective-permute-start(bf16[2,1024,256]{2,1,0:T(8,128)(2,1)S(1)} %shard_map.74.own_ref), channel_id=1, source_target_pairs={{0,1},{1,0},{2,3},{3,2},{4,5},{5,4},{6,7},{7,6},{8,9},{9,8},{10,11... | collective-permute-start | bytes 3145736 | tf_op jit(solution)/shard_map/ppermute | solution.py:120
  87.5 1.3 copy-start
  88.8 6.1 %copy-start.7 = (f32[64,2]{0,1:T(2,128)S(1)}, f32[64,2]{0,1:T(2,128)}, u32[]{:S(2)}) copy-start(f32[64,2]{0,1:T(2,128)} %param.10) | copy-start | bytes 1540
  88.8 60.8 %all-to-all-start.1 = ((bf16[128,16,512]{2,1,0:T(8,128)(2,1)}), bf16[128,16,512]{2,1,0:T(8,128)(2,1)S(1)}, u32[]{:S(2)}, u32[]{:S(2)}) async-start(bf16[128,16,512]{2,1,0:T(8,128)(2,1)} %copy-done), calls=%async_computation.1 | async-start | bytes 4194304 | tf_op jit(solution)/shard_map/all_to_all | solution.py:123

commit v3 on v2

v3 whole, which is shorter than its diff:
```python
import functools

import jax
import jax.numpy as jnp
from jax import lax
from jax.experimental import pallas as pl
from jax.experimental.pallas import tpu as pltpu
from jax.sharding import Mesh, PartitionSpec as P

CAP = 8
EPS = 1e-06
INFO = 8
F32 = jnp.float32
BF16 = jnp.bfloat16
dot = functools.partial(jnp.dot, preferred_element_type=F32)


def iota(shape, dim):
    return lax.broadcasted_iota(jnp.int32, shape, dim)


def one_hot(mask):
    return mask.astype(F32).astype(BF16)


def norm_kernel(own_ref, other_ref, gain_ref, route_ref, weight_ref, out_ref):
    rows, half = own_ref.shape
    own = own_ref[...].astype(F32)
    other = other_ref[...].astype(F32)
    total = jnp.sum(own * own, axis=1, keepdims=True) + jnp.sum(other * other, axis=1, keepdims=True)
    scale = lax.rsqrt(total / (2 * half) + EPS)
    out_ref[0:rows, :] = (own * scale * gain_ref[...]).astype(BF16)
    weight = weight_ref[...]
    high = weight.astype(BF16).astype(F32)
    middle = (weight - high).astype(BF16).astype(F32)
    low = weight - high - middle
    info = jnp.concatenate([route_ref[...].astype(F32), high, middle, low], axis=0)
    out_ref[rows:, :] = jnp.zeros((INFO, half), BF16)
    out_ref[rows:, 0:rows] = info.astype(BF16)


def dispatch_kernel(column_ref, *refs):
    blocks, (out_ref, table_ref) = refs[:-2], refs[-2:]
    rows = blocks[0].shape[0] - INFO
    span = 2 * rows
    peers, block, half = out_ref.shape
    experts = 2 * peers
    first_expert = column_ref[0] * experts
    earlier = one_hot(
        (iota((span, span), 0) < iota((span, span), 1))
        & (iota((span, span), 0) // rows == iota((span, span), 1) // rows)
    )
    side = iota((1, span), 1) // rows
    expert = iota((experts, span), 0)
    slots, weights = [], []
    for pair in range(len(blocks) // 2):
        a, b = blocks[2 * pair], blocks[2 * pair + 1]
        info = jnp.concatenate([a[rows:, 0:rows].astype(F32), b[rows:, 0:rows].astype(F32)], axis=1)
        tokens = jnp.concatenate([a[0:rows, :], b[0:rows, :]], axis=0)
        picks = [info[k : k + 1].astype(jnp.int32) - first_expert for k in range(2)]
        ahead = dot(one_hot((expert == picks[0]) | (expert == picks[1])), earlier)
        places = []
        for k in range(2):
            rank = jnp.sum(jnp.where(expert == picks[k], ahead, 0.0), axis=0, keepdims=True)
            inside = (picks[k] >= 0) & (picks[k] < experts)
            place = (picks[k] % 2) * (16 * peers) + (picks[k] // 2) * 16 + side * CAP + rank.astype(jnp.int32)
            places.append(jnp.where(inside, place, -1))
            slots.append(places[k].astype(F32))
            weights.append(info[2 + k : 3 + k] + info[4 + k : 5 + k] + info[6 + k : 7 + k])
        for local in range(2):
            at = local * (block // 2) + 16 * pair
            place = iota((16 * peers, span), 0) + local * 16 * peers
            sent = dot(one_hot((place == places[0]) | (place == places[1])), tokens)
            out_ref[:, at : at + 16, :] = sent.astype(BF16).reshape(peers, 16, half)
    table_ref[...] = jnp.concatenate(slots + weights, axis=0).T


def halves(core_ref, half):
    core = core_ref[0]
    here = pl.ds(pl.multiple_of(core * half, half), half)
    there = pl.ds(pl.multiple_of((1 - core) * half, half), half)
    return here, there


def half_kernel(core_ref, own_ref, gate_ref, up_ref, out_ref):
    peers, block, half = own_ref.shape
    width = gate_ref.shape[2]
    here, _ = halves(core_ref, half)
    part = block // 2
    step = 256 // part
    for expert in range(2):
        for at in range(0, peers, step):
            own = own_ref[at : at + step, expert * part : (expert + 1) * part].reshape(256, half)
            rows = slice(at * part, (at + step) * part)
            out_ref[expert, rows, 0:width] = dot(own, gate_ref[expert, here, :])
            out_ref[expert, rows, width:] = dot(own, up_ref[expert, here, :])


def hidden_kernel(core_ref, half_ref, other_ref, gate_ref, up_ref, out_ref):
    peers, block, half = other_ref.shape
    width = gate_ref.shape[2]
    _, there = halves(core_ref, half)
    part = block // 2
    step = 256 // part
    for expert in range(2):
        for at in range(0, peers, step):
            other = other_ref[at : at + step, expert * part : (expert + 1) * part].reshape(256, half)
            rows = slice(at * part, (at + step) * part)
            gate = half_ref[expert, rows, 0:width] + dot(other, gate_ref[expert, there, :])
            up = half_ref[expert, rows, width:] + dot(other, up_ref[expert, there, :])
            out_ref[expert, rows] = (gate / (1.0 + jnp.exp(-gate)) * up).astype(BF16)


def down_kernel(core_ref, own_ref, other_ref, down_ref, out_ref):
    experts, total, quarter = own_ref.shape
    here, there = halves(core_ref, quarter)
    peers, block, half = out_ref.shape
    part = block // 2
    step = 256 // part
    for expert in range(experts):
        for at in range(0, peers, step):
            rows = slice(at * part, (at + step) * part)
            result = dot(own_ref[expert, rows], down_ref[expert, here, :]) + dot(
                other_ref[expert, rows], down_ref[expert, there, :]
            )
            out_ref[at : at + step, expert * part : (expert + 1) * part] = result.astype(BF16).reshape(
                step, part, half
            )


def combine_kernel(column_ref, back_ref, table_ref, out_ref):
    columns, rows, half = out_ref.shape
    peers, block, _ = back_ref.shape
    span = 2 * rows
    for pair in range(columns // 2):
        picked = [None, None]
        for local in range(2):
            at = local * (block // 2) + 16 * pair
            back = back_ref[:, at : at + 16, :].reshape(16 * peers, half)
            place = iota((span, 16 * peers), 1) + local * 16 * peers
            for k in range(2):
                index = 2 * pair + k
                slot = table_ref[:, index : index + 1].astype(jnp.int32)
                term = dot(one_hot(place == slot), back)
                picked[k] = term if picked[k] is None else picked[k] + term
        index = columns + 2 * pair
        total = picked[0] * table_ref[:, index : index + 1] + picked[1] * table_ref[:, index + 1 : index + 2]
        total = total.astype(BF16)
        for side in range(2):
            to = lax.rem(column_ref[0] - (2 * pair + side) + columns, columns)
            out_ref[to] = total[side * rows : (side + 1) * rows]


def call(kernel, out_shape, args, flops, grant, scalars=0):
    moved = sum(a.size * a.dtype.itemsize for a in args)
    smem = pl.BlockSpec(memory_space=pltpu.SMEM)
    whole = pl.BlockSpec(memory_space=pltpu.VMEM)
    return pl.pallas_call(
        kernel,
        out_shape=out_shape,
        in_specs=[smem] * scalars + [whole] * (len(args) - scalars),
        cost_estimate=pl.CostEstimate(flops=flops, bytes_accessed=moved, transcendentals=0),
        compiler_params=pltpu.CompilerParams(vmem_limit_bytes=grant << 20),
    )(*args)


def local(tokens, norm_gain, routing, route_weight, w_gate, w_up, w_down):
    rows, half = tokens.shape
    columns = lax.axis_size("zh")
    plane = ("zl", "y", "x")
    peers = lax.axis_size(plane)
    experts, _, width = w_gate.shape
    block = experts * columns * CAP
    total = peers * block
    core = lax.axis_index("tp").astype(jnp.int32).reshape(1)
    column = lax.axis_index("zh").astype(jnp.int32).reshape(1)

    def swap(v):
        return lax.ppermute(v, "tp", [(0, 1), (1, 0)])

    def shift(v, by):
        return lax.ppermute(v, "zh", [(i, (i + by) % columns) for i in range(columns)])

    def exchange(v, axes):
        return lax.all_to_all(v, axes, split_axis=0, concat_axis=0, tiled=True)

    own = call(
        norm_kernel,
        jax.ShapeDtypeStruct((rows + INFO, half), BF16),
        (tokens, swap(tokens), norm_gain.reshape(1, half), routing.T, route_weight.T),
        4 * rows * half,
        4,
    )
    before, after = shift(own, 1), shift(own, -1)
    blocks = (own, before, shift(before, 1), after)

    buffer = jax.ShapeDtypeStruct((peers, block, half), BF16)
    sent, table = call(
        dispatch_kernel,
        (buffer, jax.ShapeDtypeStruct((2 * rows, 2 * columns), F32)),
        (column, *blocks),
        2 * total * 2 * rows * half,
        12,
        1,
    )
    arrived = exchange(sent, plane)
    other = swap(arrived)
    partial = call(
        half_kernel,
        jax.ShapeDtypeStruct((experts, total // experts, 2 * width), F32),
        (core, arrived, w_gate, w_up),
        4 * total * half * width,
        16,
        1,
    )
    hidden = call(
        hidden_kernel,
        jax.ShapeDtypeStruct((experts, total // experts, width), BF16),
        (core, partial, other, w_gate, w_up),
        4 * total * half * width,
        16,
        1,
    )
    result = call(down_kernel, buffer, (core, hidden, swap(hidden), w_down), 4 * total * width * half, 12, 1)
    back = exchange(result, plane)
    mixed = call(
        combine_kernel,
        jax.ShapeDtypeStruct((columns, rows, half), BF16),
        (column, back, table),
        4 * total * 2 * rows * half,
        12,
        1,
    )
    home = exchange(mixed, "zh")
    return jnp.sum(home.astype(F32), axis=0).astype(BF16)


def solution(mesh):
    mesh = Mesh(mesh.devices.reshape(4, 2, 4, 4, 2), ("zh", "zl", "y", "x", "tp"))
    ep = ("zh", "zl", "y", "x")
    in_specs = (
        P(ep, "tp"),
        P("tp"),
        P(ep, None),
        P(ep, None),
        P(ep, None, "tp"),
        P(ep, None, "tp"),
        P(ep, None, "tp"),
    )
    return jax.shard_map(local, mesh=mesh, in_specs=in_specs, out_specs=P(ep, "tp"), check_vma=False)
```

time: 151 us -> 127 us (0.84); the launches traced: 151 us -> 126 us
  waiting for transfers between devices: 62.7 us -> 16 us
  blocking collectives: 69.3 us -> 90.5 us
    all_to_all x1 -> x0, waiting for transfers between devices: 54.4 us -> none  [exchange(): return lax.all_to_all(v, 'ep', split_axis=0, concat_axis=0, tiled=True)]
    all_to_all x1 -> x3, blocking collectives: 69.3 us -> 90.5 us  [exchange(): return lax.all_to_all(v, axes, split_axis=0, concat_axis=0, tiled=True)]
    ppermute x0 -> x3, waiting for transfers between devices: none -> 10.3 us  [shift(): lax.ppermute(v, 'zh', [(i, (i + by) % columns) for i in range(columns)])]
    ppermute x0 -> x3, starting transfers between devices: none -> 6.41 us  [shift(): lax.ppermute(v, 'zh', [(i, (i + by) % columns) for i in range(columns)])]
    all_to_all x1 -> x0, starting transfers between devices: 6.13 us -> none  [exchange(): return lax.all_to_all(v, 'ep', split_axis=0, concat_axis=0, tiled=True)]
    ppermute x3, waiting for transfers between devices: 8.27 us -> 5.76 us  [swap(): return lax.ppermute(v, 'tp', [(0, 1), (1, 0)])]
    unnamed x17 -> x14, local copies, waits for them, and re-layouts: 4.85 us -> 4.11 us
    pallas_call x4 -> x6, Pallas kernels: 7.76 us -> 7.48 us  [call(): pl.pallas_call(kernel, out_shape=out_shape, in_specs=[smem] * scalars + [...]
  transfers between devices with their start and end apart: 4 -> 6, of which waited for: 4 -> 5; matrix products, arithmetic and copies ran while one was open for 0% -> 0% of each run, Pallas kernels for 0% -> 1%
where the time goes in v3:
time: 127 us; the launch traced here: 126 us
  blocking collectives  90.5 us (71%)
  waiting for transfers between devices  16 us (13%)
  Pallas kernels  7.48 us (6%)
  starting transfers between devices  6.64 us (5%)
  local copies, waits for them, and re-layouts  4.11 us (3%)
    all_to_all x3, blocking collectives, exchange(): return lax.all_to_all(v, axes, split_axis=0, concat_axis=0, tiled=True)  90.5 us
    ppermute x3, waiting for transfers between devices, shift(): lax.ppermute(v, 'zh', [(i, (i + by) % columns) for i in range(columns)])  10.3 us
    pallas_call x6, Pallas kernels, call(): pl.pallas_call(kernel, out_shape=out_shape, in_specs=[smem] * scalars + [...  7.48 us
    ppermute x3, starting transfers between devices, shift(): lax.ppermute(v, 'zh', [(i, (i + by) % columns) for i in range(columns)])  6.41 us
    ppermute x3, waiting for transfers between devices, swap(): return lax.ppermute(v, 'tp', [(0, 1), (1, 0)])  5.76 us
    unnamed x14, local copies, waits for them, and re-layouts  4.11 us
  transfers between devices with their start and end apart: 6, of which 5 were waited for; matrix products, arithmetic and copies ran while one was open for 0% of the time, Pallas kernels for 1%

profile of v3, /device:TPU:32, one launch (start us, length us, event | category | flops | bytes accessed | tf_op | source)
XLA Modules:
  0.0 125.5 jit_solution(13112009559874135195)
XLA Ops:
  0.0 0.0 collective-permute-start
  0.0 1.5 %collective-permute-done.other_ref = bf16[64,512]{1,0:T(8,128)(2,1)S(1)} collective-permute-done((bf16[64,512]{1,0:T(8,128)(2,1)}, bf16[64,512]{1,0:T(8,128)(2,1)S(1)}, u32[]{:S(2)}, u32[]{:S(2)}) %collective-permute-start) | collective-permute-done | bytes 65568 | tf_op jit(solution)/shard_map/ppermute | solution.py:179
  1.5 0.0 copy-start.3
  1.5 0.8 copy-done.3
  2.3 0.0 copy-start.4
  2.3 0.7 copy-done.4
  3.0 0.0 copy-start.5
  3.0 0.7 copy-done.5
  3.7 0.0 copy-start.6
  3.7 0.7 copy-done.6
  4.3 0.1 shard_map.73.refs_0_
  4.5 3.3 %collective-permute-start.1 = (bf16[72,512]{1,0:T(8,128)(2,1)S(1)}, bf16[72,512]{1,0:T(8,128)(2,1)S(1)}, u32[]{:S(2)}, u32[]{:S(2)}) collective-permute-start(bf16[72,512]{1,0:T(8,128)(2,1)S(1)} %shard_map.73.refs_0_), channel_id=1, source_target_pairs={{0,64},{64,128},{128,192},{192,0},{1,65},{65,129},{129,193},{193,1... | collective-permute-start | bytes 221192 | tf_op jit(solution)/shard_map/ppermute | solution.py:182
  7.8 2.2 %collective-permute-start.3 = (bf16[72,512]{1,0:T(8,128)(2,1)S(1)}, bf16[72,512]{1,0:T(8,128)(2,1)S(1)}, u32[]{:S(2)}, u32[]{:S(2)}) collective-permute-start(bf16[72,512]{1,0:T(8,128)(2,1)S(1)} %shard_map.73.refs_0_), channel_id=1, source_target_pairs={{0,192},{64,0},{128,64},{192,128},{1,193},{65,1},{129,65},{193,129... | collective-permute-start | bytes 221192 | tf_op jit(solution)/shard_map/ppermute | solution.py:182
  10.0 4.1 %collective-permute-done.1.refs_1_ = bf16[72,512]{1,0:T(8,128)(2,1)S(1)} collective-permute-done((bf16[72,512]{1,0:T(8,128)(2,1)S(1)}, bf16[72,512]{1,0:T(8,128)(2,1)S(1)}, u32[]{:S(2)}, u32[]{:S(2)}) %collective-permute-start.1) | collective-permute-done | bytes 73760 | tf_op jit(solution)/shard_map/ppermute | solution.py:182
  14.2 0.8 collective-permute-start.2
  15.0 0.0 collective-permute-done.3.refs_3_
  15.0 6.2 %collective-permute-done.2.refs_2_ = bf16[72,512]{1,0:T(8,128)(2,1)S(1)} collective-permute-done((bf16[72,512]{1,0:T(8,128)(2,1)S(1)}, bf16[72,512]{1,0:T(8,128)(2,1)S(1)}, u32[]{:S(2)}, u32[]{:S(2)}) %collective-permute-start.2) | collective-permute-done | bytes 73760 | tf_op jit(solution)/shard_map/ppermute | solution.py:182
  21.2 1.0 shard_map.74
  22.2 0.0 copy-start
  22.2 36.5 %all_to_all.15.own_ref = bf16[32,64,512]{2,1,0:T(8,128)(2,1)S(1)} all-to-all(bf16[32,64,512]{2,1,0:T(8,128)(2,1)S(1)} %get-tuple-element.7), channel_id=1, replica_groups=mesh['zh'=4,'zl'=2,'y'=4,'x'=4,'tp'=2] {'zl','y','x'}, dimensions={0} | all-to-all | bytes 4194304 | tf_op jit(solution)/shard_map/all_to_all | solution.py:185
  58.7 0.0 collective-permute-start.4
  58.7 0.0 copy-done
  58.7 0.0 copy-start.1
  58.7 1.2 copy-done.1
  59.9 1.3 %shard_map.75.half_ref = f32[2,1024,512]{2,1,0:T(8,128)S(1)} custom-call(s32[1]{0:T(128)} %bitcast.1.core_ref, bf16[32,64,512]{2,1,0:T(8,128)(2,1)S(1)} %all_to_all.15.own_ref, bf16[2,1024,256]{2,1,0:T(8,128)(2,1)S(1)} %copy-done, bf16[2,1024,256]{2,1,0:T(8,128)(2,1)S(1)} %copy-done.1), custom_call_target="tpu_custom_call" | custom-call | flops 1073741824 | bytes 4194308 | tf_op jit(solution)/shard_map/pallas_call | solution.py:158
  61.2 0.0 copy-start.2
  61.2 1.8 %collective-permute-done.4.other_ref = bf16[32,64,512]{2,1,0:T(8,128)(2,1)} collective-permute-done((bf16[32,64,512]{2,1,0:T(8,128)(2,1)S(1)}, bf16[32,64,512]{2,1,0:T(8,128)(2,1)}, u32[]{:S(2)}, u32[]{:S(2)}) %collective-permute-start.4) | collective-permute-done | bytes 2097184 | tf_op jit(solution)/shard_map/ppermute | solution.py:179
  63.0 3.0 %shard_map.76.own_ref = bf16[2,1024,256]{2,1,0:T(8,128)(2,1)S(1)} custom-call(s32[1]{0:T(128)} %bitcast.1.core_ref, f32[2,1024,512]{2,1,0:T(8,128)S(1)} %shard_map.75.half_ref, bf16[32,64,512]{2,1,0:T(8,128)(2,1)} %collective-permute-done.4.other_ref, bf16[2,1024,256]{2,1,0:T(8,128)(2,1)S(1)} %copy-done, bf16[2,1024,256]{2,1,0:T(8,128)(2,1)S(1)} %copy-done.1), custom_call_target="tpu_custom_call" | custom-call | flops 1073741824 | bytes 8388612 | tf_op jit(solution)/shard_map/pallas_call | solution.py:158
  66.0 0.2 collective-permute-start.5
  66.2 2.5 %collective-permute-done.5.other_ref = bf16[2,1024,256]{2,1,0:T(8,128)(2,1)S(1)} collective-permute-done((bf16[2,1024,256]{2,1,0:T(8,128)(2,1)S(1)}, bf16[2,1024,256]{2,1,0:T(8,128)(2,1)S(1)}, u32[]{:S(2)}, u32[]{:S(2)}) %collective-permute-start.5) | collective-permute-done | bytes 1048608 | tf_op jit(solution)/shard_map/ppermute | solution.py:179
  68.8 0.0 copy-done.2
  68.8 1.3 shard_map.77
  70.0 34.3 %all_to_all.16.back_ref = bf16[32,64,512]{2,1,0:T(8,128)(2,1)S(1)} all-to-all(bf16[32,64,512]{2,1,0:T(8,128)(2,1)S(1)} %shard_map.77), channel_id=1, replica_groups=mesh['zh'=4,'zl'=2,'y'=4,'x'=4,'tp'=2] {'zl','y','x'}, dimensions={0} | all-to-all | bytes 4194304 | tf_op jit(solution)/shard_map/all_to_all | solution.py:185
  104.4 0.8 shard_map.78
  105.2 19.7 %all_to_all.17 = bf16[4,64,512]{2,1,0:T(8,128)(2,1)S(1)} all-to-all(bf16[4,64,512]{2,1,0:T(8,128)(2,1)S(1)} %shard_map.78), channel_id=1, replica_groups=mesh['zh'=4,'zl'=2,'y'=4,'x'=4,'tp'=2] {'zh'}, dimensions={0} | all-to-all | bytes 524288 | tf_op jit(solution)/shard_map/all_to_all | solution.py:185
  124.8 0.7 reduce_sum.12
Async XLA Ops:
  0.0 1.5 %collective-permute-start = (bf16[64,512]{1,0:T(8,128)(2,1)}, bf16[64,512]{1,0:T(8,128)(2,1)S(1)}, u32[]{:S(2)}, u32[]{:S(2)}) collective-permute-start(bf16[64,512]{1,0:T(8,128)(2,1)} %own_ref.1), channel_id=1, source_target_pairs={{0,1},{1,0},{2,3},{3,2},{4,5},{5,4},{6,7},{7,6},{8,9},{9,8},{10,11... | collective-permute-start | bytes 196616 | tf_op jit(solution)/shard_map/ppermute | solution.py:179
  1.5 0.8 copy-start.3
  2.3 0.7 copy-start.4
  3.0 0.7 copy-start.5
  3.7 0.7 copy-start.6
  4.5 9.7 %collective-permute-start.1 = (bf16[72,512]{1,0:T(8,128)(2,1)S(1)}, bf16[72,512]{1,0:T(8,128)(2,1)S(1)}, u32[]{:S(2)}, u32[]{:S(2)}) collective-permute-start(bf16[72,512]{1,0:T(8,128)(2,1)S(1)} %shard_map.73.refs_0_), channel_id=1, source_target_pairs={{0,64},{64,128},{128,192},{192,0},{1,65},{65,129},{129,193},{193,1... | collective-permute-start | bytes 221192 | tf_op jit(solution)/shard_map/ppermute | solution.py:182
  7.8 7.2 %collective-permute-start.3 = (bf16[72,512]{1,0:T(8,128)(2,1)S(1)}, bf16[72,512]{1,0:T(8,128)(2,1)S(1)}, u32[]{:S(2)}, u32[]{:S(2)}) collective-permute-start(bf16[72,512]{1,0:T(8,128)(2,1)S(1)} %shard_map.73.refs_0_), channel_id=1, source_target_pairs={{0,192},{64,0},{128,64},{192,128},{1,193},{65,1},{129,65},{193,129... | collective-permute-start | bytes 221192 | tf_op jit(solution)/shard_map/ppermute | solution.py:182
  14.2 7.0 %collective-permute-start.2 = (bf16[72,512]{1,0:T(8,128)(2,1)S(1)}, bf16[72,512]{1,0:T(8,128)(2,1)S(1)}, u32[]{:S(2)}, u32[]{:S(2)}) collective-permute-start(bf16[72,512]{1,0:T(8,128)(2,1)S(1)} %collective-permute-done.1.refs_1_), channel_id=1, source_target_pairs={{0,64},{64,128},{128,192},{192,0},{1,65},{65,129},{129,193},{193,1... | collective-permute-start | bytes 221192 | tf_op jit(solution)/shard_map/ppermute | solution.py:182
  22.2 36.5 %copy-start = (bf16[2,1024,256]{2,1,0:T(8,128)(2,1)S(1)}, bf16[2,1024,256]{2,1,0:T(8,128)(2,1)}, u32[]{:S(2)}) copy-start(bf16[2,1024,256]{2,1,0:T(8,128)(2,1)} %gate_ref.3) | copy-start | bytes 3145732
  58.7 4.3 %collective-permute-start.4 = (bf16[32,64,512]{2,1,0:T(8,128)(2,1)S(1)}, bf16[32,64,512]{2,1,0:T(8,128)(2,1)}, u32[]{:S(2)}, u32[]{:S(2)}) collective-permute-start(bf16[32,64,512]{2,1,0:T(8,128)(2,1)S(1)} %all_to_all.15.own_ref), channel_id=1, source_target_pairs={{0,1},{1,0},{2,3},{3,2},{4,5},{5,4},{6,7},{7,6},{8,9},{9,8},{10,11... | collective-permute-start | bytes 6291464 | tf_op jit(solution)/shard_map/ppermute | solution.py:179
  58.7 1.2 copy-start.1
  61.2 7.6 %copy-start.2 = (bf16[2,512,512]{2,1,0:T(8,128)(2,1)S(1)}, bf16[2,512,512]{2,1,0:T(8,128)(2,1)}, u32[]{:S(2)}) copy-start(bf16[2,512,512]{2,1,0:T(8,128)(2,1)} %down_ref.1) | copy-start | bytes 3145732
  66.0 2.7 %collective-permute-start.5 = (bf16[2,1024,256]{2,1,0:T(8,128)(2,1)S(1)}, bf16[2,1024,256]{2,1,0:T(8,128)(2,1)S(1)}, u32[]{:S(2)}, u32[]{:S(2)}) collective-permute-start(bf16[2,1024,256]{2,1,0:T(8,128)(2,1)S(1)} %shard_map.76.own_ref), channel_id=1, source_target_pairs={{0,1},{1,0},{2,3},{3,2},{4,5},{5,4},{6,7},{7,6},{8,9},{9,8},{10,11... | collective-permute-start | bytes 3145736 | tf_op jit(solution)/shard_map/ppermute | solution.py:179

commit v4 on v3

v4 whole, which is shorter than its diff:
```python
import functools

import jax
import jax.numpy as jnp
from jax import lax
from jax.experimental import pallas as pl
from jax.experimental.pallas import tpu as pltpu
from jax.sharding import Mesh, PartitionSpec as P


CAP = 8
EPS = 1e-06
INFO = 8
F32 = jnp.float32
BF16 = jnp.bfloat16
dot = functools.partial(jnp.dot, preferred_element_type=F32)


def iota(shape, dim):
    return lax.broadcasted_iota(jnp.int32, shape, dim)


def one_hot(mask):
    return mask.astype(F32).astype(BF16)


def block_kernel(own_ref, gain_ref, route_ref, weight_ref, out_ref, total_ref, gain_out_ref):
    rows, half = own_ref.shape
    out_ref[0:rows, :] = own_ref[...]
    own = own_ref[...].astype(F32)
    total_ref[...] = jnp.broadcast_to(jnp.sum(own * own, axis=1, keepdims=True), total_ref.shape)
    gain_out_ref[...] = gain_ref[...]
    weight = weight_ref[...]
    high = weight.astype(BF16).astype(F32)
    middle = (weight - high).astype(BF16).astype(F32)
    low = weight - high - middle
    info = jnp.concatenate([route_ref[...].astype(F32), high, middle, low], axis=0)
    out_ref[rows:, :] = jnp.zeros((INFO, half), BF16)
    out_ref[rows:, 0:rows] = info.astype(BF16)


def norm_kernel(block_ref, total_ref, gain_ref, other_ref, out_ref):
    rows, half = other_ref.shape
    other = other_ref[...].astype(F32)
    total = total_ref[:, 0:1] + jnp.sum(other * other, axis=1, keepdims=True)
    scale = lax.rsqrt(total / (2 * half) + EPS)
    out_ref[0:rows, :] = (block_ref[0:rows, :].astype(F32) * scale * gain_ref[...]).astype(BF16)
    out_ref[rows:, :] = block_ref[rows:, :]


def dispatch_kernel(place_ref, *refs):
    blocks, (out_ref, table_ref) = refs[:-2], refs[-2:]
    rows = blocks[0].shape[0] - INFO
    span = 2 * rows
    peers, block, half = out_ref.shape
    experts = 2 * peers
    first_expert = place_ref[0] // 2 * experts
    earlier = one_hot(
        (iota((span, span), 0) < iota((span, span), 1))
        & (iota((span, span), 0) // rows == iota((span, span), 1) // rows)
    )
    side = iota((1, span), 1) // rows
    expert = iota((experts, span), 0)
    slots, weights = [], []
    for pair in range(len(blocks) // 2):
        a, b = blocks[2 * pair], blocks[2 * pair + 1]
        info = jnp.concatenate([a[rows:, 0:rows].astype(F32), b[rows:, 0:rows].astype(F32)], axis=1)
        tokens = jnp.concatenate([a[0:rows, :], b[0:rows, :]], axis=0)
        picks = [info[k : k + 1].astype(jnp.int32) - first_expert for k in range(2)]
        ahead = dot(one_hot((expert == picks[0]) | (expert == picks[1])), earlier)
        places = []
        for k in range(2):
            rank = jnp.sum(jnp.where(expert == picks[k], ahead, 0.0), axis=0, keepdims=True)
            inside = (picks[k] >= 0) & (picks[k] < experts)
            place = (picks[k] % 2) * (16 * peers) + (picks[k] // 2) * 16 + side * CAP + rank.astype(jnp.int32)
            places.append(jnp.where(inside, place, -1))
            slots.append(places[k].astype(F32))
            weights.append(info[2 + k : 3 + k] + info[4 + k : 5 + k] + info[6 + k : 7 + k])
        for local in range(2):
            at = local * (block // 2) + 16 * pair
            place = iota((16 * peers, span), 0) + local * 16 * peers
            sent = dot(one_hot((place == places[0]) | (place == places[1])), tokens)
            out_ref[:, at : at + 16, :] = sent.astype(BF16).reshape(peers, 16, half)
    table_ref[...] = jnp.concatenate(slots + weights, axis=0).T


def expert_kernel(place_ref, rows_ref, gate_ref, up_ref, gate2_ref, up2_ref, down_ref, down2_ref, out_ref):
    core = place_ref[0] % 2
    chips, _, block, half = rows_ref.shape
    width = gate_ref.shape[2]
    sides = (core, 1 - core)
    spans = [pl.ds(pl.multiple_of(side * width, width), width) for side in sides]
    step = 256 // block
    for at in range(0, chips, step):
        low = rows_ref[at : at + step, 0].reshape(256, half)
        high = rows_ref[at : at + step, 1].reshape(256, half)

        def through(ref):
            return dot(low, ref[core, 0:half, :]) + dot(high, ref[core, half:, :])

        hidden = []
        for gate_half, up_half in ((gate_ref, up_ref), (gate2_ref, up2_ref)):
            gate = through(gate_half)
            hidden.append((gate / (1.0 + jnp.exp(-gate)) * through(up_half)).astype(BF16))
        for side, down in zip(sides, (down_ref, down2_ref)):
            result = dot(hidden[0], down[core, spans[0], :]) + dot(hidden[1], down[core, spans[1], :])
            out_ref[at : at + step, side] = result.astype(BF16).reshape(step, block, half)


def combine_kernel(place_ref, back_ref, table_ref, out_ref):
    columns, rows, half = out_ref.shape
    peers, block, _ = back_ref.shape
    span = 2 * rows
    for pair in range(columns // 2):
        picked = [None, None]
        for local in range(2):
            at = local * (block // 2) + 16 * pair
            back = back_ref[:, at : at + 16, :].reshape(16 * peers, half)
            place = iota((span, 16 * peers), 1) + local * 16 * peers
            for k in range(2):
                index = 2 * pair + k
                slot = table_ref[:, index : index + 1].astype(jnp.int32)
                term = dot(one_hot(place == slot), back)
                picked[k] = term if picked[k] is None else picked[k] + term
        index = columns + 2 * pair
        total = picked[0] * table_ref[:, index : index + 1] + picked[1] * table_ref[:, index + 1 : index + 2]
        total = total.astype(BF16)
        for side in range(2):
            to = lax.rem(place_ref[0] // 2 - (2 * pair + side) + columns, columns)
            out_ref[to] = total[side * rows : (side + 1) * rows]


def call(kernel, out_shape, args, flops, grant, scalars=0, **kw):
    moved = sum(a.size * a.dtype.itemsize for a in args)
    smem = pl.BlockSpec(memory_space=pltpu.SMEM)
    whole = pl.BlockSpec(memory_space=pltpu.VMEM)
    kw.setdefault("in_specs", [smem] * scalars + [whole] * (len(args) - scalars))
    return pl.pallas_call(
        kernel,
        out_shape=out_shape,
        cost_estimate=pl.CostEstimate(flops=flops, bytes_accessed=moved, transcendentals=0),
        compiler_params=pltpu.CompilerParams(vmem_limit_bytes=grant << 20),
        **kw,
    )(*args)


def local(tokens, norm_gain, routing, route_weight, w_gate, w_up, w_down):
    rows, half = tokens.shape
    columns = lax.axis_size("zh")
    plane = ("zl", "y", "x", "tp")
    peers = lax.axis_size(plane) // 2
    experts, _, width = w_gate.shape
    block = experts * columns * CAP
    total = peers * block
    place = (lax.axis_index("zh") * 2 + lax.axis_index("tp")).astype(jnp.int32).reshape(1)

    def swap(v):
        return lax.ppermute(v, "tp", [(0, 1), (1, 0)])

    def shift(v, by):
        return lax.ppermute(v, "zh", [(i, (i + by) % columns) for i in range(columns)])

    def exchange(v, axes):
        return lax.all_to_all(v, axes, split_axis=0, concat_axis=0, tiled=True)

    other = swap(tokens)
    gate2, up2, down2 = swap(w_gate), swap(w_up), swap(w_down)
    own = call(
        block_kernel,
        (
            jax.ShapeDtypeStruct((rows + INFO, half), BF16),
            jax.ShapeDtypeStruct((rows, 128), F32),
            jax.ShapeDtypeStruct((1, half), F32),
        ),
        (tokens, norm_gain.reshape(1, half), routing.T, route_weight.T),
        rows * half,
        4,
    )
    own = call(norm_kernel, jax.ShapeDtypeStruct((rows + INFO, half), BF16), (*own, other), rows * half, 4)
    opposite, before, after = shift(own, 2), shift(own, 1), shift(own, -1)
    blocks = (own, before, opposite, after)

    sent, table = call(
        dispatch_kernel,
        (
            jax.ShapeDtypeStruct((peers, block, half), BF16),
            jax.ShapeDtypeStruct((2 * rows, 2 * columns), F32),
        ),
        (place, *blocks),
        2 * total * 2 * rows * half,
        12,
        1,
    )
    arrived = exchange(sent.reshape(2 * peers, block // 2, half), plane)
    result = call(
        expert_kernel,
        jax.ShapeDtypeStruct((peers, 2, block // 2, half), BF16),
        (place, arrived.reshape(peers, 2, block // 2, half), w_gate, w_up, gate2, up2, w_down, down2),
        total * half * width * 12,
        20,
        1,
    )
    back = exchange(result.reshape(2 * peers, block // 2, half), plane)
    mixed = call(
        combine_kernel,
        jax.ShapeDtypeStruct((columns, rows, half), BF16),
        (place, back.reshape(peers, block, half), table),
        4 * total * 2 * rows * half,
        12,
        1,
    )
    home = exchange(mixed, "zh")
    return jnp.sum(home.astype(F32), axis=0).astype(BF16)


def solution(mesh):
    mesh = Mesh(mesh.devices.reshape(4, 2, 4, 4, 2), ("zh", "zl", "y", "x", "tp"))
    ep = ("zh", "zl", "y", "x")
    in_specs = (
        P(ep, "tp"),
        P("tp"),
        P(ep, None),
        P(ep, None),
        P(ep, None, "tp"),
        P(ep, None, "tp"),
        P(ep, None, "tp"),
    )

    return jax.shard_map(local, mesh=mesh, in_specs=in_specs, out_specs=P(ep, "tp"), check_vma=False)
```

time: 127 us -> 122 us (0.961)
  blocking collectives: 90.5 us -> 51.9 us
  starting transfers between devices: 6.64 us -> 21 us
  waiting for transfers between devices: 16 us -> 27.9 us
  local copies, waits for them, and re-layouts: 4.11 us -> 11.9 us
    all_to_all x3 -> x2, blocking collectives: 90.5 us -> 51.9 us  [exchange(): return lax.all_to_all(v, axes, split_axis=0, concat_axis=0, tiled=True)]
    all_to_all x0 -> x1, waiting for transfers between devices: none -> 20.5 us  [exchange(): return lax.all_to_all(v, axes, split_axis=0, concat_axis=0, tiled=True)]
    all_to_all x0 -> x1, starting transfers between devices: none -> 9.75 us  [exchange(): return lax.all_to_all(v, axes, split_axis=0, concat_axis=0, tiled=True)]
    unnamed x14 -> x26, local copies, waits for them, and re-layouts: 4.11 us -> 11.9 us
    ppermute x3, waiting for transfers between devices: 10.3 us -> 4.26 us  [shift(): lax.ppermute(v, 'zh', [(i, (i + by) % columns) for i in range(columns)])]
    ppermute x3, starting transfers between devices: 6.41 us -> 10.5 us  [shift(): lax.ppermute(v, 'zh', [(i, (i + by) % columns) for i in range(columns)])]
    ppermute x3 -> x4, waiting for transfers between devices: 5.76 us -> 3.07 us  [swap(): return lax.ppermute(v, 'tp', [(0, 1), (1, 0)])]
    pallas_call x6 -> x5, Pallas kernels: 7.48 us -> 7.28 us  [call(): pl.pallas_call(kernel, out_shape=out_shape, cost_estimate=pl.CostEstimate...]
  transfers between devices with their start and end apart: 6 -> 8, of which waited for: 5 -> 6; matrix products, arithmetic and copies ran while one was open for 0% -> 0% of each run, Pallas kernels for 1% -> 0%
where the time goes in v4:
time: 122 us; the launch traced here: 121 us
  blocking collectives  51.9 us (43%)
  waiting for transfers between devices  27.9 us (23%)
  starting transfers between devices  21 us (17%)
  local copies, waits for them, and re-layouts  11.9 us (10%)
  Pallas kernels  7.28 us (6%)
    all_to_all x2, blocking collectives, exchange(): return lax.all_to_all(v, axes, split_axis=0, concat_axis=0, tiled=True)  51.9 us
    all_to_all x1, waiting for transfers between devices, exchange(): return lax.all_to_all(v, axes, split_axis=0, concat_axis=0, tiled=True)  20.5 us
    unnamed x26, local copies, waits for them, and re-layouts  11.9 us
    ppermute x3, starting transfers between devices, shift(): lax.ppermute(v, 'zh', [(i, (i + by) % columns) for i in range(columns)])  10.5 us
    all_to_all x1, starting transfers between devices, exchange(): return lax.all_to_all(v, axes, split_axis=0, concat_axis=0, tiled=True)  9.75 us
    pallas_call x5, Pallas kernels, call(): pl.pallas_call(kernel, out_shape=out_shape, cost_estimate=pl.CostEstimate...  7.28 us
    ppermute x3, waiting for transfers between devices, shift(): lax.ppermute(v, 'zh', [(i, (i + by) % columns) for i in range(columns)])  4.26 us
    ppermute x4, waiting for transfers between devices, swap(): return lax.ppermute(v, 'tp', [(0, 1), (1, 0)])  3.07 us
  transfers between devices with their start and end apart: 8, of which 6 were waited for; matrix products, arithmetic and copies ran while one was open for 0% of the time, Pallas kernels for 0%

profile of v4, /device:TPU:32, one launch (start us, length us, event | category | flops | bytes accessed | tf_op | source)
XLA Modules:
  0.0 120.7 jit_solution(9318286189993751764)
XLA Ops:
  0.0 0.0 collective-permute-start
  0.0 0.0 copy-start
  0.0 0.8 copy-done
  0.8 0.0 copy-start.1
  0.8 0.7 copy-done.1
  1.5 0.0 copy-start.2
  1.5 0.7 copy-done.2
  2.2 0.0 copy-start.3
  2.2 0.7 copy-done.3
  2.9 0.1 shard_map.73
  3.0 0.0 collective-permute-done.other_ref
  3.0 0.2 shard_map.74.refs_0_
  3.2 3.3 %collective-permute-start.1 = (bf16[72,512]{1,0:T(8,128)(2,1)S(1)}, bf16[72,512]{1,0:T(8,128)(2,1)S(1)}, u32[]{:S(2)}, u32[]{:S(2)}) collective-permute-start(bf16[72,512]{1,0:T(8,128)(2,1)S(1)} %shard_map.74.refs_0_), channel_id=1, source_target_pairs={{0,64},{64,128},{128,192},{192,0},{1,65},{65,129},{129,193},{193,1... | collective-permute-start | bytes 221192 | tf_op jit(solution)/shard_map/ppermute | solution.py:161
  6.5 4.5 %collective-permute-start.2 = (bf16[72,512]{1,0:T(8,128)(2,1)S(1)}, bf16[72,512]{1,0:T(8,128)(2,1)S(1)}, u32[]{:S(2)}, u32[]{:S(2)}) collective-permute-start(bf16[72,512]{1,0:T(8,128)(2,1)S(1)} %shard_map.74.refs_0_), channel_id=1, source_target_pairs={{0,128},{64,192},{128,0},{192,64},{1,129},{65,193},{129,1},{193,65... | collective-permute-start | bytes 221192 | tf_op jit(solution)/shard_map/ppermute | solution.py:161
  11.0 2.7 %collective-permute-start.3 = (bf16[72,512]{1,0:T(8,128)(2,1)S(1)}, bf16[72,512]{1,0:T(8,128)(2,1)S(1)}, u32[]{:S(2)}, u32[]{:S(2)}) collective-permute-start(bf16[72,512]{1,0:T(8,128)(2,1)S(1)} %shard_map.74.refs_0_), channel_id=1, source_target_pairs={{0,192},{64,0},{128,64},{192,128},{1,193},{65,1},{129,65},{193,129... | collective-permute-start | bytes 221192 | tf_op jit(solution)/shard_map/ppermute | solution.py:161
  13.7 0.0 collective-permute-done.1.refs_1_
  13.7 1.3 %collective-permute-done.2.refs_2_ = bf16[72,512]{1,0:T(8,128)(2,1)S(1)} collective-permute-done((bf16[72,512]{1,0:T(8,128)(2,1)S(1)}, bf16[72,512]{1,0:T(8,128)(2,1)S(1)}, u32[]{:S(2)}, u32[]{:S(2)}) %collective-permute-start.2) | collective-permute-done | bytes 73760 | tf_op jit(solution)/shard_map/ppermute | solution.py:161
  15.1 2.9 %collective-permute-done.3.refs_3_ = bf16[72,512]{1,0:T(8,128)(2,1)S(1)} collective-permute-done((bf16[72,512]{1,0:T(8,128)(2,1)S(1)}, bf16[72,512]{1,0:T(8,128)(2,1)S(1)}, u32[]{:S(2)}, u32[]{:S(2)}) %collective-permute-start.3) | collective-permute-done | bytes 73760 | tf_op jit(solution)/shard_map/ppermute | solution.py:161
  18.0 2.4 %shard_map.75 = (bf16[32,64,512]{2,1,0:T(8,128)(2,1)}, f32[128,8]{1,0:T(8,128)S(1)}) custom-call(s32[1]{0:T(128)} %bitcast.place_ref, bf16[72,512]{1,0:T(8,128)(2,1)S(1)} %shard_map.74.refs_0_, bf16[72,512]{1,0:T(8,128)(2,1)S(1)} %collective-permute-done.1.refs_1_, bf16[72,512]{1,0:T(8,128)(2,1)S(1)} %collective-permute-done.2.refs_2_, ...), custom_call_target="tpu_custom_call" | custom-call | flops 268435456 | bytes 294916 | tf_op jit(solution)/shard_map/pallas_call | solution.py:138
  20.3 0.0 copy-start.4
  20.3 9.8 %all-to-all-start = ((bf16[64,32,512]{2,1,0:T(8,128)(2,1)}), bf16[64,32,512]{2,1,0:T(8,128)(2,1)S(1)}, u32[]{:S(2)}, u32[]{:S(2)}) async-start(bf16[64,32,512]{2,1,0:T(8,128)(2,1)} %bitcast.4), calls=%async_computation | async-start | bytes 4194304 | tf_op jit(solution)/shard_map/all_to_all | solution.py:164
  30.1 0.0 copy-done.4
  30.1 0.2 collective-permute-start.4
  30.3 0.4 collective-permute-start.5
  30.7 0.1 collective-permute-start.6
  30.8 2.0 %collective-permute-done.4.gate2_ref = bf16[2,1024,256]{2,1,0:T(8,128)(2,1)S(1)} collective-permute-done((bf16[2,1024,256]{2,1,0:T(8,128)(2,1)S(1)}, bf16[2,1024,256]{2,1,0:T(8,128)(2,1)S(1)}, u32[]{:S(2)}, u32[]{:S(2)}) %collective-permute-start.4) | collective-permute-done | bytes 1048608 | tf_op jit(solution)/shard_map/ppermute | solution.py:158
  32.9 0.0 copy-start.7
  32.9 1.0 copy-done.7
  33.8 0.5 collective-permute-done.5.up2_ref
  34.4 0.0 copy-start.9
  34.4 1.0 copy-done.9
  35.3 0.5 collective-permute-done.6.down2_ref
  35.9 0.0 copy-start.11
  35.9 1.0 copy-done.11
  36.8 20.5 %all-to-all-done = bf16[64,32,512]{2,1,0:T(8,128)(2,1)S(1)} async-done(((bf16[64,32,512]{2,1,0:T(8,128)(2,1)}), bf16[64,32,512]{2,1,0:T(8,128)(2,1)S(1)}, u32[]{:S(2)}, u32[]{:S(2)}) %all-to-all-start) | async-done | bytes 2097184 | tf_op jit(solution)/shard_map/all_to_all | solution.py:164
  57.4 0.0 copy-start.5
  57.4 1.2 %copy-done.5 = bf16[2,1024,256]{2,1,0:T(8,128)(2,1)S(1)} copy-done((bf16[2,1024,256]{2,1,0:T(8,128)(2,1)S(1)}, bf16[2,1024,256]{2,1,0:T(8,128)(2,1)}, u32[]{:S(2)}) %copy-start.5) | copy-done | bytes 1048600
  58.6 0.0 copy-start.6
  58.6 1.2 %copy-done.6 = bf16[2,512,512]{2,1,0:T(8,128)(2,1)S(1)} copy-done((bf16[2,512,512]{2,1,0:T(8,128)(2,1)S(1)}, bf16[2,512,512]{2,1,0:T(8,128)(2,1)}, u32[]{:S(2)}) %copy-start.6) | copy-done | bytes 1048600
  59.8 0.0 copy-start.8
  59.8 1.2 %copy-done.8 = bf16[2,1024,256]{2,1,0:T(8,128)(2,1)S(1)} copy-done((bf16[2,1024,256]{2,1,0:T(8,128)(2,1)S(1)}, bf16[2,1024,256]{2,1,0:T(8,128)(2,1)}, u32[]{:S(2)}) %copy-start.8) | copy-done | bytes 1048600
  61.0 0.0 copy-start.10
  61.0 1.2 %copy-done.10 = bf16[2,1024,256]{2,1,0:T(8,128)(2,1)S(1)} copy-done((bf16[2,1024,256]{2,1,0:T(8,128)(2,1)S(1)}, bf16[2,1024,256]{2,1,0:T(8,128)(2,1)}, u32[]{:S(2)}) %copy-start.10) | copy-done | bytes 1048600
  62.3 0.0 copy-start.12
  62.3 1.2 %copy-done.12 = bf16[2,512,512]{2,1,0:T(8,128)(2,1)S(1)} copy-done((bf16[2,512,512]{2,1,0:T(8,128)(2,1)S(1)}, bf16[2,512,512]{2,1,0:T(8,128)(2,1)}, u32[]{:S(2)}) %copy-start.12) | copy-done | bytes 1048600
  63.5 3.8 %shard_map.76 = bf16[32,2,32,512]{3,2,1,0:T(8,128)(2,1)S(1)} custom-call(s32[1]{0:T(128)} %bitcast.place_ref, bf16[32,2,32,512]{3,2,1,0:T(8,128)(2,1)S(1)} %bitcast.9, bf16[2,1024,256]{2,1,0:T(8,128)(2,1)S(1)} %copy-done.4, bf16[2,1024,256]{2,1,0:T(8,128)(2,1)S(1)} %copy-done.5, bf16[2,1024,256]{2,1,0:T(8,128)(2,1)S(1)} %copy-done.8, ...), custom_call_target="tpu_custom_call" | custom-call | flops 3221225472 | bytes 8388612 | tf_op jit(solution)/shard_map/pallas_call | solution.py:138
  67.3 34.8 %all_to_all.15 = bf16[64,32,512]{2,1,0:T(8,128)(2,1)S(1)} all-to-all(bf16[64,32,512]{2,1,0:T(8,128)(2,1)S(1)} %bitcast.10), channel_id=1, replica_groups=mesh['zh'=4,'zl'=2,'y'=4,'x'=4,'tp'=2] {'zl','y','x','tp'}, dimensions={0} | all-to-all | bytes 4194304 | tf_op jit(solution)/shard_map/all_to_all | solution.py:164
  102.2 0.8 shard_map.77
  103.0 17.1 %all_to_all.16 = bf16[4,64,512]{2,1,0:T(8,128)(2,1)S(1)} all-to-all(bf16[4,64,512]{2,1,0:T(8,128)(2,1)S(1)} %shard_map.77), channel_id=1, replica_groups=mesh['zh'=4,'zl'=2,'y'=4,'x'=4,'tp'=2] {'zh'}, dimensions={0} | all-to-all | bytes 524288 | tf_op jit(solution)/shard_map/all_to_all | solution.py:164
  120.0 0.7 reduce_sum.12
Async XLA Ops:
  0.0 3.0 %collective-permute-start = (bf16[64,512]{1,0:T(8,128)(2,1)}, bf16[64,512]{1,0:T(8,128)(2,1)S(1)}, u32[]{:S(2)}, u32[]{:S(2)}) collective-permute-start(bf16[64,512]{1,0:T(8,128)(2,1)} %own_ref.1), channel_id=1, source_target_pairs={{0,1},{1,0},{2,3},{3,2},{4,5},{5,4},{6,7},{7,6},{8,9},{9,8},{10,11... | collective-permute-start | bytes 196616 | tf_op jit(solution)/shard_map/ppermute | solution.py:158
  0.0 0.8 copy-start
  0.8 0.7 copy-start.1
  1.5 0.7 copy-start.2
  2.2 0.7 copy-start.3
  3.2 10.5 %collective-permute-start.1 = (bf16[72,512]{1,0:T(8,128)(2,1)S(1)}, bf16[72,512]{1,0:T(8,128)(2,1)S(1)}, u32[]{:S(2)}, u32[]{:S(2)}) collective-permute-start(bf16[72,512]{1,0:T(8,128)(2,1)S(1)} %shard_map.74.refs_0_), channel_id=1, source_target_pairs={{0,64},{64,128},{128,192},{192,0},{1,65},{65,129},{129,193},{193,1... | collective-permute-start | bytes 221192 | tf_op jit(solution)/shard_map/ppermute | solution.py:161
  6.5 8.5 %collective-permute-start.2 = (bf16[72,512]{1,0:T(8,128)(2,1)S(1)}, bf16[72,512]{1,0:T(8,128)(2,1)S(1)}, u32[]{:S(2)}, u32[]{:S(2)}) collective-permute-start(bf16[72,512]{1,0:T(8,128)(2,1)S(1)} %shard_map.74.refs_0_), channel_id=1, source_target_pairs={{0,128},{64,192},{128,0},{192,64},{1,129},{65,193},{129,1},{193,65... | collective-permute-start | bytes 221192 | tf_op jit(solution)/shard_map/ppermute | solution.py:161
  11.0 6.9 %collective-permute-start.3 = (bf16[72,512]{1,0:T(8,128)(2,1)S(1)}, bf16[72,512]{1,0:T(8,128)(2,1)S(1)}, u32[]{:S(2)}, u32[]{:S(2)}) collective-permute-start(bf16[72,512]{1,0:T(8,128)(2,1)S(1)} %shard_map.74.refs_0_), channel_id=1, source_target_pairs={{0,192},{64,0},{128,64},{192,128},{1,193},{65,1},{129,65},{193,129... | collective-permute-start | bytes 221192 | tf_op jit(solution)/shard_map/ppermute | solution.py:161
  20.3 9.8 %copy-start.4 = (bf16[2,1024,256]{2,1,0:T(8,128)(2,1)S(1)}, bf16[2,1024,256]{2,1,0:T(8,128)(2,1)}, u32[]{:S(2)}) copy-start(bf16[2,1024,256]{2,1,0:T(8,128)(2,1)} %gate_ref.1) | copy-start | bytes 3145732
  20.3 37.0 %all-to-all-start = ((bf16[64,32,512]{2,1,0:T(8,128)(2,1)}), bf16[64,32,512]{2,1,0:T(8,128)(2,1)S(1)}, u32[]{:S(2)}, u32[]{:S(2)}) async-start(bf16[64,32,512]{2,1,0:T(8,128)(2,1)} %bitcast.4), calls=%async_computation | async-start | bytes 4194304 | tf_op jit(solution)/shard_map/all_to_all | solution.py:164
  30.1 2.7 %collective-permute-start.4 = (bf16[2,1024,256]{2,1,0:T(8,128)(2,1)S(1)}, bf16[2,1024,256]{2,1,0:T(8,128)(2,1)S(1)}, u32[]{:S(2)}, u32[]{:S(2)}) collective-permute-start(bf16[2,1024,256]{2,1,0:T(8,128)(2,1)S(1)} %copy-done.4), channel_id=1, source_target_pairs={{0,1},{1,0},{2,3},{3,2},{4,5},{5,4},{6,7},{7,6},{8,9},{9,8},{10,11... | collective-permute-start | bytes 3145736 | tf_op jit(solution)/shard_map/ppermute | solution.py:158
  30.3 4.0 %collective-permute-start.5 = (bf16[2,1024,256]{2,1,0:T(8,128)(2,1)}, bf16[2,1024,256]{2,1,0:T(8,128)(2,1)S(1)}, u32[]{:S(2)}, u32[]{:S(2)}) collective-permute-start(bf16[2,1024,256]{2,1,0:T(8,128)(2,1)} %up_ref.1), channel_id=1, source_target_pairs={{0,1},{1,0},{2,3},{3,2},{4,5},{5,4},{6,7},{7,6},{8,9},{9,8},{10,11... | collective-permute-start | bytes 3145736 | tf_op jit(solution)/shard_map/ppermute | solution.py:158
  30.7 5.1 %collective-permute-start.6 = (bf16[2,512,512]{2,1,0:T(8,128)(2,1)}, bf16[2,512,512]{2,1,0:T(8,128)(2,1)S(1)}, u32[]{:S(2)}, u32[]{:S(2)}) collective-permute-start(bf16[2,512,512]{2,1,0:T(8,128)(2,1)} %down_ref.1), channel_id=1, source_target_pairs={{0,1},{1,0},{2,3},{3,2},{4,5},{5,4},{6,7},{7,6},{8,9},{9,8},{10,11... | collective-permute-start | bytes 3145736 | tf_op jit(solution)/shard_map/ppermute | solution.py:158
  32.9 1.0 copy-start.7
  34.4 1.0 copy-start.9
  35.9 1.0 copy-start.11
  57.4 1.2 %copy-start.5 = (bf16[2,1024,256]{2,1,0:T(8,128)(2,1)S(1)}, bf16[2,1024,256]{2,1,0:T(8,128)(2,1)}, u32[]{:S(2)}) copy-start(bf16[2,1024,256]{2,1,0:T(8,128)(2,1)} %up_ref.1) | copy-start | bytes 3145732
  58.6 1.2 %copy-start.6 = (bf16[2,512,512]{2,1,0:T(8,128)(2,1)S(1)}, bf16[2,512,512]{2,1,0:T(8,128)(2,1)}, u32[]{:S(2)}) copy-start(bf16[2,512,512]{2,1,0:T(8,128)(2,1)} %down_ref.1) | copy-start | bytes 3145732
  59.8 1.2 %copy-start.8 = (bf16[2,1024,256]{2,1,0:T(8,128)(2,1)S(1)}, bf16[2,1024,256]{2,1,0:T(8,128)(2,1)}, u32[]{:S(2)}) copy-start(bf16[2,1024,256]{2,1,0:T(8,128)(2,1)} %copy-done.7) | copy-start | bytes 3145732
  61.0 1.2 %copy-start.10 = (bf16[2,1024,256]{2,1,0:T(8,128)(2,1)S(1)}, bf16[2,1024,256]{2,1,0:T(8,128)(2,1)}, u32[]{:S(2)}) copy-start(bf16[2,1024,256]{2,1,0:T(8,128)(2,1)} %copy-done.9) | copy-start | bytes 3145732
  62.3 1.2 %copy-start.12 = (bf16[2,512,512]{2,1,0:T(8,128)(2,1)S(1)}, bf16[2,512,512]{2,1,0:T(8,128)(2,1)}, u32[]{:S(2)}) copy-start(bf16[2,512,512]{2,1,0:T(8,128)(2,1)} %copy-done.11) | copy-start | bytes 3145732

commit v5 on v4

--- a/solution.py
+++ b/solution.py
@@ -24,28 +24,26 @@
     return mask.astype(F32).astype(BF16)
 
 
-def block_kernel(own_ref, gain_ref, route_ref, weight_ref, out_ref, total_ref, gain_out_ref):
+def gather_kernel(own_ref, gain_ref, route_ref, weight_ref, out_ref):
     rows, half = own_ref.shape
-    out_ref[0:rows, :] = own_ref[...]
-    own = own_ref[...].astype(F32)
-    total_ref[...] = jnp.broadcast_to(jnp.sum(own * own, axis=1, keepdims=True), total_ref.shape)
-    gain_out_ref[...] = gain_ref[...]
+    out_ref[0:rows, :] = own_ref[...].astype(F32)
+    out_ref[rows : rows + 8, :] = jnp.broadcast_to(gain_ref[...], (8, half))
     weight = weight_ref[...]
     high = weight.astype(BF16).astype(F32)
     middle = (weight - high).astype(BF16).astype(F32)
     low = weight - high - middle
-    info = jnp.concatenate([route_ref[...].astype(F32), high, middle, low], axis=0)
-    out_ref[rows:, :] = jnp.zeros((INFO, half), BF16)
-    out_ref[rows:, 0:rows] = info.astype(BF16)
-
-
-def norm_kernel(block_ref, total_ref, gain_ref, other_ref, out_ref):
+    out_ref[rows + 8 :, :] = jnp.zeros((INFO, half), F32)
+    out_ref[rows + 8 :, 0:rows] = jnp.concatenate([route_ref[...].astype(F32), high, middle, low], axis=0)
+
+
+def norm_kernel(held_ref, other_ref, out_ref):
     rows, half = other_ref.shape
+    own = held_ref[0:rows, :]
     other = other_ref[...].astype(F32)
-    total = total_ref[:, 0:1] + jnp.sum(other * other, axis=1, keepdims=True)
+    total = jnp.sum(own * own, axis=1, keepdims=True) + jnp.sum(other * other, axis=1, keepdims=True)
     scale = lax.rsqrt(total / (2 * half) + EPS)
-    out_ref[0:rows, :] = (block_ref[0:rows, :].astype(F32) * scale * gain_ref[...]).astype(BF16)
-    out_ref[rows:, :] = block_ref[rows:, :]
+    out_ref[0:rows, :] = (own * scale * held_ref[rows : rows + 1, :]).astype(BF16)
+    out_ref[rows:, :] = held_ref[rows + 8 :, :].astype(BF16)
 
 
 def dispatch_kernel(place_ref, *refs):
@@ -84,26 +82,31 @@
     table_ref[...] = jnp.concatenate(slots + weights, axis=0).T
 
 
-def expert_kernel(place_ref, rows_ref, gate_ref, up_ref, gate2_ref, up2_ref, down_ref, down2_ref, out_ref):
+def hidden_part(rows_ref, at, gate_ref, up_ref, core):
+    _, _, block, half = rows_ref.shape
+    low, high = (rows_ref[at : at + 256 // block, side].reshape(256, half) for side in range(2))
+    gate, up = (dot(low, ref[core, 0:half, :]) + dot(high, ref[core, half:, :]) for ref in (gate_ref, up_ref))
+    return (gate / (1.0 + jnp.exp(-gate)) * up).astype(BF16)
+
+
+def own_kernel(place_ref, rows_ref, gate_ref, up_ref, out_ref):
+    chips, _, block, _ = rows_ref.shape
+    for at in range(0, chips, 256 // block):
+        out_ref[at * block : at * block + 256] = hidden_part(rows_ref, at, gate_ref, up_ref, place_ref[0] % 2)
+
+
+def expert_kernel(place_ref, rows_ref, own_ref, gate2_ref, up2_ref, down_ref, down2_ref, out_ref):
     core = place_ref[0] % 2
     chips, _, block, half = rows_ref.shape
-    width = gate_ref.shape[2]
+    width = own_ref.shape[1]
     sides = (core, 1 - core)
     spans = [pl.ds(pl.multiple_of(side * width, width), width) for side in sides]
     step = 256 // block
     for at in range(0, chips, step):
-        low = rows_ref[at : at + step, 0].reshape(256, half)
-        high = rows_ref[at : at + step, 1].reshape(256, half)
-
-        def through(ref):
-            return dot(low, ref[core, 0:half, :]) + dot(high, ref[core, half:, :])
-
-        hidden = []
-        for gate_half, up_half in ((gate_ref, up_ref), (gate2_ref, up2_ref)):
-            gate = through(gate_half)
-            hidden.append((gate / (1.0 + jnp.exp(-gate)) * through(up_half)).astype(BF16))
+        own = own_ref[at * block : at * block + 256]
+        other = hidden_part(rows_ref, at, gate2_ref, up2_ref, core)
         for side, down in zip(sides, (down_ref, down2_ref)):
-            result = dot(hidden[0], down[core, spans[0], :]) + dot(hidden[1], down[core, spans[1], :])
+            result = dot(own, down[core, spans[0], :]) + dot(other, down[core, spans[1], :])
             out_ref[at : at + step, side] = result.astype(BF16).reshape(step, block, half)
 
 
@@ -165,18 +168,14 @@
 
     other = swap(tokens)
     gate2, up2, down2 = swap(w_gate), swap(w_up), swap(w_down)
-    own = call(
-        block_kernel,
-        (
-            jax.ShapeDtypeStruct((rows + INFO, half), BF16),
-            jax.ShapeDtypeStruct((rows, 128), F32),
-            jax.ShapeDtypeStruct((1, half), F32),
-        ),
+    held = call(
+        gather_kernel,
+        jax.ShapeDtypeStruct((rows + 8 + INFO, half), F32),
         (tokens, norm_gain.reshape(1, half), routing.T, route_weight.T),
         rows * half,
-        4,
-    )
-    own = call(norm_kernel, jax.ShapeDtypeStruct((rows + INFO, half), BF16), (*own, other), rows * half, 4)
+        60,
+    )
+    own = call(norm_kernel, jax.ShapeDtypeStruct((rows + INFO, half), BF16), (held, other), rows * half, 4)
     opposite, before, after = shift(own, 2), shift(own, 1), shift(own, -1)
     blocks = (own, before, opposite, after)
 
@@ -192,12 +191,21 @@
         1,
     )
     arrived = exchange(sent.reshape(2 * peers, block // 2, half), plane)
+    arrived = arrived.reshape(peers, 2, block // 2, half)
+    hidden = call(
+        own_kernel,
+        jax.ShapeDtypeStruct((total // 2, width), BF16),
+        (place, arrived, w_gate, w_up),
+        total * half * width * 4,
+        12,
+        1,
+    )
     result = call(
         expert_kernel,
         jax.ShapeDtypeStruct((peers, 2, block // 2, half), BF16),
-        (place, arrived.reshape(peers, 2, block // 2, half), w_gate, w_up, gate2, up2, w_down, down2),
-        total * half * width * 12,
-        20,
+        (place, arrived, hidden, gate2, up2, w_down, down2),
+        total * half * width * 8,
+        16,
         1,
     )
     back = exchange(result.reshape(2 * peers, block // 2, half), plane)

time: 122 us -> 119 us (0.975)
  local copies, waits for them, and re-layouts: 11.9 us -> 3.47 us
  waiting for transfers between devices: 27.9 us -> 33.2 us
  Pallas kernels: 7.28 us -> 9.33 us
  starting transfers between devices: 21 us -> 19.4 us
    unnamed x26 -> x10, local copies, waits for them, and re-layouts: 11.9 us -> 3.47 us
    all_to_all x1, waiting for transfers between devices: 20.5 us -> 26.5 us  [exchange(): return lax.all_to_all(v, axes, split_axis=0, concat_axis=0, tiled=True)]
    ppermute x4, waiting for transfers between devices: 3.07 us -> 0.01 us  [swap(): return lax.ppermute(v, 'tp', [(0, 1), (1, 0)])]
    ppermute x3, waiting for transfers between devices: 4.26 us -> 6.62 us  [shift(): lax.ppermute(v, 'zh', [(i, (i + by) % columns) for i in range(columns)])]
    pallas_call x5 -> x6, Pallas kernels: 7.28 us -> 9.33 us  [call(): pl.pallas_call(kernel, out_shape=out_shape, cost_estimate=pl.CostEstimate...]
  transfers between devices with their start and end apart: 8 -> 8, of which waited for: 6 -> 3; matrix products, arithmetic and copies ran while one was open for 0% -> 0% of each run, Pallas kernels for 0% -> 2%
where the time goes in v5:
time: 119 us; the launch traced here: 118 us
  blocking collectives  52 us (44%)
  waiting for transfers between devices  33.2 us (28%)
  starting transfers between devices  19.4 us (16%)
  Pallas kernels  9.33 us (8%)
  local copies, waits for them, and re-layouts  3.47 us (3%)
    all_to_all x2, blocking collectives, exchange(): return lax.all_to_all(v, axes, split_axis=0, concat_axis=0, tiled=True)  52 us
    all_to_all x1, waiting for transfers between devices, exchange(): return lax.all_to_all(v, axes, split_axis=0, concat_axis=0, tiled=True)  26.5 us
    all_to_all x1, starting transfers between devices, exchange(): return lax.all_to_all(v, axes, split_axis=0, concat_axis=0, tiled=True)  9.34 us
    pallas_call x6, Pallas kernels, call(): pl.pallas_call(kernel, out_shape=out_shape, cost_estimate=pl.CostEstimate...  9.33 us
    ppermute x3, starting transfers between devices, shift(): lax.ppermute(v, 'zh', [(i, (i + by) % columns) for i in range(columns)])  9.29 us
    ppermute x3, waiting for transfers between devices, shift(): lax.ppermute(v, 'zh', [(i, (i + by) % columns) for i in range(columns)])  6.62 us
    unnamed x10, local copies, waits for them, and re-layouts  3.47 us
  transfers between devices with their start and end apart: 8, of which 3 were waited for; matrix products, arithmetic and copies ran while one was open for 0% of the time, Pallas kernels for 2%

profile of v5, /device:TPU:32, one launch (start us, length us, event | category | flops | bytes accessed | tf_op | source)
XLA Modules:
  0.0 118.1 jit_solution(13343621020462122664)
XLA Ops:
  0.0 0.0 collective-permute-start
  0.0 1.5 %shard_map.73.held_ref = f32[80,512]{1,0:T(8,128)} custom-call(bf16[64,512]{1,0:T(8,128)(2,1)} %own_ref.1, f32[1,512]{1,0:T(1,128)} %bitcast.13, s32[2,64]{1,0:T(2,128)} %bitcast.14, f32[2,64]{1,0:T(2,128)} %bitcast.15), custom_call_target="tpu_custom_call" | custom-call | flops 32768 | bytes 68608 | tf_op jit(solution)/shard_map/pallas_call | solution.py:141
  1.5 0.0 collective-permute-done.other_ref
  1.5 0.0 copy-start.4
  1.6 0.9 copy-done.4
  2.5 0.1 shard_map.74.refs_0_
  2.6 5.5 %collective-permute-start.3 = (bf16[72,512]{1,0:T(8,128)(2,1)S(1)}, bf16[72,512]{1,0:T(8,128)(2,1)S(1)}, u32[]{:S(2)}, u32[]{:S(2)}) collective-permute-start(bf16[72,512]{1,0:T(8,128)(2,1)S(1)} %shard_map.74.refs_0_), channel_id=1, source_target_pairs={{0,192},{64,0},{128,64},{192,128},{1,193},{65,1},{129,65},{193,129... | collective-permute-start | bytes 221192 | tf_op jit(solution)/shard_map/ppermute | solution.py:164
  8.1 1.4 %collective-permute-start.2 = (bf16[72,512]{1,0:T(8,128)(2,1)S(1)}, bf16[72,512]{1,0:T(8,128)(2,1)S(1)}, u32[]{:S(2)}, u32[]{:S(2)}) collective-permute-start(bf16[72,512]{1,0:T(8,128)(2,1)S(1)} %shard_map.74.refs_0_), channel_id=1, source_target_pairs={{0,128},{64,192},{128,0},{192,64},{1,129},{65,193},{129,1},{193,65... | collective-permute-start | bytes 221192 | tf_op jit(solution)/shard_map/ppermute | solution.py:164
  9.5 2.4 %collective-permute-start.1 = (bf16[72,512]{1,0:T(8,128)(2,1)S(1)}, bf16[72,512]{1,0:T(8,128)(2,1)S(1)}, u32[]{:S(2)}, u32[]{:S(2)}) collective-permute-start(bf16[72,512]{1,0:T(8,128)(2,1)S(1)} %shard_map.74.refs_0_), channel_id=1, source_target_pairs={{0,64},{64,128},{128,192},{192,0},{1,65},{65,129},{129,193},{193,1... | collective-permute-start | bytes 221192 | tf_op jit(solution)/shard_map/ppermute | solution.py:164
  11.9 0.0 collective-permute-done.3.refs_3_
  11.9 6.2 %collective-permute-done.2.refs_2_ = bf16[72,512]{1,0:T(8,128)(2,1)S(1)} collective-permute-done((bf16[72,512]{1,0:T(8,128)(2,1)S(1)}, bf16[72,512]{1,0:T(8,128)(2,1)S(1)}, u32[]{:S(2)}, u32[]{:S(2)}) %collective-permute-start.2) | collective-permute-done | bytes 73760 | tf_op jit(solution)/shard_map/ppermute | solution.py:164
  18.1 0.4 collective-permute-done.1.refs_1_
  18.5 1.0 shard_map.75
  19.5 0.0 copy-start
  19.6 1.3 %copy-done = bf16[32,64,512]{2,1,0:T(8,128)(2,1)} copy-done((bf16[32,64,512]{2,1,0:T(8,128)(2,1)}, bf16[32,64,512]{2,1,0:T(8,128)(2,1)S(1)}, u32[]{:S(2)}) %copy-start) | copy-done | bytes 2097176
  20.9 0.0 copy-start.1
  20.9 9.3 %all-to-all-start = ((bf16[64,32,512]{2,1,0:T(8,128)(2,1)}), bf16[64,32,512]{2,1,0:T(8,128)(2,1)S(1)}, u32[]{:S(2)}, u32[]{:S(2)}) async-start(bf16[64,32,512]{2,1,0:T(8,128)(2,1)} %bitcast.12), calls=%async_computation | async-start | bytes 4194304 | tf_op jit(solution)/shard_map/all_to_all | solution.py:167
  30.2 0.0 copy-done.1
  30.2 0.2 collective-permute-start.4
  30.4 0.4 collective-permute-start.5
  30.8 0.1 collective-permute-start.6
  31.0 26.5 %all-to-all-done = bf16[64,32,512]{2,1,0:T(8,128)(2,1)S(1)} async-done(((bf16[64,32,512]{2,1,0:T(8,128)(2,1)}), bf16[64,32,512]{2,1,0:T(8,128)(2,1)S(1)}, u32[]{:S(2)}, u32[]{:S(2)}) %all-to-all-start) | async-done | bytes 2097184 | tf_op jit(solution)/shard_map/all_to_all | solution.py:167
  57.5 0.0 copy-start.2
  57.5 1.2 %copy-done.2 = bf16[2,1024,256]{2,1,0:T(8,128)(2,1)S(1)} copy-done((bf16[2,1024,256]{2,1,0:T(8,128)(2,1)S(1)}, bf16[2,1024,256]{2,1,0:T(8,128)(2,1)}, u32[]{:S(2)}) %copy-start.2) | copy-done | bytes 1048600
  58.7 0.0 copy-start.3
  58.7 1.3 %shard_map.76.own_ref = bf16[1024,256]{1,0:T(8,128)(2,1)S(1)} custom-call(s32[1]{0:T(128)} %bitcast.place_ref, bf16[32,2,32,512]{3,2,1,0:T(8,128)(2,1)S(1)} %bitcast.8, bf16[2,1024,256]{2,1,0:T(8,128)(2,1)S(1)} %copy-done.1, bf16[2,1024,256]{2,1,0:T(8,128)(2,1)S(1)} %copy-done.2), custom_call_target="tpu_custom_call" | custom-call | flops 1073741824 | bytes 4194308 | tf_op jit(solution)/shard_map/pallas_call | solution.py:141
  60.0 0.0 collective-permute-done.4.gate2_ref
  60.0 0.0 collective-permute-done.5.up2_ref
  60.0 0.0 collective-permute-done.6.down2_ref
  60.0 0.0 copy-done.3
  60.0 4.6 %shard_map.77 = bf16[32,2,32,512]{3,2,1,0:T(8,128)(2,1)S(1)} custom-call(s32[1]{0:T(128)} %bitcast.place_ref, bf16[32,2,32,512]{3,2,1,0:T(8,128)(2,1)S(1)} %bitcast.9, bf16[1024,256]{1,0:T(8,128)(2,1)S(1)} %shard_map.76.own_ref, bf16[2,1024,256]{2,1,0:T(8,128)(2,1)} %collective-permute-done.4.gate2_ref, ...), custom_call_target="tpu_custom_call" | custom-call | flops 2147483648 | bytes 6815748 | tf_op jit(solution)/shard_map/pallas_call | solution.py:141
  64.7 34.8 %all_to_all.15 = bf16[64,32,512]{2,1,0:T(8,128)(2,1)S(1)} all-to-all(bf16[64,32,512]{2,1,0:T(8,128)(2,1)S(1)} %bitcast.10), channel_id=1, replica_groups=mesh['zh'=4,'zl'=2,'y'=4,'x'=4,'tp'=2] {'zl','y','x','tp'}, dimensions={0} | all-to-all | bytes 4194304 | tf_op jit(solution)/shard_map/all_to_all | solution.py:167
  99.5 0.8 shard_map.78
  100.3 17.2 %all_to_all.16 = bf16[4,64,512]{2,1,0:T(8,128)(2,1)S(1)} all-to-all(bf16[4,64,512]{2,1,0:T(8,128)(2,1)S(1)} %shard_map.78), channel_id=1, replica_groups=mesh['zh'=4,'zl'=2,'y'=4,'x'=4,'tp'=2] {'zh'}, dimensions={0} | all-to-all | bytes 524288 | tf_op jit(solution)/shard_map/all_to_all | solution.py:167
  117.4 0.7 reduce_sum.12
Async XLA Ops:
  0.0 1.5 %collective-permute-start = (bf16[64,512]{1,0:T(8,128)(2,1)}, bf16[64,512]{1,0:T(8,128)(2,1)S(1)}, u32[]{:S(2)}, u32[]{:S(2)}) collective-permute-start(bf16[64,512]{1,0:T(8,128)(2,1)} %own_ref.1), channel_id=1, source_target_pairs={{0,1},{1,0},{2,3},{3,2},{4,5},{5,4},{6,7},{7,6},{8,9},{9,8},{10,11... | collective-permute-start | bytes 196616 | tf_op jit(solution)/shard_map/ppermute | solution.py:161
  1.5 0.9 copy-start.4
  2.6 9.3 %collective-permute-start.3 = (bf16[72,512]{1,0:T(8,128)(2,1)S(1)}, bf16[72,512]{1,0:T(8,128)(2,1)S(1)}, u32[]{:S(2)}, u32[]{:S(2)}) collective-permute-start(bf16[72,512]{1,0:T(8,128)(2,1)S(1)} %shard_map.74.refs_0_), channel_id=1, source_target_pairs={{0,192},{64,0},{128,64},{192,128},{1,193},{65,1},{129,65},{193,129... | collective-permute-start | bytes 221192 | tf_op jit(solution)/shard_map/ppermute | solution.py:164
  8.1 10.0 %collective-permute-start.2 = (bf16[72,512]{1,0:T(8,128)(2,1)S(1)}, bf16[72,512]{1,0:T(8,128)(2,1)S(1)}, u32[]{:S(2)}, u32[]{:S(2)}) collective-permute-start(bf16[72,512]{1,0:T(8,128)(2,1)S(1)} %shard_map.74.refs_0_), channel_id=1, source_target_pairs={{0,128},{64,192},{128,0},{192,64},{1,129},{65,193},{129,1},{193,65... | collective-permute-start | bytes 221192 | tf_op jit(solution)/shard_map/ppermute | solution.py:164
  9.5 9.0 %collective-permute-start.1 = (bf16[72,512]{1,0:T(8,128)(2,1)S(1)}, bf16[72,512]{1,0:T(8,128)(2,1)S(1)}, u32[]{:S(2)}, u32[]{:S(2)}) collective-permute-start(bf16[72,512]{1,0:T(8,128)(2,1)S(1)} %shard_map.74.refs_0_), channel_id=1, source_target_pairs={{0,64},{64,128},{128,192},{192,0},{1,65},{65,129},{129,193},{193,1... | collective-permute-start | bytes 221192 | tf_op jit(solution)/shard_map/ppermute | solution.py:164
  19.5 1.3 %copy-start = (bf16[32,64,512]{2,1,0:T(8,128)(2,1)}, bf16[32,64,512]{2,1,0:T(8,128)(2,1)S(1)}, u32[]{:S(2)}) copy-start(bf16[32,64,512]{2,1,0:T(8,128)(2,1)S(1)} %get-tuple-element.7) | copy-start | bytes 6291460
  20.9 9.4 %copy-start.1 = (bf16[2,1024,256]{2,1,0:T(8,128)(2,1)S(1)}, bf16[2,1024,256]{2,1,0:T(8,128)(2,1)}, u32[]{:S(2)}) copy-start(bf16[2,1024,256]{2,1,0:T(8,128)(2,1)} %gate_ref.1) | copy-start | bytes 3145732
  20.9 36.6 %all-to-all-start = ((bf16[64,32,512]{2,1,0:T(8,128)(2,1)}), bf16[64,32,512]{2,1,0:T(8,128)(2,1)S(1)}, u32[]{:S(2)}, u32[]{:S(2)}) async-start(bf16[64,32,512]{2,1,0:T(8,128)(2,1)} %bitcast.12), calls=%async_computation | async-start | bytes 4194304 | tf_op jit(solution)/shard_map/all_to_all | solution.py:167
  30.2 29.8 %collective-permute-start.4 = (bf16[2,1024,256]{2,1,0:T(8,128)(2,1)S(1)}, bf16[2,1024,256]{2,1,0:T(8,128)(2,1)}, u32[]{:S(2)}, u32[]{:S(2)}) collective-permute-start(bf16[2,1024,256]{2,1,0:T(8,128)(2,1)S(1)} %copy-done.1), channel_id=1, source_target_pairs={{0,1},{1,0},{2,3},{3,2},{4,5},{5,4},{6,7},{7,6},{8,9},{9,8},{10,11... | collective-permute-start | bytes 3145736 | tf_op jit(solution)/shard_map/ppermute | solution.py:161
  30.4 29.6 %collective-permute-start.5 = (bf16[2,1024,256]{2,1,0:T(8,128)(2,1)}, bf16[2,1024,256]{2,1,0:T(8,128)(2,1)}, u32[]{:S(2)}, u32[]{:S(2)}) collective-permute-start(bf16[2,1024,256]{2,1,0:T(8,128)(2,1)} %up_ref.1), channel_id=1, source_target_pairs={{0,1},{1,0},{2,3},{3,2},{4,5},{5,4},{6,7},{7,6},{8,9},{9,8},{10,11... | collective-permute-start | bytes 3145736 | tf_op jit(solution)/shard_map/ppermute | solution.py:161
  30.8 29.2 %collective-permute-start.6 = (bf16[2,512,512]{2,1,0:T(8,128)(2,1)}, bf16[2,512,512]{2,1,0:T(8,128)(2,1)}, u32[]{:S(2)}, u32[]{:S(2)}) collective-permute-start(bf16[2,512,512]{2,1,0:T(8,128)(2,1)} %down_ref.1), channel_id=1, source_target_pairs={{0,1},{1,0},{2,3},{3,2},{4,5},{5,4},{6,7},{7,6},{8,9},{9,8},{10,11... | collective-permute-start | bytes 3145736 | tf_op jit(solution)/shard_map/ppermute | solution.py:161
  57.5 1.2 %copy-start.2 = (bf16[2,1024,256]{2,1,0:T(8,128)(2,1)S(1)}, bf16[2,1024,256]{2,1,0:T(8,128)(2,1)}, u32[]{:S(2)}) copy-start(bf16[2,1024,256]{2,1,0:T(8,128)(2,1)} %up_ref.1) | copy-start | bytes 3145732
  58.7 1.3 %copy-start.3 = (bf16[2,512,512]{2,1,0:T(8,128)(2,1)S(1)}, bf16[2,512,512]{2,1,0:T(8,128)(2,1)}, u32[]{:S(2)}) copy-start(bf16[2,512,512]{2,1,0:T(8,128)(2,1)} %down_ref.1) | copy-start | bytes 3145732

commit v6 on v5

--- a/solution.py
+++ b/solution.py
@@ -24,7 +24,7 @@
     return mask.astype(F32).astype(BF16)
 
 
-def gather_kernel(own_ref, gain_ref, route_ref, weight_ref, out_ref):
+def gather_kernel(place_ref, own_ref, gain_ref, route_ref, weight_ref, out_ref):
     rows, half = own_ref.shape
     out_ref[0:rows, :] = own_ref[...].astype(F32)
     out_ref[rows : rows + 8, :] = jnp.broadcast_to(gain_ref[...], (8, half))
@@ -42,13 +42,15 @@
     other = other_ref[...].astype(F32)
     total = jnp.sum(own * own, axis=1, keepdims=True) + jnp.sum(other * other, axis=1, keepdims=True)
     scale = lax.rsqrt(total / (2 * half) + EPS)
-    out_ref[0:rows, :] = (own * scale * held_ref[rows : rows + 1, :]).astype(BF16)
-    out_ref[rows:, :] = held_ref[rows + 8 :, :].astype(BF16)
-
-
-def dispatch_kernel(place_ref, *refs):
-    blocks, (out_ref, table_ref) = refs[:-2], refs[-2:]
-    rows = blocks[0].shape[0] - INFO
+    normed = (own * scale * held_ref[rows : rows + 1, :]).astype(BF16)
+    info = held_ref[rows + 8 :, :].astype(BF16)
+    for peer in range(out_ref.shape[0]):
+        out_ref[peer, 0:rows, :] = normed
+        out_ref[peer, rows:, :] = info
+
+
+def dispatch_kernel(place_ref, block_ref, out_ref, table_ref):
+    columns, rows = block_ref.shape[0], block_ref.shape[1] - INFO
     span = 2 * rows
     peers, block, half = out_ref.shape
     experts = 2 * peers
@@ -60,8 +62,8 @@
     side = iota((1, span), 1) // rows
     expert = iota((experts, span), 0)
     slots, weights = [], []
-    for pair in range(len(blocks) // 2):
-        a, b = blocks[2 * pair], blocks[2 * pair + 1]
+    for pair in range(columns // 2):
+        a, b = block_ref.at[2 * pair], block_ref.at[2 * pair + 1]
         info = jnp.concatenate([a[rows:, 0:rows].astype(F32), b[rows:, 0:rows].astype(F32)], axis=1)
         tokens = jnp.concatenate([a[0:rows, :], b[0:rows, :]], axis=0)
         picks = [info[k : k + 1].astype(jnp.int32) - first_expert for k in range(2)]
@@ -110,7 +112,7 @@
             out_ref[at : at + step, side] = result.astype(BF16).reshape(step, block, half)
 
 
-def combine_kernel(place_ref, back_ref, table_ref, out_ref):
+def combine_kernel(back_ref, table_ref, out_ref):
     columns, rows, half = out_ref.shape
     peers, block, _ = back_ref.shape
     span = 2 * rows
@@ -129,8 +131,7 @@
         total = picked[0] * table_ref[:, index : index + 1] + picked[1] * table_ref[:, index + 1 : index + 2]
         total = total.astype(BF16)
         for side in range(2):
-            to = lax.rem(place_ref[0] // 2 - (2 * pair + side) + columns, columns)
-            out_ref[to] = total[side * rows : (side + 1) * rows]
+            out_ref[2 * pair + side] = total[side * rows : (side + 1) * rows]
 
 
 def call(kernel, out_shape, args, flops, grant, scalars=0, **kw):
@@ -160,9 +161,6 @@
     def swap(v):
         return lax.ppermute(v, "tp", [(0, 1), (1, 0)])
 
-    def shift(v, by):
-        return lax.ppermute(v, "zh", [(i, (i + by) % columns) for i in range(columns)])
-
     def exchange(v, axes):
         return lax.all_to_all(v, axes, split_axis=0, concat_axis=0, tiled=True)
 
@@ -171,13 +169,13 @@
     held = call(
         gather_kernel,
         jax.ShapeDtypeStruct((rows + 8 + INFO, half), F32),
-        (tokens, norm_gain.reshape(1, half), routing.T, route_weight.T),
+        (place, tokens, norm_gain.reshape(1, half), routing.T, route_weight.T),
         rows * half,
         60,
-    )
-    own = call(norm_kernel, jax.ShapeDtypeStruct((rows + INFO, half), BF16), (held, other), rows * half, 4)
-    opposite, before, after = shift(own, 2), shift(own, 1), shift(own, -1)
-    blocks = (own, before, opposite, after)
+        1,
+    )
+    own = call(norm_kernel, jax.ShapeDtypeStruct((columns, rows + INFO, half), BF16), (held, other), rows * half, 4)
+    blocks = exchange(own, "zh")
 
     sent, table = call(
         dispatch_kernel,
@@ -185,7 +183,7 @@
             jax.ShapeDtypeStruct((peers, block, half), BF16),
             jax.ShapeDtypeStruct((2 * rows, 2 * columns), F32),
         ),
-        (place, *blocks),
+        (place, blocks),
         2 * total * 2 * rows * half,
         12,
         1,
@@ -212,10 +210,9 @@
     mixed = call(
         combine_kernel,
         jax.ShapeDtypeStruct((columns, rows, half), BF16),
-        (place, back.reshape(peers, block, half), table),
+        (back.reshape(peers, block, half), table),
         4 * total * 2 * rows * half,
         12,
-        1,
     )
     home = exchange(mixed, "zh")
     return jnp.sum(home.astype(F32), axis=0).astype(BF16)

time: 119 us -> 121 us (1.017)
  blocking collectives: 52 us -> 69.2 us
  starting transfers between devices: 19.4 us -> 9.89 us
  waiting for transfers between devices: 33.2 us -> 26.5 us
    all_to_all x2 -> x3, blocking collectives: 52 us -> 69.2 us  [exchange(): return lax.all_to_all(v, axes, split_axis=0, concat_axis=0, tiled=True)]
    ppermute x3 -> x0, starting transfers between devices: 9.29 us -> none  [shift(): lax.ppermute(v, 'zh', [(i, (i + by) % columns) for i in range(columns)])]
    ppermute x3 -> x0, waiting for transfers between devices: 6.62 us -> none  [shift(): lax.ppermute(v, 'zh', [(i, (i + by) % columns) for i in range(columns)])]
  transfers between devices with their start and end apart: 8 -> 5, of which waited for: 3 -> 1; matrix products, arithmetic and copies ran while one was open for 0% -> 0% of each run, Pallas kernels for 2% -> 2%
where the time goes in v6:
time: 121 us; the launch traced here: 119 us
  blocking collectives  69.2 us (57%)
  waiting for transfers between devices  26.5 us (22%)
  starting transfers between devices  9.89 us (8%)
  Pallas kernels  9.32 us (8%)
  local copies, waits for them, and re-layouts  3.48 us (3%)
    all_to_all x3, blocking collectives, exchange(): return lax.all_to_all(v, axes, split_axis=0, concat_axis=0, tiled=True)  69.2 us
    all_to_all x1, waiting for transfers between devices, exchange(): return lax.all_to_all(v, axes, split_axis=0, concat_axis=0, tiled=True)  26.5 us
    pallas_call x6, Pallas kernels, call(): pl.pallas_call(kernel, out_shape=out_shape, cost_estimate=pl.CostEstimate...  9.32 us
    all_to_all x1, starting transfers between devices, exchange(): return lax.all_to_all(v, axes, split_axis=0, concat_axis=0, tiled=True)  9.17 us
    unnamed x10, local copies, waits for them, and re-layouts  3.48 us
  transfers between devices with their start and end apart: 5, of which 1 were waited for; matrix products, arithmetic and copies ran while one was open for 0% of the time, Pallas kernels for 2%

profile of v6, /device:TPU:32, one launch (start us, length us, event | category | flops | bytes accessed | tf_op | source)
XLA Modules:
  0.0 119.2 jit_solution(12155523440038962277)
XLA Ops:
  0.0 0.0 collective-permute-start
  0.0 1.5 %shard_map.73.held_ref = f32[80,512]{1,0:T(8,128)} custom-call(s32[1]{0:T(128)} %bitcast.place_ref, bf16[64,512]{1,0:T(8,128)(2,1)} %own_ref.1, f32[1,512]{1,0:T(1,128)} %bitcast.13, s32[2,64]{1,0:T(2,128)} %bitcast.14, f32[2,64]{1,0:T(2,128)} %bitcast.15), custom_call_target="tpu_custom_call" | custom-call | flops 32768 | bytes 68612 | tf_op jit(solution)/shard_map/pallas_call | solution.py:142
  1.5 0.0 collective-permute-done.other_ref
  1.5 0.0 copy-start.4
  1.5 0.9 copy-done.4
  2.5 0.1 shard_map.74
  2.6 20.1 %all_to_all.20.block_ref = bf16[4,72,512]{2,1,0:T(8,128)(2,1)S(1)} all-to-all(bf16[4,72,512]{2,1,0:T(8,128)(2,1)S(1)} %shard_map.74), channel_id=1, replica_groups=mesh['zh'=4,'zl'=2,'y'=4,'x'=4,'tp'=2] {'zh'}, dimensions={0} | all-to-all | bytes 589824 | tf_op jit(solution)/shard_map/all_to_all | solution.py:165
  22.6 1.0 shard_map.75
  23.7 0.0 copy-start
  23.7 1.3 %copy-done = bf16[32,64,512]{2,1,0:T(8,128)(2,1)} copy-done((bf16[32,64,512]{2,1,0:T(8,128)(2,1)}, bf16[32,64,512]{2,1,0:T(8,128)(2,1)S(1)}, u32[]{:S(2)}) %copy-start) | copy-done | bytes 2097176
  25.0 0.0 copy-start.1
  25.0 9.2 %all-to-all-start.1 = ((bf16[64,32,512]{2,1,0:T(8,128)(2,1)}), bf16[64,32,512]{2,1,0:T(8,128)(2,1)S(1)}, u32[]{:S(2)}, u32[]{:S(2)}) async-start(bf16[64,32,512]{2,1,0:T(8,128)(2,1)} %bitcast.12), calls=%async_computation.1 | async-start | bytes 4194304 | tf_op jit(solution)/shard_map/all_to_all | solution.py:165
  34.2 0.0 copy-done.1
  34.2 0.2 collective-permute-start.1
  34.4 0.4 collective-permute-start.2
  34.8 0.1 collective-permute-start.3
  35.0 26.5 %all-to-all-done.1 = bf16[64,32,512]{2,1,0:T(8,128)(2,1)S(1)} async-done(((bf16[64,32,512]{2,1,0:T(8,128)(2,1)}), bf16[64,32,512]{2,1,0:T(8,128)(2,1)S(1)}, u32[]{:S(2)}, u32[]{:S(2)}) %all-to-all-start.1) | async-done | bytes 2097184 | tf_op jit(solution)/shard_map/all_to_all | solution.py:165
  61.5 0.0 copy-start.2
  61.5 1.2 %copy-done.2 = bf16[2,1024,256]{2,1,0:T(8,128)(2,1)S(1)} copy-done((bf16[2,1024,256]{2,1,0:T(8,128)(2,1)S(1)}, bf16[2,1024,256]{2,1,0:T(8,128)(2,1)}, u32[]{:S(2)}) %copy-start.2) | copy-done | bytes 1048600
  62.7 0.0 copy-start.3
  62.7 1.3 %shard_map.76.own_ref = bf16[1024,256]{1,0:T(8,128)(2,1)S(1)} custom-call(s32[1]{0:T(128)} %bitcast.place_ref, bf16[32,2,32,512]{3,2,1,0:T(8,128)(2,1)S(1)} %bitcast.8, bf16[2,1024,256]{2,1,0:T(8,128)(2,1)S(1)} %copy-done.1, bf16[2,1024,256]{2,1,0:T(8,128)(2,1)S(1)} %copy-done.2), custom_call_target="tpu_custom_call" | custom-call | flops 1073741824 | bytes 4194308 | tf_op jit(solution)/shard_map/pallas_call | solution.py:142
  64.0 0.0 collective-permute-done.1.gate2_ref
  64.0 0.0 collective-permute-done.2.up2_ref
  64.0 0.0 collective-permute-done.3.down2_ref
  64.0 0.0 copy-done.3
  64.0 4.6 %shard_map.77 = bf16[32,2,32,512]{3,2,1,0:T(8,128)(2,1)S(1)} custom-call(s32[1]{0:T(128)} %bitcast.place_ref, bf16[32,2,32,512]{3,2,1,0:T(8,128)(2,1)S(1)} %bitcast.9, bf16[1024,256]{1,0:T(8,128)(2,1)S(1)} %shard_map.76.own_ref, bf16[2,1024,256]{2,1,0:T(8,128)(2,1)} %collective-permute-done.1.gate2_ref, ...), custom_call_target="tpu_custom_call" | custom-call | flops 2147483648 | bytes 6815748 | tf_op jit(solution)/shard_map/pallas_call | solution.py:142
  68.6 34.8 %all_to_all.21 = bf16[64,32,512]{2,1,0:T(8,128)(2,1)S(1)} all-to-all(bf16[64,32,512]{2,1,0:T(8,128)(2,1)S(1)} %bitcast.10), channel_id=1, replica_groups=mesh['zh'=4,'zl'=2,'y'=4,'x'=4,'tp'=2] {'zl','y','x','tp'}, dimensions={0} | all-to-all | bytes 4194304 | tf_op jit(solution)/shard_map/all_to_all | solution.py:165
  103.5 0.8 shard_map.78
  104.2 14.3 %all_to_all.22 = bf16[4,64,512]{2,1,0:T(8,128)(2,1)S(1)} all-to-all(bf16[4,64,512]{2,1,0:T(8,128)(2,1)S(1)} %shard_map.78), channel_id=1, replica_groups=mesh['zh'=4,'zl'=2,'y'=4,'x'=4,'tp'=2] {'zh'}, dimensions={0} | all-to-all | bytes 524288 | tf_op jit(solution)/shard_map/all_to_all | solution.py:165
  118.5 0.7 reduce_sum.12
Async XLA Ops:
  0.0 1.5 %collective-permute-start = (bf16[64,512]{1,0:T(8,128)(2,1)}, bf16[64,512]{1,0:T(8,128)(2,1)S(1)}, u32[]{:S(2)}, u32[]{:S(2)}) collective-permute-start(bf16[64,512]{1,0:T(8,128)(2,1)} %own_ref.1), channel_id=1, source_target_pairs={{0,1},{1,0},{2,3},{3,2},{4,5},{5,4},{6,7},{7,6},{8,9},{9,8},{10,11... | collective-permute-start | bytes 196616 | tf_op jit(solution)/shard_map/ppermute | solution.py:162
  1.5 0.9 copy-start.4
  23.7 1.3 %copy-start = (bf16[32,64,512]{2,1,0:T(8,128)(2,1)}, bf16[32,64,512]{2,1,0:T(8,128)(2,1)S(1)}, u32[]{:S(2)}) copy-start(bf16[32,64,512]{2,1,0:T(8,128)(2,1)S(1)} %get-tuple-element.7) | copy-start | bytes 6291460
  25.0 9.2 %copy-start.1 = (bf16[2,1024,256]{2,1,0:T(8,128)(2,1)S(1)}, bf16[2,1024,256]{2,1,0:T(8,128)(2,1)}, u32[]{:S(2)}) copy-start(bf16[2,1024,256]{2,1,0:T(8,128)(2,1)} %gate_ref.1) | copy-start | bytes 3145732
  25.0 36.4 %all-to-all-start.1 = ((bf16[64,32,512]{2,1,0:T(8,128)(2,1)}), bf16[64,32,512]{2,1,0:T(8,128)(2,1)S(1)}, u32[]{:S(2)}, u32[]{:S(2)}) async-start(bf16[64,32,512]{2,1,0:T(8,128)(2,1)} %bitcast.12), calls=%async_computation.1 | async-start | bytes 4194304 | tf_op jit(solution)/shard_map/all_to_all | solution.py:165
  34.2 29.8 %collective-permute-start.1 = (bf16[2,1024,256]{2,1,0:T(8,128)(2,1)S(1)}, bf16[2,1024,256]{2,1,0:T(8,128)(2,1)}, u32[]{:S(2)}, u32[]{:S(2)}) collective-permute-start(bf16[2,1024,256]{2,1,0:T(8,128)(2,1)S(1)} %copy-done.1), channel_id=1, source_target_pairs={{0,1},{1,0},{2,3},{3,2},{4,5},{5,4},{6,7},{7,6},{8,9},{9,8},{10,11... | collective-permute-start | bytes 3145736 | tf_op jit(solution)/shard_map/ppermute | solution.py:162
  34.4 29.6 %collective-permute-start.2 = (bf16[2,1024,256]{2,1,0:T(8,128)(2,1)}, bf16[2,1024,256]{2,1,0:T(8,128)(2,1)}, u32[]{:S(2)}, u32[]{:S(2)}) collective-permute-start(bf16[2,1024,256]{2,1,0:T(8,128)(2,1)} %up_ref.1), channel_id=1, source_target_pairs={{0,1},{1,0},{2,3},{3,2},{4,5},{5,4},{6,7},{7,6},{8,9},{9,8},{10,11... | collective-permute-start | bytes 3145736 | tf_op jit(solution)/shard_map/ppermute | solution.py:162
  34.8 29.2 %collective-permute-start.3 = (bf16[2,512,512]{2,1,0:T(8,128)(2,1)}, bf16[2,512,512]{2,1,0:T(8,128)(2,1)}, u32[]{:S(2)}, u32[]{:S(2)}) collective-permute-start(bf16[2,512,512]{2,1,0:T(8,128)(2,1)} %down_ref.1), channel_id=1, source_target_pairs={{0,1},{1,0},{2,3},{3,2},{4,5},{5,4},{6,7},{7,6},{8,9},{9,8},{10,11... | collective-permute-start | bytes 3145736 | tf_op jit(solution)/shard_map/ppermute | solution.py:162
  61.5 1.2 %copy-start.2 = (bf16[2,1024,256]{2,1,0:T(8,128)(2,1)S(1)}, bf16[2,1024,256]{2,1,0:T(8,128)(2,1)}, u32[]{:S(2)}) copy-start(bf16[2,1024,256]{2,1,0:T(8,128)(2,1)} %up_ref.1) | copy-start | bytes 3145732
  62.7 1.3 %copy-start.3 = (bf16[2,512,512]{2,1,0:T(8,128)(2,1)S(1)}, bf16[2,512,512]{2,1,0:T(8,128)(2,1)}, u32[]{:S(2)}) copy-start(bf16[2,512,512]{2,1,0:T(8,128)(2,1)} %down_ref.1) | copy-start | bytes 3145732

commit v7 on v5

--- a/solution.py
+++ b/solution.py
@@ -110,8 +110,8 @@
             out_ref[at : at + step, side] = result.astype(BF16).reshape(step, block, half)
 
 
-def combine_kernel(place_ref, back_ref, table_ref, out_ref):
-    columns, rows, half = out_ref.shape
+def combine_kernel(back_ref, table_ref, *out_refs):
+    columns, (rows, half) = len(out_refs), out_refs[0].shape
     peers, block, _ = back_ref.shape
     span = 2 * rows
     for pair in range(columns // 2):
@@ -129,8 +129,7 @@
         total = picked[0] * table_ref[:, index : index + 1] + picked[1] * table_ref[:, index + 1 : index + 2]
         total = total.astype(BF16)
         for side in range(2):
-            to = lax.rem(place_ref[0] // 2 - (2 * pair + side) + columns, columns)
-            out_ref[to] = total[side * rows : (side + 1) * rows]
+            out_refs[2 * pair + side][...] = total[side * rows : (side + 1) * rows]
 
 
 def call(kernel, out_shape, args, flops, grant, scalars=0, **kw):
@@ -211,14 +210,13 @@
     back = exchange(result.reshape(2 * peers, block // 2, half), plane)
     mixed = call(
         combine_kernel,
-        jax.ShapeDtypeStruct((columns, rows, half), BF16),
-        (place, back.reshape(peers, block, half), table),
+        (jax.ShapeDtypeStruct((rows, half), BF16),) * columns,
+        (back.reshape(peers, block, half), table),
         4 * total * 2 * rows * half,
         12,
-        1,
-    )
-    home = exchange(mixed, "zh")
-    return jnp.sum(home.astype(F32), axis=0).astype(BF16)
+    )
+    home = [shift(mixed[by], -by) for by in (2, 1, 3)]
+    return sum((part.astype(F32) for part in home), mixed[0].astype(F32)).astype(BF16)
 
 
 def solution(mesh):

time: 119 us -> 116 us (0.975)
  the two profiles are of different devices: /device:TPU:32 before, /device:TPU:1 now
where the time goes in v7:
time: 116 us; the launch traced here: 115 us
  waiting for transfers between devices  38 us (33%)
  blocking collectives  34.8 us (30%)
  starting transfers between devices  29 us (25%)
  Pallas kernels  9.34 us (8%)
  local copies, waits for them, and re-layouts  3.48 us (3%)
    all_to_all x1, blocking collectives, exchange(): return lax.all_to_all(v, axes, split_axis=0, concat_axis=0, tiled=True)  34.8 us
    all_to_all x1, waiting for transfers between devices, exchange(): return lax.all_to_all(v, axes, split_axis=0, concat_axis=0, tiled=True)  26.5 us
    ppermute x6, starting transfers between devices, shift(): lax.ppermute(v, 'zh', [(i, (i + by) % columns) for i in range(columns)])  14.2 us
    ppermute x6, waiting for transfers between devices, shift(): lax.ppermute(v, 'zh', [(i, (i + by) % columns) for i in range(columns)])  11.5 us
    all_to_all x1, starting transfers between devices, exchange(): return lax.all_to_all(v, axes, split_axis=0, concat_axis=0, tiled=True)  10.6 us
    pallas_call x6, Pallas kernels, call(): pl.pallas_call(kernel, out_shape=out_shape, cost_estimate=pl.CostEstimate...  9.34 us
    ppermute x4, starting transfers between devices, swap(): return lax.ppermute(v, 'tp', [(0, 1), (1, 0)])  4.25 us
    unnamed x10, local copies, waits for them, and re-layouts  3.48 us
  transfers between devices with their start and end apart: 11, of which 5 were waited for; matrix products, arithmetic and copies ran while one was open for 0% of the time, Pallas kernels for 2%

profile of v7, /device:TPU:1, one launch (start us, length us, event | category | flops | bytes accessed | tf_op | source)
XLA Modules:
  0.0 115.4 jit_solution(14537000930693518705)
XLA Ops:
  0.0 3.2 %collective-permute-start = (bf16[64,512]{1,0:T(8,128)(2,1)}, bf16[64,512]{1,0:T(8,128)(2,1)S(1)}, u32[]{:S(2)}, u32[]{:S(2)}) collective-permute-start(bf16[64,512]{1,0:T(8,128)(2,1)} %own_ref.1), channel_id=1, source_target_pairs={{0,1},{1,0},{2,3},{3,2},{4,5},{5,4},{6,7},{7,6},{8,9},{9,8},{10,11... | collective-permute-start | bytes 196616 | tf_op jit(solution)/shard_map/ppermute | solution.py:160
  3.2 1.5 %shard_map.73.held_ref = f32[80,512]{1,0:T(8,128)} custom-call(bf16[64,512]{1,0:T(8,128)(2,1)} %own_ref.1, f32[1,512]{1,0:T(1,128)} %bitcast.13, s32[2,64]{1,0:T(2,128)} %bitcast.14, f32[2,64]{1,0:T(2,128)} %bitcast.15), custom_call_target="tpu_custom_call" | custom-call | flops 32768 | bytes 68608 | tf_op jit(solution)/shard_map/pallas_call | solution.py:140
  4.7 0.0 collective-permute-done.other_ref
  4.7 0.0 copy-start.4
  4.8 0.9 copy-done.4
  5.7 0.1 shard_map.74.refs_0_
  5.8 4.4 %collective-permute-start.3 = (bf16[72,512]{1,0:T(8,128)(2,1)S(1)}, bf16[72,512]{1,0:T(8,128)(2,1)S(1)}, u32[]{:S(2)}, u32[]{:S(2)}) collective-permute-start(bf16[72,512]{1,0:T(8,128)(2,1)S(1)} %shard_map.74.refs_0_), channel_id=1, source_target_pairs={{0,192},{64,0},{128,64},{192,128},{1,193},{65,1},{129,65},{193,129... | collective-permute-start | bytes 221192 | tf_op jit(solution)/shard_map/ppermute | solution.py:163
  10.2 1.0 collective-permute-start.2
  11.2 2.3 %collective-permute-start.1 = (bf16[72,512]{1,0:T(8,128)(2,1)S(1)}, bf16[72,512]{1,0:T(8,128)(2,1)S(1)}, u32[]{:S(2)}, u32[]{:S(2)}) collective-permute-start(bf16[72,512]{1,0:T(8,128)(2,1)S(1)} %shard_map.74.refs_0_), channel_id=1, source_target_pairs={{0,64},{64,128},{128,192},{192,0},{1,65},{65,129},{129,193},{193,1... | collective-permute-start | bytes 221192 | tf_op jit(solution)/shard_map/ppermute | solution.py:163
  13.4 0.0 collective-permute-done.3.refs_3_
  13.4 4.2 %collective-permute-done.2.refs_2_ = bf16[72,512]{1,0:T(8,128)(2,1)S(1)} collective-permute-done((bf16[72,512]{1,0:T(8,128)(2,1)S(1)}, bf16[72,512]{1,0:T(8,128)(2,1)S(1)}, u32[]{:S(2)}, u32[]{:S(2)}) %collective-permute-start.2) | collective-permute-done | bytes 73760 | tf_op jit(solution)/shard_map/ppermute | solution.py:163
  17.6 0.9 collective-permute-done.1.refs_1_
  18.6 1.0 shard_map.75
  19.6 0.0 copy-start
  19.6 1.3 %copy-done = bf16[32,64,512]{2,1,0:T(8,128)(2,1)} copy-done((bf16[32,64,512]{2,1,0:T(8,128)(2,1)}, bf16[32,64,512]{2,1,0:T(8,128)(2,1)S(1)}, u32[]{:S(2)}) %copy-start) | copy-done | bytes 2097176
  20.9 0.0 copy-start.1
  20.9 10.6 %all-to-all-start = ((bf16[64,32,512]{2,1,0:T(8,128)(2,1)}), bf16[64,32,512]{2,1,0:T(8,128)(2,1)S(1)}, u32[]{:S(2)}, u32[]{:S(2)}) async-start(bf16[64,32,512]{2,1,0:T(8,128)(2,1)} %bitcast.12), calls=%async_computation | async-start | bytes 4194304 | tf_op jit(solution)/shard_map/all_to_all | solution.py:166
  31.5 0.0 copy-done.1
  31.5 0.5 collective-permute-start.4
  32.1 0.1 collective-permute-start.5
  32.2 0.4 collective-permute-start.6
  32.6 26.5 %all-to-all-done = bf16[64,32,512]{2,1,0:T(8,128)(2,1)S(1)} async-done(((bf16[64,32,512]{2,1,0:T(8,128)(2,1)}), bf16[64,32,512]{2,1,0:T(8,128)(2,1)S(1)}, u32[]{:S(2)}, u32[]{:S(2)}) %all-to-all-start) | async-done | bytes 2097184 | tf_op jit(solution)/shard_map/all_to_all | solution.py:166
  59.1 0.0 copy-start.2
  59.1 1.2 %copy-done.2 = bf16[2,1024,256]{2,1,0:T(8,128)(2,1)S(1)} copy-done((bf16[2,1024,256]{2,1,0:T(8,128)(2,1)S(1)}, bf16[2,1024,256]{2,1,0:T(8,128)(2,1)}, u32[]{:S(2)}) %copy-start.2) | copy-done | bytes 1048600
  60.3 0.0 copy-start.3
  60.3 1.3 %shard_map.76.own_ref = bf16[1024,256]{1,0:T(8,128)(2,1)S(1)} custom-call(s32[1]{0:T(128)} %bitcast.place_ref, bf16[32,2,32,512]{3,2,1,0:T(8,128)(2,1)S(1)} %bitcast.8, bf16[2,1024,256]{2,1,0:T(8,128)(2,1)S(1)} %copy-done.1, bf16[2,1024,256]{2,1,0:T(8,128)(2,1)S(1)} %copy-done.2), custom_call_target="tpu_custom_call" | custom-call | flops 1073741824 | bytes 4194308 | tf_op jit(solution)/shard_map/pallas_call | solution.py:140
  61.6 0.0 collective-permute-done.4.gate2_ref
  61.6 0.0 collective-permute-done.5.up2_ref
  61.6 0.0 collective-permute-done.6.down2_ref
  61.6 0.0 copy-done.3
  61.6 4.6 %shard_map.77 = bf16[32,2,32,512]{3,2,1,0:T(8,128)(2,1)S(1)} custom-call(s32[1]{0:T(128)} %bitcast.place_ref, bf16[32,2,32,512]{3,2,1,0:T(8,128)(2,1)S(1)} %bitcast.9, bf16[1024,256]{1,0:T(8,128)(2,1)S(1)} %shard_map.76.own_ref, bf16[2,1024,256]{2,1,0:T(8,128)(2,1)} %collective-permute-done.4.gate2_ref, ...), custom_call_target="tpu_custom_call" | custom-call | flops 2147483648 | bytes 6815748 | tf_op jit(solution)/shard_map/pallas_call | solution.py:140
  66.2 34.8 %all_to_all.10 = bf16[64,32,512]{2,1,0:T(8,128)(2,1)S(1)} all-to-all(bf16[64,32,512]{2,1,0:T(8,128)(2,1)S(1)} %bitcast.10), channel_id=1, replica_groups=mesh['zh'=4,'zl'=2,'y'=4,'x'=4,'tp'=2] {'zl','y','x','tp'}, dimensions={0} | all-to-all | bytes 4194304 | tf_op jit(solution)/shard_map/all_to_all | solution.py:166
  101.0 0.8 shard_map.78
  101.8 4.2 %collective-permute-start.7 = (bf16[64,512]{1,0:T(8,128)(2,1)S(1)}, bf16[64,512]{1,0:T(8,128)(2,1)S(1)}, u32[]{:S(2)}, u32[]{:S(2)}) collective-permute-start(bf16[64,512]{1,0:T(8,128)(2,1)S(1)} %get-tuple-element.14), channel_id=1, source_target_pairs={{0,128},{64,192},{128,0},{192,64},{1,129},{65,193},{129,1},{193,65... | collective-permute-start | bytes 196616 | tf_op jit(solution)/shard_map/ppermute | solution.py:163
  106.0 0.1 collective-permute-start.8
  106.1 2.2 %collective-permute-start.9 = (bf16[64,512]{1,0:T(8,128)(2,1)S(1)}, bf16[64,512]{1,0:T(8,128)(2,1)S(1)}, u32[]{:S(2)}, u32[]{:S(2)}) collective-permute-start(bf16[64,512]{1,0:T(8,128)(2,1)S(1)} %get-tuple-element.16), channel_id=1, source_target_pairs={{0,64},{64,128},{128,192},{192,0},{1,65},{65,129},{129,193},{193,1... | collective-permute-start | bytes 196616 | tf_op jit(solution)/shard_map/ppermute | solution.py:163
  108.3 0.7 collective-permute-done.7
  109.0 5.7 %collective-permute-done.8 = bf16[64,512]{1,0:T(8,128)(2,1)S(1)} collective-permute-done((bf16[64,512]{1,0:T(8,128)(2,1)S(1)}, bf16[64,512]{1,0:T(8,128)(2,1)S(1)}, u32[]{:S(2)}, u32[]{:S(2)}) %collective-permute-start.8) | collective-permute-done | bytes 65568 | tf_op jit(solution)/shard_map/ppermute | solution.py:163
  114.7 0.0 collective-permute-done.9
  114.7 0.7 add_convert_fusion
Async XLA Ops:
  0.0 4.7 %collective-permute-start = (bf16[64,512]{1,0:T(8,128)(2,1)}, bf16[64,512]{1,0:T(8,128)(2,1)S(1)}, u32[]{:S(2)}, u32[]{:S(2)}) collective-permute-start(bf16[64,512]{1,0:T(8,128)(2,1)} %own_ref.1), channel_id=1, source_target_pairs={{0,1},{1,0},{2,3},{3,2},{4,5},{5,4},{6,7},{7,6},{8,9},{9,8},{10,11... | collective-permute-start | bytes 196616 | tf_op jit(solution)/shard_map/ppermute | solution.py:160
  4.7 0.9 copy-start.4
  5.8 7.6 %collective-permute-start.3 = (bf16[72,512]{1,0:T(8,128)(2,1)S(1)}, bf16[72,512]{1,0:T(8,128)(2,1)S(1)}, u32[]{:S(2)}, u32[]{:S(2)}) collective-permute-start(bf16[72,512]{1,0:T(8,128)(2,1)S(1)} %shard_map.74.refs_0_), channel_id=1, source_target_pairs={{0,192},{64,0},{128,64},{192,128},{1,193},{65,1},{129,65},{193,129... | collective-permute-start | bytes 221192 | tf_op jit(solution)/shard_map/ppermute | solution.py:163
  10.2 7.5 %collective-permute-start.2 = (bf16[72,512]{1,0:T(8,128)(2,1)S(1)}, bf16[72,512]{1,0:T(8,128)(2,1)S(1)}, u32[]{:S(2)}, u32[]{:S(2)}) collective-permute-start(bf16[72,512]{1,0:T(8,128)(2,1)S(1)} %shard_map.74.refs_0_), channel_id=1, source_target_pairs={{0,128},{64,192},{128,0},{192,64},{1,129},{65,193},{129,1},{193,65... | collective-permute-start | bytes 221192 | tf_op jit(solution)/shard_map/ppermute | solution.py:163
  11.2 7.4 %collective-permute-start.1 = (bf16[72,512]{1,0:T(8,128)(2,1)S(1)}, bf16[72,512]{1,0:T(8,128)(2,1)S(1)}, u32[]{:S(2)}, u32[]{:S(2)}) collective-permute-start(bf16[72,512]{1,0:T(8,128)(2,1)S(1)} %shard_map.74.refs_0_), channel_id=1, source_target_pairs={{0,64},{64,128},{128,192},{192,0},{1,65},{65,129},{129,193},{193,1... | collective-permute-start | bytes 221192 | tf_op jit(solution)/shard_map/ppermute | solution.py:163
  19.6 1.3 %copy-start = (bf16[32,64,512]{2,1,0:T(8,128)(2,1)}, bf16[32,64,512]{2,1,0:T(8,128)(2,1)S(1)}, u32[]{:S(2)}) copy-start(bf16[32,64,512]{2,1,0:T(8,128)(2,1)S(1)} %get-tuple-element.11) | copy-start | bytes 6291460
  20.9 10.6 %copy-start.1 = (bf16[2,1024,256]{2,1,0:T(8,128)(2,1)S(1)}, bf16[2,1024,256]{2,1,0:T(8,128)(2,1)}, u32[]{:S(2)}) copy-start(bf16[2,1024,256]{2,1,0:T(8,128)(2,1)} %gate_ref.1) | copy-start | bytes 3145732
  20.9 38.1 %all-to-all-start = ((bf16[64,32,512]{2,1,0:T(8,128)(2,1)}), bf16[64,32,512]{2,1,0:T(8,128)(2,1)S(1)}, u32[]{:S(2)}, u32[]{:S(2)}) async-start(bf16[64,32,512]{2,1,0:T(8,128)(2,1)} %bitcast.12), calls=%async_computation | async-start | bytes 4194304 | tf_op jit(solution)/shard_map/all_to_all | solution.py:166
  31.5 30.0 %collective-permute-start.4 = (bf16[2,1024,256]{2,1,0:T(8,128)(2,1)S(1)}, bf16[2,1024,256]{2,1,0:T(8,128)(2,1)}, u32[]{:S(2)}, u32[]{:S(2)}) collective-permute-start(bf16[2,1024,256]{2,1,0:T(8,128)(2,1)S(1)} %copy-done.1), channel_id=1, source_target_pairs={{0,1},{1,0},{2,3},{3,2},{4,5},{5,4},{6,7},{7,6},{8,9},{9,8},{10,11... | collective-permute-start | bytes 3145736 | tf_op jit(solution)/shard_map/ppermute | solution.py:160
  32.1 29.5 %collective-permute-start.5 = (bf16[2,1024,256]{2,1,0:T(8,128)(2,1)}, bf16[2,1024,256]{2,1,0:T(8,128)(2,1)}, u32[]{:S(2)}, u32[]{:S(2)}) collective-permute-start(bf16[2,1024,256]{2,1,0:T(8,128)(2,1)} %up_ref.1), channel_id=1, source_target_pairs={{0,1},{1,0},{2,3},{3,2},{4,5},{5,4},{6,7},{7,6},{8,9},{9,8},{10,11... | collective-permute-start | bytes 3145736 | tf_op jit(solution)/shard_map/ppermute | solution.py:160
  32.2 29.4 %collective-permute-start.6 = (bf16[2,512,512]{2,1,0:T(8,128)(2,1)}, bf16[2,512,512]{2,1,0:T(8,128)(2,1)}, u32[]{:S(2)}, u32[]{:S(2)}) collective-permute-start(bf16[2,512,512]{2,1,0:T(8,128)(2,1)} %down_ref.1), channel_id=1, source_target_pairs={{0,1},{1,0},{2,3},{3,2},{4,5},{5,4},{6,7},{7,6},{8,9},{9,8},{10,11... | collective-permute-start | bytes 3145736 | tf_op jit(solution)/shard_map/ppermute | solution.py:160
  59.1 1.2 %copy-start.2 = (bf16[2,1024,256]{2,1,0:T(8,128)(2,1)S(1)}, bf16[2,1024,256]{2,1,0:T(8,128)(2,1)}, u32[]{:S(2)}) copy-start(bf16[2,1024,256]{2,1,0:T(8,128)(2,1)} %up_ref.1) | copy-start | bytes 3145732
  60.3 1.3 %copy-start.3 = (bf16[2,512,512]{2,1,0:T(8,128)(2,1)S(1)}, bf16[2,512,512]{2,1,0:T(8,128)(2,1)}, u32[]{:S(2)}) copy-start(bf16[2,512,512]{2,1,0:T(8,128)(2,1)} %down_ref.1) | copy-start | bytes 3145732
  101.8 7.2 %collective-permute-start.7 = (bf16[64,512]{1,0:T(8,128)(2,1)S(1)}, bf16[64,512]{1,0:T(8,128)(2,1)S(1)}, u32[]{:S(2)}, u32[]{:S(2)}) collective-permute-start(bf16[64,512]{1,0:T(8,128)(2,1)S(1)} %get-tuple-element.14), channel_id=1, source_target_pairs={{0,128},{64,192},{128,0},{192,64},{1,129},{65,193},{129,1},{193,65... | collective-permute-start | bytes 196616 | tf_op jit(solution)/shard_map/ppermute | solution.py:163
  106.0 8.8 %collective-permute-start.8 = (bf16[64,512]{1,0:T(8,128)(2,1)S(1)}, bf16[64,512]{1,0:T(8,128)(2,1)S(1)}, u32[]{:S(2)}, u32[]{:S(2)}) collective-permute-start(bf16[64,512]{1,0:T(8,128)(2,1)S(1)} %get-tuple-element.15), channel_id=1, source_target_pairs={{0,192},{64,0},{128,64},{192,128},{1,193},{65,1},{129,65},{193,129... | collective-permute-start | bytes 196616 | tf_op jit(solution)/shard_map/ppermute | solution.py:163
  106.1 8.6 %collective-permute-start.9 = (bf16[64,512]{1,0:T(8,128)(2,1)S(1)}, bf16[64,512]{1,0:T(8,128)(2,1)S(1)}, u32[]{:S(2)}, u32[]{:S(2)}) collective-permute-start(bf16[64,512]{1,0:T(8,128)(2,1)S(1)} %get-tuple-element.16), channel_id=1, source_target_pairs={{0,64},{64,128},{128,192},{192,0},{1,65},{65,129},{129,193},{193,1... | collective-permute-start | bytes 196616 | tf_op jit(solution)/shard_map/ppermute | solution.py:163
